TPU v7x, 512 devices: a whole 4x8x8 slice. The times are simulated.
512 devices in a mesh: sp: 128 (over z, y, core), tp: 4 (over x).
Axes of the slice: x: 4, y: 8, z: 8, core: 2. Of those that a mesh axis runs over, the one named last changes fastest.
Arguments:
- tokens: bfloat16 [32768, 2048], P(('sp', 'tp')), may hold values from -6 to 6
- norm_gain: float32 [2048], replicated, may hold values from 0.1 to 1.9
- ret_query: bfloat16 [2048, 1024], P('sp', 'tp'), may hold values from -0.125 to 0.125
- ret_key: bfloat16 [2048, 1024], P('sp', 'tp'), may hold values from -0.125 to 0.125
- ret_value: bfloat16 [2048, 2048], P('sp', 'tp'), may hold values from -0.125 to 0.125
- log_decay: float32 [8, 32768], P('tp', 'sp'), may hold values from -2 to 0, as said below
- att_query: bfloat16 [2048, 2048], P('sp', 'tp')
- att_key: bfloat16 [2048, 256], P('sp', 'tp')
- att_value: bfloat16 [2048, 256], P('sp', 'tp'), may hold values from -0.125 to 0.125
- sink_logits: float32 [32], P('tp'), may hold values from 3 to 6
- ret_out: bfloat16 [2048, 2048], P('tp', 'sp'), may hold values from -0.125 to 0.125
- att_out: bfloat16 [2048, 2048], P('tp', 'sp'), may hold values from -1 to 1
Outputs:
- mixed: bfloat16 [32768, 2048], P(('sp', 'tp'))
Inputs may be any that keep to these rules, and one draw needn't show every extreme that they name: `log_decay`: strictly negative.
All inputs are finite; a program needn't handle non-finite values.
Results may differ from a plain program's by a relative error of at most 0.013.
Values may be sent and summed in bfloat16 or wider, within the bound.
No kernel may reach another device: no remote copies, remote signals or barrier semaphores. Data moves between devices by JAX's collectives and lax.ppermute only.
A program may use at most 128 MiB of HBM per device.

v0:
```python
import jax
import jax.numpy as jnp
from jax import lax
from jax.sharding import Mesh
from jax.sharding import PartitionSpec as P

RETAIN_KEY_SIZE = 128
V_DIM = 256
HEAD_DIM = 64
WINDOW = 128
BLOCK = 128
SP = ("sp_0", "sp_1", "sp_2")
SP_TP = ("sp_0", "sp_1", "sp_2", "tp")


epsilon = 1e-05
rope_base = 10000.0
masked_out = -1e30


def neutral_like(value, identity):
    return jax.tree.map(
        lambda a, e: jnp.broadcast_to(jnp.asarray(e, a.dtype), a.shape), value, identity
    )


def entering(value, axes, combine, identity):
    before = start = neutral_like(value, identity)
    so_far = value
    for axis in reversed(axes):
        size, here = (lax.axis_size(axis), lax.axis_index(axis))
        pieces = jax.tree.map(lambda part: lax.all_gather(part, axis), so_far)
        inside, so_far = (start, start)
        for k in range(size):
            passed = k < here
            so_far = combine(so_far, jax.tree.map(lambda part: part[k], pieces))
            inside = jax.tree.map(lambda new, old: jnp.where(passed, new, old), so_far, inside)
        before = combine(inside, before)
    return before


def shifted(value, axis, steps):
    count = lax.axis_size(axis)
    initial, last = (max(0, -steps), min(count, count - steps))
    return lax.ppermute(value, axis, [(source, source + steps) for source in range(initial, last)])


def gather_turned(arrays, axis, dims):
    turned = [jnp.moveaxis(a, dim, 0) for a, dim in zip(arrays, dims)]
    widths = [t[0].size for t in turned]
    both = jnp.concatenate([t.reshape(-1, w) for t, w in zip(turned, widths)], axis=1)
    whole = lax.all_gather(both, axis, axis=0, tiled=True)
    tiles = jnp.split(whole, [sum(widths[:k]) for k in range(1, len(widths))], axis=1)
    return tuple(
        (
            jnp.moveaxis(b.reshape(-1, *t.shape[1:]), 0, dim)
            for b, t, dim in zip(tiles, turned, dims)
        )
    )


def laid_out(tiles, dim):
    tiles = jnp.moveaxis(tiles, 0, dim)
    shape = tiles.shape
    return tiles.reshape(*shape[:dim], shape[dim] * shape[dim + 1], *shape[dim + 2 :])


def from_everyone(value, axis):
    size = lax.axis_size(axis)
    return lax.all_to_all(
        jnp.broadcast_to(value[None], (size, *value.shape)), axis, 0, 0, tiled=True
    )


def collect(value, axis, dim):
    return laid_out(from_everyone(value, axis), dim)


def cut_along(value, dim, size):
    before, after = (value.shape[:dim], value.shape[dim + 1 :])
    return jnp.moveaxis(value.reshape(*before, size, -1, *after), dim, 0)


def sent_and_summed(value, axis, dim):
    tiles = cut_along(value, dim, lax.axis_size(axis))
    arrived = lax.all_to_all(tiles, axis, split_axis=0, concat_axis=0, tiled=True)
    return arrived.astype(jnp.float32).sum(axis=0)


def rotate(values, positions):
    half_dim = values.shape[-1] // 2
    inverse = rope_base ** (-jnp.arange(half_dim, dtype=jnp.float32) / half_dim)
    angles = positions.astype(jnp.float32)[:, None] * inverse[None, :]
    cosine = jnp.cos(angles)[:, None, :]
    sine_part = jnp.sin(angles)[:, None, :]
    first_half = values[..., :half_dim].astype(jnp.float32)
    second_half = values[..., half_dim:].astype(jnp.float32)
    return jnp.concatenate(
        [
            first_half * cosine - second_half * sine_part,
            second_half * cosine + first_half * sine_part,
        ],
        axis=-1,
    )


def chain_join(earlier_part, later_part):
    return (
        earlier_part[0] * later_part[0],
        later_part[0][:, None, None] * earlier_part[1] + later_part[1],
    )


def retention_path(query_ret, key_ret, value_ret, log_decay):
    tok_count, heads_here = (query_ret.shape[0], query_ret.shape[1])
    blocks = tok_count // BLOCK
    q_blocks = query_ret.reshape(blocks, BLOCK, heads_here, RETAIN_KEY_SIZE)
    k_blocks = key_ret.reshape(blocks, BLOCK, heads_here, RETAIN_KEY_SIZE)
    v_blocks = value_ret.reshape(blocks, BLOCK, heads_here, V_DIM)
    running = jnp.cumsum(log_decay.reshape(heads_here, blocks, BLOCK), axis=-1)
    closing = running[:, :, -1:]
    within = running[:, :, :, None] - running[:, :, None, :]
    causal_mask = jnp.arange(BLOCK)[:, None] >= jnp.arange(BLOCK)[None, :]
    weighting = jnp.where(causal_mask, jnp.exp(jnp.minimum(within, 0.0)), 0.0)
    scores = (
        jnp.einsum("nihd,njhd->hnij", q_blocks, k_blocks, preferred_element_type=jnp.float32)
        * weighting
    )
    in_block = jnp.einsum(
        "hnij,njhv->nihv", scores.astype(jnp.bfloat16), v_blocks, preferred_element_type=jnp.float32
    )
    key_fade = (
        k_blocks.astype(jnp.float32) * jnp.exp(closing - running).transpose(1, 2, 0)[..., None]
    ).astype(jnp.bfloat16)
    contrib = jnp.einsum("njhd,njhv->nhdv", key_fade, v_blocks, preferred_element_type=jnp.float32)
    block_fade = jnp.exp(closing[:, :, 0]).T

    def advance(carried, entry_pair):
        addend, factor = entry_pair
        return (carried * factor[:, None, None] + addend, carried)

    final_state, before = lax.scan(
        advance, jnp.zeros((heads_here, RETAIN_KEY_SIZE, V_DIM), jnp.float32), (contrib, block_fade)
    )
    device_fade = jnp.exp(jnp.sum(closing[:, :, 0], axis=1))
    identity = (jnp.ones_like(device_fade), jnp.zeros_like(final_state))
    arrived = entering((device_fade, final_state), SP, chain_join, identity)
    leading = jnp.cumsum(closing[:, :, 0], axis=1) - closing[:, :, 0]
    before = before + arrived[1][None] * jnp.exp(leading).T[:, :, None, None]
    query_fade = (
        q_blocks.astype(jnp.float32) * jnp.exp(running).transpose(1, 2, 0)[..., None]
    ).astype(jnp.bfloat16)
    carried_term = jnp.einsum("nihd,nhdv->nihv", query_fade.astype(jnp.float32), before)
    final_product = in_block + carried_term
    final_product = final_product * lax.rsqrt(
        jnp.mean(final_product * final_product, axis=-1, keepdims=True) + epsilon
    )
    return final_product.reshape(tok_count, heads_here * V_DIM).astype(jnp.bfloat16)


def attention_path(query_att, key_att, value_att, sink_logits, anchor):
    tok_count = query_att.shape[0]
    kv_here = key_att.shape[1] // HEAD_DIM
    group_size = query_att.shape[1] // (kv_here * HEAD_DIM)
    stacked = jnp.concatenate([key_att, value_att], axis=1)
    window_rim = shifted(stacked[tok_count - WINDOW :], SP, 1)
    blocks = tok_count // WINDOW
    extended = jnp.concatenate([window_rim, stacked], axis=0).reshape(
        blocks + 1, WINDOW, 2, kv_here, HEAD_DIM
    )
    paired = jnp.concatenate([extended[:-1], extended[1:]], axis=1)
    keys_pair = paired[:, :, 0]
    values_pair = paired[:, :, 1]
    q_blocks = query_att.reshape(blocks, WINDOW, kv_here, group_size, HEAD_DIM)
    scores = jnp.einsum(
        "nihgd,njhd->nhgij", q_blocks, keys_pair, preferred_element_type=jnp.float32
    ) * HEAD_DIM ** (-0.5)
    query_pos = anchor + (jnp.arange(blocks) * WINDOW)[:, None] + jnp.arange(WINDOW)[None, :]
    key_pos = (
        anchor + (jnp.arange(blocks) * WINDOW - WINDOW)[:, None] + jnp.arange(2 * WINDOW)[None, :]
    )
    allowed = (
        (key_pos[:, None, :] >= 0)
        & (key_pos[:, None, :] <= query_pos[:, :, None])
        & (query_pos[:, :, None] - key_pos[:, None, :] < WINDOW)
    )
    scores = jnp.where(allowed[:, None, None], scores, masked_out)
    sink_logit = sink_logits.reshape(kv_here, group_size)[None, :, :, None]
    highest = jnp.maximum(jnp.max(scores, axis=-1), sink_logit)
    lifted = jnp.exp(scores - highest[..., None])
    denominator = jnp.sum(lifted, axis=-1) + jnp.exp(sink_logit - highest)
    attn_weights = (lifted / denominator[..., None]).astype(jnp.bfloat16)
    final_product = jnp.einsum(
        "nhgij,njhd->nihgd", attn_weights, values_pair, preferred_element_type=jnp.float32
    )
    return final_product.reshape(tok_count, kv_here * group_size * HEAD_DIM).astype(jnp.bfloat16)


def on_device(
    tokens,
    norm_gain,
    ret_query,
    ret_key,
    ret_value,
    log_decay,
    att_query,
    att_key,
    att_value,
    sink_logits,
    ret_out,
    att_out,
):
    tok_float = tokens.astype(jnp.float32)
    normed = (
        tok_float
        * lax.rsqrt(jnp.mean(tok_float * tok_float, axis=-1, keepdims=True) + epsilon)
        * norm_gain
    ).astype(jnp.bfloat16)
    weights = (ret_query, ret_key, ret_value, att_query, att_key, att_value)
    widths = [weight.shape[1] for weight in weights]
    points = [sum(widths[:index]) for index in range(1, len(widths))]
    every_weight = gather_turned(
        (ret_query, ret_key, ret_value, att_query, att_key, att_value, ret_out, att_out),
        SP,
        (0, 0, 0, 0, 0, 0, 1, 1),
    )
    gathered = every_weight[:6]
    out_whole = every_weight[6:]
    joined = jnp.concatenate(gathered, axis=1)
    projected = jnp.dot(
        collect(normed, "tp", 0), joined, preferred_element_type=jnp.float32
    ).astype(jnp.bfloat16)
    sections = jnp.split(projected, points, axis=1)
    tok_count = sections[0].shape[0]
    anchor = lax.axis_index(SP) * tok_count
    positions = anchor + jnp.arange(tok_count, dtype=jnp.int32)
    query_ret = rotate(sections[0].reshape(tok_count, -1, RETAIN_KEY_SIZE), positions).astype(
        jnp.bfloat16
    )
    key_ret = (
        rotate(sections[1].reshape(tok_count, -1, RETAIN_KEY_SIZE), positions)
        * RETAIN_KEY_SIZE ** (-0.5)
    ).astype(jnp.bfloat16)
    value_ret = sections[2].reshape(tok_count, -1, V_DIM)
    ret_mix = retention_path(query_ret, key_ret, value_ret, log_decay)
    att_mix = attention_path(sections[3], sections[4], sections[5], sink_logits, anchor)
    mixed = sent_and_summed(
        (
            jnp.dot(ret_mix, out_whole[0], preferred_element_type=jnp.float32)
            + jnp.dot(att_mix, out_whole[1], preferred_element_type=jnp.float32)
        ).astype(jnp.bfloat16),
        "tp",
        0,
    )
    return mixed.astype(jnp.bfloat16)


def solution(mesh):
    split = Mesh(mesh.devices.reshape(8, 8, 2, mesh.shape["tp"]), ("sp_0", "sp_1", "sp_2", "tp"))
    placed = (
        P(SP_TP, None),
        P(),
        P(SP, "tp"),
        P(SP, "tp"),
        P(SP, "tp"),
        P("tp", SP),
        P(SP, "tp"),
        P(SP, "tp"),
        P(SP, "tp"),
        P("tp"),
        P("tp", SP),
        P("tp", SP),
    )
    return jax.shard_map(
        on_device, mesh=split, in_specs=placed, out_specs=P(SP_TP, None), check_vma=False
    )
```

profile of v0, /device:TPU:1, one launch (start us, length us, event | category | flops | bytes accessed | tf_op | source)
XLA Modules:
  0.0 230.1 jit_solution(2828885828884508952)
XLA Ops:
  6.5 1.5 concatenate.31
  8.1 1.1 fusion.15
  9.2 1.1 fusion.17
  10.3 1.1 broadcast_in_dim.19
  11.4 4.8 %all-to-all-start = ((bf16[4,64,2048]{2,1,0:T(8,128)(2,1)}), bf16[4,64,2048]{2,1,0:T(8,128)(2,1)S(1)}, u32[]{:S(2)}, u32[]{:S(2)}) async-start(bf16[4,64,2048]{2,1,0:T(8,128)(2,1)} %broadcast_in_dim.19), calls=%async_computation | async-start | bytes 2097152 | tf_op jit(solution)/shard_map/all_to_all | solution.py:70
  17.2 1.3 dynamic-slice
  19.4 7.7 %all-reduce = f32[4]{0:T(128)S(1)} all-reduce(f32[4]{0:T(128)S(1)} %exponential_dynamic-update-slice_fusion), channel_id=2, replica_groups=mesh['sp_0'=8,'sp_1'=8,'sp_2'=2,'tp'=4] {'sp_2'}, use_global_device_ids=true, to_apply=%add | all-reduce | flops 4 | bytes 32
  27.2 1.3 dynamic-slice.1
  29.7 76.7 %all-gather.8.cloned.1.call-done = bf16[2048,2688]{1,0:T(8,128)(2,1)} async-done(((bf16[16,2688]{1,0:T(8,128)(2,1)}), bf16[2048,2688]{1,0:T(8,128)(2,1)}) %all-gather.8.cloned.1.call-update) | async-done | bytes 11010064 | tf_op jit(solution)/shard_map/all_gather | solution.py:52
  106.4 5.0 %fusion.4 = bf16[256,1664]{1,0:T(8,128)(2,1)S(1)} fusion(bf16[256,2048]{1,0:T(8,128)(2,1)S(1)} %bitcast.128, bf16[2048,2688]{1,0:T(8,128)(2,1)} %all-gather.8.cloned.1.call-done), kind=kOutput, calls=%fused_computation.8 | convolution fusion | flops 1745256448 | bytes 8716288 | tf_op jit(solution)/shard_map/dot_general | solution.py:230
  112.8 1.7 while.13
  114.5 2.2 all-gather.1
  117.6 12.1 %all-reduce.1 = f32[16]{0:T(128)S(1)} all-reduce(f32[16]{0:T(128)S(1)} %get-tuple-element.116), channel_id=4, replica_groups=mesh['sp_0'=8,'sp_1'=8,'sp_2'=2,'tp'=4] {'sp_1'}, use_global_device_ids=true, to_apply=%add.1 | all-reduce | flops 16 | bytes 128
  129.8 23.1 %all-gather.10.cloned.1.call-done = f32[8,2,128,256]{3,2,1,0:T(8,128)} async-done(((f32[1,2,128,256]{3,2,1,0:T(8,128)}), f32[8,2,128,256]{3,2,1,0:T(8,128)}) %all-gather.10.cloned.1.call-update) | async-done | bytes 2097168 | tf_op jit(solution)/shard_map/all_gather | solution.py:32
  152.9 2.5 %slice_add_fusion.8 = (f32[1,2,128,256]{3,2,1,0:T(8,128)}, f32[1,2,128,256]{3,2,1,0:T(8,128)}) fusion(f32[8,2,128,256]{3,2,1,0:T(8,128)} %all-gather.10.cloned.1.call-done, f32[2]{0:T(128)S(1)} %get-tuple-element.115, f32[2]{0:T(128)S(1)} %get-tuple-element.114, f32[2]{0:T(128)S(1)} %get-tuple-element.111, f32[2]{0:T(128)S(1)} %get-tuple-element.110, ...), kind=kLoop, calls=%fused_computation.48 | loop fusion | flops 983040 | bytes 2621504 | tf_op jit(solution)/shard_map/add | solution.py:110
  155.5 13.5 %all-gather.3 = f32[8,1,2]{2,1,0:T(1,128)S(1)} all-gather(f32[1,1,2]{2,1,0:T(1,128)S(1)} %fusion.62), channel_id=1, replica_groups=mesh['sp_0'=8,'sp_1'=8,'sp_2'=2,'tp'=4] {'sp_0'}, dimensions={0}, use_global_device_ids=true | all-gather | bytes 72 | tf_op jit(solution)/shard_map/all_gather | solution.py:32
  170.8 11.4 %collective-permute-start = (bf16[128,128]{1,0:T(8,128)(2,1)S(1)}, bf16[128,128]{1,0:T(8,128)(2,1)S(1)}, u32[]{:S(2)}, u32[]{:S(2)}) collective-permute-start(bf16[128,128]{1,0:T(8,128)(2,1)S(1)} %slice.243), channel_id=1, source_target_pairs={{0,4},{4,8},{8,12},{12,16},{16,20},{20,24},{24,28},{28,32},{32,36}... | collective-permute-start | bytes 98312 | tf_op jit(solution)/shard_map/ppermute | solution.py:45
  186.5 1.4 fusion.12
  188.9 10.2 %all-gather.12.cloned.1.call-done = f32[8,2,128,256]{3,2,1,0:T(8,128)} async-done(((f32[1,2,128,256]{3,2,1,0:T(8,128)}), f32[8,2,128,256]{3,2,1,0:T(8,128)}) %all-gather.12.cloned.1.call-update) | async-done | bytes 2097168 | tf_op jit(solution)/shard_map/all_gather | solution.py:32
  199.1 2.3 fusion.27
  201.9 1.2 multiply_reduce_fusion
  203.4 2.4 %fusion.8 = f32[256,2048]{1,0:T(8,128)S(1)} fusion(bf16[256,512]{1,0:T(8,128)(2,1)S(1)} %bitcast.127, bf16[2048,2688]{1,0:T(8,128)(2,1)} %all-gather.8.cloned.1.call-done), kind=kOutput, calls=%fused_computation.10 | convolution fusion | flops 536870912 | bytes 4456448 | tf_op jit(solution)/shard_map/dot_general | solution.py:249
  205.8 2.4 %fusion.3 = bf16[256,2048]{1,0:T(8,128)(2,1)S(1)} fusion(f32[256,2048]{1,0:T(8,128)S(1)} %fusion.8, bf16[2048,2688]{1,0:T(8,128)(2,1)} %all-gather.8.cloned.1.call-done, bf16[64,8,2,128]{3,2,1,0:T(2,128)(2,1)S(1)} %bitcast.130), kind=kOutput, calls=%fused_computation.7 | convolution fusion | flops 537919488 | bytes 5505024 | tf_op jit(solution)/shard_map/dot_general | solution.py:250
  208.2 14.5 %all_to_all.10 = bf16[4,64,2048]{2,1,0:T(8,128)(2,1)S(1)} all-to-all(bf16[4,64,2048]{2,1,0:T(8,128)(2,1)S(1)} %bitcast.126), channel_id=1, replica_groups=mesh['sp_0'=8,'sp_1'=8,'sp_2'=2,'tp'=4] {'tp'}, dimensions={0} | all-to-all | bytes 2097152 | tf_op jit(solution)/shard_map/all_to_all | solution.py:86
  (119 shorter events, 14.3 us)
Async XLA Ops:
  6.5 99.9 %all-gather.8.cloned.1.call-start = ((), (), s32[]{:S(2)}) async-start(), calls=%async_computation.2 | async-start | bytes 11096064 | tf_op jit(solution)/shard_map/all_gather | solution.py:52
  8.1 8.2 %copy-start.18 = (f32[2,256]{1,0:T(2,128)S(1)}, f32[2,256]{1,0:T(2,128)}, u32[]{:S(2)}) copy-start(f32[2,256]{1,0:T(2,128)} %param.19) | copy-start | bytes 6148
  11.4 18.3 %all-to-all-start = ((bf16[4,64,2048]{2,1,0:T(8,128)(2,1)}), bf16[4,64,2048]{2,1,0:T(8,128)(2,1)S(1)}, u32[]{:S(2)}, u32[]{:S(2)}) async-start(bf16[4,64,2048]{2,1,0:T(8,128)(2,1)} %broadcast_in_dim.19), calls=%async_computation | async-start | bytes 2097152 | tf_op jit(solution)/shard_map/all_to_all | solution.py:70
  16.3 136.6 %all-gather.10.cloned.1.call-start = ((), (), s32[]{:S(2)}) async-start(), calls=%async_computation.3 | async-start | bytes 2359296 | tf_op jit(solution)/shard_map/all_gather | solution.py:32
  29.4 87.3 %copy-start.14 = (f32[2]{0:T(128)}, f32[2]{0:T(128)S(1)}, u32[]{:S(2)}) copy-start(f32[2]{0:T(128)S(1)} %get-tuple-element.117) | copy-start | bytes 28
  29.4 87.3 %copy-start.15 = (f32[2]{0:T(128)}, f32[2]{0:T(128)S(1)}, u32[]{:S(2)}) copy-start(f32[2]{0:T(128)S(1)} %get-tuple-element.118) | copy-start | bytes 28
  117.5 81.6 %all-gather.12.cloned.1.call-start = ((), (), s32[]{:S(2)}) async-start(), calls=%async_computation.4 | async-start | bytes 2359296 | tf_op jit(solution)/shard_map/all_gather | solution.py:32
  129.8 40.7 %copy-start.8 = (f32[2]{0:T(128)}, f32[2]{0:T(128)S(1)}, u32[]{:S(2)}) copy-start(f32[2]{0:T(128)S(1)} %get-tuple-element.109) | copy-start | bytes 28
  129.8 40.7 %copy-start.9 = (f32[2]{0:T(128)}, f32[2]{0:T(128)S(1)}, u32[]{:S(2)}) copy-start(f32[2]{0:T(128)S(1)} %get-tuple-element.110) | copy-start | bytes 28
  129.8 40.7 %copy-start.10 = (f32[2]{0:T(128)}, f32[2]{0:T(128)S(1)}, u32[]{:S(2)}) copy-start(f32[2]{0:T(128)S(1)} %get-tuple-element.111) | copy-start | bytes 28
  129.8 40.7 %copy-start.11 = (f32[2]{0:T(128)}, f32[2]{0:T(128)S(1)}, u32[]{:S(2)}) copy-start(f32[2]{0:T(128)S(1)} %get-tuple-element.112) | copy-start | bytes 28
  129.8 40.7 %copy-start.12 = (f32[2]{0:T(128)}, f32[2]{0:T(128)S(1)}, u32[]{:S(2)}) copy-start(f32[2]{0:T(128)S(1)} %get-tuple-element.113) | copy-start | bytes 28
  129.8 40.7 %copy-start.13 = (f32[2]{0:T(128)}, f32[2]{0:T(128)S(1)}, u32[]{:S(2)}) copy-start(f32[2]{0:T(128)S(1)} %get-tuple-element.115) | copy-start | bytes 28
  170.8 14.1 %collective-permute-start = (bf16[128,128]{1,0:T(8,128)(2,1)S(1)}, bf16[128,128]{1,0:T(8,128)(2,1)S(1)}, u32[]{:S(2)}, u32[]{:S(2)}) collective-permute-start(bf16[128,128]{1,0:T(8,128)(2,1)S(1)} %slice.243), channel_id=1, source_target_pairs={{0,4},{4,8},{8,12},{12,16},{16,20},{20,24},{24,28},{28,32},{32,36}... | collective-permute-start | bytes 98312 | tf_op jit(solution)/shard_map/ppermute | solution.py:45
  184.2 1.4 copy-start.4
  184.5 1.1 copy-start.17
  185.1 0.9 copy-start.6
  185.6 0.8 copy-start.5
  186.5 12.6 %copy-start = (f32[8,2,128,256]{3,2,1,0:T(8,128)S(1)}, f32[8,2,128,256]{3,2,1,0:T(8,128)}, u32[]{:S(2)}) copy-start(f32[8,2,128,256]{3,2,1,0:T(8,128)} %all-gather.10.cloned.1.call-done) | copy-start | bytes 6291460
  186.5 12.6 %copy-start.1 = (f32[1,2,128,256]{3,2,1,0:T(8,128)S(1)}, f32[1,2,128,256]{3,2,1,0:T(8,128)}, u32[]{:S(2)}) copy-start(f32[1,2,128,256]{3,2,1,0:T(8,128)} %get-tuple-element.82) | copy-start | bytes 786436
  199.1 2.3 copy-start.3
  199.1 2.3 %copy-start.7 = (f32[2,128,2]{1,2,0:T(2,128)S(1)}, f32[2,128,2]{1,2,0:T(2,128)}, u32[]{:S(2)}) copy-start(f32[2,128,2]{1,2,0:T(2,128)} %copy.64) | copy-start | bytes 6148
  199.1 2.3 %copy-start.16 = (f32[2,2]{1,0:T(2,128)S(1)}, f32[2,2]{1,0:T(2,128)}, u32[]{:S(2)}) copy-start(f32[2,2]{1,0:T(2,128)} %copy.63) | copy-start | bytes 52
  203.4 2.4 %copy-start.2 = (bf16[2,128,1,8,64]{1,0,4,3,2:T(2,128)(2,1)S(1)}, bf16[2,128,1,8,64]{1,0,4,3,2:T(2,128)(2,1)}, u32[]{:S(2)}) copy-start(bf16[2,128,1,8,64]{1,0,4,3,2:T(2,128)(2,1)} %copy.74) | copy-start | bytes 786436
Sparse Core Ops, SparseCore 0:
  10.5 95.8 all-gather.7
  117.7 35.1 all-gather.9
  155.5 43.5 all-gather.11
where the time goes:
time: 234 us; the launch traced here: 230 us
  waiting for transfers between devices  110 us (47%)
  blocking collectives  50 us (21%)
  starting transfers between devices  16.3 us (7%)
  between operations  14.9 us (6%)
  other arithmetic  14.5 us (6%)
  matrix products  13.6 us (6%)
  local copies, waits for them, and re-layouts  10.6 us (5%)
    all_gather x1, waiting for transfers between devices, gather_turned(): whole = lax.all_gather(both, axis, axis=0, tiled=True)  76.7 us
    all_gather x2, waiting for transfers between devices, entering(): pieces = jax.tree.map(lambda part: lax.all_gather(part, axis), so_far)  33.3 us
    unnamed x2, blocking collectives  19.8 us
    all_gather x2, blocking collectives, entering(): pieces = jax.tree.map(lambda part: lax.all_gather(part, axis), so_far)  15.7 us
    all_to_all x1, blocking collectives, sent_and_summed(): lax.all_to_all(tiles, axis, split_axis=0, concat_axis=0, tiled=True)  14.5 us
    ppermute x1, starting transfers between devices, shifted(): lax.ppermute(value, axis, [(source, source + steps) for source in range(i...  11.4 us
    dot_general x1, matrix products, on_device(): jnp.dot(collect(normed, 'tp', 0), joined, preferred_element_type=jnp.floa...  4.99 us
    all_to_all x1, starting transfers between devices, from_everyone(): lax.all_to_all(jnp.broadcast_to(value[None], (size, *value.shape)), axis,...  4.83 us
  transfers between devices with their start and end apart: 5, of which 3 were waited for; matrix products, arithmetic and copies ran while one was open for 7% of the time, Pallas kernels for 0%

commit v1 on v0

--- a/solution.py
+++ b/solution.py
@@ -1,6 +1,7 @@
 import jax
 import jax.numpy as jnp
 from jax import lax
+from jax.experimental import pallas as pl
 from jax.sharding import Mesh
 from jax.sharding import PartitionSpec as P
 
@@ -16,27 +17,6 @@
 epsilon = 1e-05
 rope_base = 10000.0
 masked_out = -1e30
-
-
-def neutral_like(value, identity):
-    return jax.tree.map(
-        lambda a, e: jnp.broadcast_to(jnp.asarray(e, a.dtype), a.shape), value, identity
-    )
-
-
-def entering(value, axes, combine, identity):
-    before = start = neutral_like(value, identity)
-    so_far = value
-    for axis in reversed(axes):
-        size, here = (lax.axis_size(axis), lax.axis_index(axis))
-        pieces = jax.tree.map(lambda part: lax.all_gather(part, axis), so_far)
-        inside, so_far = (start, start)
-        for k in range(size):
-            passed = k < here
-            so_far = combine(so_far, jax.tree.map(lambda part: part[k], pieces))
-            inside = jax.tree.map(lambda new, old: jnp.where(passed, new, old), so_far, inside)
-        before = combine(inside, before)
-    return before
 
 
 def shifted(value, axis, steps):
@@ -57,23 +37,6 @@
             for b, t, dim in zip(tiles, turned, dims)
         )
     )
-
-
-def laid_out(tiles, dim):
-    tiles = jnp.moveaxis(tiles, 0, dim)
-    shape = tiles.shape
-    return tiles.reshape(*shape[:dim], shape[dim] * shape[dim + 1], *shape[dim + 2 :])
-
-
-def from_everyone(value, axis):
-    size = lax.axis_size(axis)
-    return lax.all_to_all(
-        jnp.broadcast_to(value[None], (size, *value.shape)), axis, 0, 0, tiled=True
-    )
-
-
-def collect(value, axis, dim):
-    return laid_out(from_everyone(value, axis), dim)
 
 
 def cut_along(value, dim, size):
@@ -104,53 +67,104 @@
     )
 
 
-def chain_join(earlier_part, later_part):
-    return (
-        earlier_part[0] * later_part[0],
-        later_part[0][:, None, None] * earlier_part[1] + later_part[1],
-    )
-
-
-def retention_path(query_ret, key_ret, value_ret, log_decay):
+ZY = ("sp_0", "sp_1")
+CORE = "sp_2"
+
+
+def core_swap(value):
+    return lax.ppermute(value, CORE, [(0, 1), (1, 0)])
+
+
+def in_core_order(own, other, axis):
+    first = lax.axis_index(CORE) == 0
+    return jnp.concatenate(
+        [jnp.where(first, own, other), jnp.where(first, other, own)], axis=axis
+    )
+
+
+def prefix_body(parts_ref, out_ref):
+    count = parts_ref.shape[0]
+    carried = jnp.zeros(out_ref.shape[1:], jnp.float32)
+    for k in range(count):
+        out_ref[k] = carried
+        carried = carried * jnp.exp(parts_ref[k, 2:3]) + parts_ref[k, :2]
+
+
+def state_before(total, log_total):
+    count = lax.axis_size(ZY)
+    slices = total.reshape(count, 2, V_DIM)
+    marks = jnp.broadcast_to(log_total, (count, 1, V_DIM))
+    sent = jnp.concatenate([slices, marks], axis=1)
+    arrived = lax.all_to_all(sent, ZY, 0, 0, tiled=True)
+    prefix = pl.pallas_call(
+        prefix_body, out_shape=jax.ShapeDtypeStruct((count, 2, V_DIM), jnp.float32)
+    )(arrived)
+    return lax.all_to_all(prefix, ZY, 0, 0, tiled=True).reshape(RETAIN_KEY_SIZE, V_DIM)
+
+
+def weight_of_head(ret_key, ret_value):
+    devices = lax.axis_size(SP)
+    rows = ret_key.shape[0]
+    heads = lax.axis_size(CORE)
+    keys = ret_key.reshape(rows, heads, RETAIN_KEY_SIZE)
+    values = ret_value.reshape(rows, heads, V_DIM)
+    both = jnp.moveaxis(jnp.concatenate([keys, values], axis=2), 1, 0)
+    sent = jnp.broadcast_to(both[None], (devices // heads, *both.shape)).reshape(
+        devices, rows, -1
+    )
+    arrived = lax.all_to_all(sent, SP, 0, 0, tiled=True)
+    return arrived.reshape(devices * rows, -1)
+
+
+def chain_of_head(kv, log_decay, anchor):
+    length = kv.shape[0]
+    blocks = length // BLOCK
+    positions = anchor + jnp.arange(length, dtype=jnp.int32)
+    keys = (
+        rotate(kv[:, None, :RETAIN_KEY_SIZE], positions)[:, 0] * RETAIN_KEY_SIZE ** (-0.5)
+    ).astype(jnp.bfloat16)
+    values = kv[:, RETAIN_KEY_SIZE:]
+    running = jnp.cumsum(log_decay.reshape(blocks, BLOCK), axis=-1)
+    closing = running[:, -1]
+    faded = (
+        keys.reshape(blocks, BLOCK, -1).astype(jnp.float32)
+        * jnp.exp(closing[:, None] - running)[..., None]
+    ).astype(jnp.bfloat16)
+    contrib = jnp.einsum(
+        "njd,njv->ndv", faded, values.reshape(blocks, BLOCK, -1), preferred_element_type=jnp.float32
+    )
+    total = contrib[0]
+    for n in range(1, blocks):
+        total = total * jnp.exp(closing[n]) + contrib[n]
+    state = state_before(total, jnp.sum(closing))
+    before = []
+    for n in range(blocks):
+        before.append(state)
+        state = state * jnp.exp(closing[n]) + contrib[n]
+    return keys, values, jnp.stack(before)
+
+
+def retention_path(query_ret, key_ret, value_ret, log_decay, before):
     tok_count, heads_here = (query_ret.shape[0], query_ret.shape[1])
     blocks = tok_count // BLOCK
     q_blocks = query_ret.reshape(blocks, BLOCK, heads_here, RETAIN_KEY_SIZE)
-    k_blocks = key_ret.reshape(blocks, BLOCK, heads_here, RETAIN_KEY_SIZE)
-    v_blocks = value_ret.reshape(blocks, BLOCK, heads_here, V_DIM)
+    k_blocks = key_ret.reshape(heads_here, blocks, BLOCK, RETAIN_KEY_SIZE)
+    v_blocks = value_ret.reshape(heads_here, blocks, BLOCK, V_DIM)
     running = jnp.cumsum(log_decay.reshape(heads_here, blocks, BLOCK), axis=-1)
-    closing = running[:, :, -1:]
     within = running[:, :, :, None] - running[:, :, None, :]
     causal_mask = jnp.arange(BLOCK)[:, None] >= jnp.arange(BLOCK)[None, :]
     weighting = jnp.where(causal_mask, jnp.exp(jnp.minimum(within, 0.0)), 0.0)
     scores = (
-        jnp.einsum("nihd,njhd->hnij", q_blocks, k_blocks, preferred_element_type=jnp.float32)
+        jnp.einsum("nihd,hnjd->hnij", q_blocks, k_blocks, preferred_element_type=jnp.float32)
         * weighting
     )
     in_block = jnp.einsum(
-        "hnij,njhv->nihv", scores.astype(jnp.bfloat16), v_blocks, preferred_element_type=jnp.float32
-    )
-    key_fade = (
-        k_blocks.astype(jnp.float32) * jnp.exp(closing - running).transpose(1, 2, 0)[..., None]
-    ).astype(jnp.bfloat16)
-    contrib = jnp.einsum("njhd,njhv->nhdv", key_fade, v_blocks, preferred_element_type=jnp.float32)
-    block_fade = jnp.exp(closing[:, :, 0]).T
-
-    def advance(carried, entry_pair):
-        addend, factor = entry_pair
-        return (carried * factor[:, None, None] + addend, carried)
-
-    final_state, before = lax.scan(
-        advance, jnp.zeros((heads_here, RETAIN_KEY_SIZE, V_DIM), jnp.float32), (contrib, block_fade)
-    )
-    device_fade = jnp.exp(jnp.sum(closing[:, :, 0], axis=1))
-    identity = (jnp.ones_like(device_fade), jnp.zeros_like(final_state))
-    arrived = entering((device_fade, final_state), SP, chain_join, identity)
-    leading = jnp.cumsum(closing[:, :, 0], axis=1) - closing[:, :, 0]
-    before = before + arrived[1][None] * jnp.exp(leading).T[:, :, None, None]
+        "hnij,hnjv->nihv", scores.astype(jnp.bfloat16), v_blocks, preferred_element_type=jnp.float32
+    )
     query_fade = (
         q_blocks.astype(jnp.float32) * jnp.exp(running).transpose(1, 2, 0)[..., None]
     ).astype(jnp.bfloat16)
-    carried_term = jnp.einsum("nihd,nhdv->nihv", query_fade.astype(jnp.float32), before)
+    carried_term = jnp.einsum("nihd,hndv->nihv", query_fade.astype(jnp.float32), before)
     final_product = in_block + carried_term
     final_product = final_product * lax.rsqrt(
         jnp.mean(final_product * final_product, axis=-1, keepdims=True) + epsilon
@@ -210,40 +224,62 @@
     ret_out,
     att_out,
 ):
+    core = lax.axis_index(CORE)
     tok_float = tokens.astype(jnp.float32)
     normed = (
         tok_float
         * lax.rsqrt(jnp.mean(tok_float * tok_float, axis=-1, keepdims=True) + epsilon)
         * norm_gain
     ).astype(jnp.bfloat16)
-    weights = (ret_query, ret_key, ret_value, att_query, att_key, att_value)
+    weights = (ret_query, att_query, att_key, att_value)
     widths = [weight.shape[1] for weight in weights]
     points = [sum(widths[:index]) for index in range(1, len(widths))]
     every_weight = gather_turned(
-        (ret_query, ret_key, ret_value, att_query, att_key, att_value, ret_out, att_out),
-        SP,
-        (0, 0, 0, 0, 0, 0, 1, 1),
-    )
-    gathered = every_weight[:6]
-    out_whole = every_weight[6:]
+        (ret_query, att_query, att_key, att_value, ret_out, att_out), SP, (0, 0, 0, 0, 1, 1)
+    )
+    gathered = every_weight[:4]
+    out_whole = every_weight[4:]
+
+    pair = jnp.stack([normed, core_swap(normed)])
+    size = lax.axis_size("tp")
+    arrived = lax.all_to_all(
+        jnp.broadcast_to(pair[None], (size, *pair.shape)), "tp", 0, 0, tiled=True
+    )
+    chip_rows = arrived.reshape(-1, arrived.shape[-1])
+    head_weight = weight_of_head(ret_key, ret_value)
+    kv = jnp.dot(chip_rows, head_weight, preferred_element_type=jnp.float32).astype(jnp.bfloat16)
+    kv = jnp.moveaxis(kv.reshape(size, 2, -1, kv.shape[-1]), 1, 0)
+    kv = kv.reshape(2, -1, kv.shape[-1])
+    decay_other = core_swap(log_decay)
+    own_head = lax.dynamic_index_in_dim(log_decay, core, 0, keepdims=False)
+    other_half = lax.dynamic_index_in_dim(decay_other, core, 0, keepdims=False)
+    tok_count = kv.shape[1]
+    anchor = lax.axis_index(SP) * tok_count
+    chip_anchor = lax.axis_index(ZY) * (2 * tok_count)
+    keys, values, before = chain_of_head(
+        in_core_order(kv[0], kv[1], 0), in_core_order(own_head, other_half, 0), chip_anchor
+    )
+
+    def heads_of_own_rows(value):
+        halves = value.reshape(2, value.shape[0] // 2, *value.shape[1:])
+        mine = lax.dynamic_index_in_dim(halves, core, 0, keepdims=False)
+        theirs = lax.dynamic_index_in_dim(halves, 1 - core, 0, keepdims=False)
+        return in_core_order(mine[None], core_swap(theirs)[None], 0)
+
+    key_ret = heads_of_own_rows(keys)
+    value_ret = heads_of_own_rows(values)
+    before = heads_of_own_rows(before)
+
     joined = jnp.concatenate(gathered, axis=1)
-    projected = jnp.dot(
-        collect(normed, "tp", 0), joined, preferred_element_type=jnp.float32
-    ).astype(jnp.bfloat16)
+    own_rows = arrived.reshape(size, 2, -1, arrived.shape[-1])[:, 0].reshape(tok_count, -1)
+    projected = jnp.dot(own_rows, joined, preferred_element_type=jnp.float32).astype(jnp.bfloat16)
     sections = jnp.split(projected, points, axis=1)
-    tok_count = sections[0].shape[0]
-    anchor = lax.axis_index(SP) * tok_count
     positions = anchor + jnp.arange(tok_count, dtype=jnp.int32)
     query_ret = rotate(sections[0].reshape(tok_count, -1, RETAIN_KEY_SIZE), positions).astype(
         jnp.bfloat16
     )
-    key_ret = (
-        rotate(sections[1].reshape(tok_count, -1, RETAIN_KEY_SIZE), positions)
-        * RETAIN_KEY_SIZE ** (-0.5)
-    ).astype(jnp.bfloat16)
-    value_ret = sections[2].reshape(tok_count, -1, V_DIM)
-    ret_mix = retention_path(query_ret, key_ret, value_ret, log_decay)
-    att_mix = attention_path(sections[3], sections[4], sections[5], sink_logits, anchor)
+    ret_mix = retention_path(query_ret, key_ret, value_ret, log_decay, before)
+    att_mix = attention_path(sections[1], sections[2], sections[3], sink_logits, anchor)
     mixed = sent_and_summed(
         (
             jnp.dot(ret_mix, out_whole[0], preferred_element_type=jnp.float32)

time: 234 us -> 211 us (0.902); the launches traced: 230 us -> 210 us
  starting transfers between devices: 16.3 us -> 55.5 us
  blocking collectives: 50 us -> 17.8 us
  waiting for transfers between devices: 110 us -> 83.6 us
  other arithmetic: 14.5 us -> 9.55 us
    all_to_all x1 -> x4, waiting for transfers between devices: 0.01 us -> 82.9 us  [the longest x1 39.2 us: weight_of_head(): arrived = lax.all_to_all(sent, SP, 0, 0, tiled=True)]
    all_gather x1, waiting for transfers between devices: 76.7 us -> 0.02 us  [gather_turned(): whole = lax.all_gather(both, axis, axis=0, tiled=True)]
    all_gather x2 -> x0, waiting for transfers between devices: 33.3 us -> none  [entering(): pieces = jax.tree.map(lambda part: lax.all_gather(part, axis), so_far)]
    all_to_all x1 -> x4, starting transfers between devices: 4.83 us -> 32.8 us  [the longest x1 13.6 us: weight_of_head(): arrived = lax.all_to_all(sent, SP, 0, 0, tiled=True)]
    ppermute x0 -> x5, starting transfers between devices: none -> 20.2 us  [core_swap(): return lax.ppermute(value, CORE, [(0, 1), (1, 0)])]
    unnamed x2 -> x0, blocking collectives: 19.8 us -> none
    all_gather x2 -> x0, blocking collectives: 15.7 us -> none  [entering(): pieces = jax.tree.map(lambda part: lax.all_gather(part, axis), so_far)]
    ppermute x1, starting transfers between devices: 11.4 us -> 2.59 us  [shifted(): lax.ppermute(value, axis, [(source, source + steps) for source in range(i...]
  transfers between devices with their start and end apart: 5 -> 11, of which waited for: 3 -> 5; matrix products, arithmetic and copies ran while one was open for 7% -> 11% of each run, Pallas kernels for 0% -> 1%
where the time goes in v1:
time: 211 us; the launch traced here: 210 us
  waiting for transfers between devices  83.6 us (40%)
  starting transfers between devices  55.5 us (26%)
  blocking collectives  17.8 us (8%)
  between operations  16.9 us (8%)
  matrix products  12.9 us (6%)
  local copies, waits for them, and re-layouts  12.1 us (6%)
  other arithmetic  9.55 us (5%)
    all_to_all x1, waiting for transfers between devices, weight_of_head(): arrived = lax.all_to_all(sent, SP, 0, 0, tiled=True)  39.2 us
    all_to_all x1, waiting for transfers between devices, on_device(): lax.all_to_all(jnp.broadcast_to(pair[None], (size, *pair.shape)), 'tp', 0...  25.9 us
    ppermute x5, starting transfers between devices, core_swap(): return lax.ppermute(value, CORE, [(0, 1), (1, 0)])  20.2 us
    all_to_all x1, blocking collectives, sent_and_summed(): lax.all_to_all(tiles, axis, split_axis=0, concat_axis=0, tiled=True)  17.8 us
    all_to_all x1, starting transfers between devices, weight_of_head(): arrived = lax.all_to_all(sent, SP, 0, 0, tiled=True)  13.6 us
    all_to_all x1, waiting for transfers between devices, state_before(): lax.all_to_all(prefix, ZY, 0, 0, tiled=True).reshape(RETAIN_KEY_SIZE, V_DIM)  11.5 us
    all_to_all x1, starting transfers between devices, state_before(): arrived = lax.all_to_all(sent, ZY, 0, 0, tiled=True)  9.56 us
    all_to_all x1, waiting for transfers between devices, state_before(): arrived = lax.all_to_all(sent, ZY, 0, 0, tiled=True)  6.35 us
  transfers between devices with their start and end apart: 11, of which 5 were waited for; matrix products, arithmetic and copies ran while one was open for 11% of the time, Pallas kernels for 1%

profile of v1, /device:TPU:1, one launch (start us, length us, event | category | flops | bytes accessed | tf_op | source)
XLA Modules:
  0.0 210.0 jit_solution(87903960481149908)
XLA Ops:
  6.5 1.5 concatenate.51
  10.3 8.7 %collective-permute-start = (bf16[64,2048]{1,0:T(8,128)(2,1)S(1)}, bf16[64,2048]{1,0:T(8,128)(2,1)S(1)}, u32[]{:S(2)}, u32[]{:S(2)}) collective-permute-start(bf16[64,2048]{1,0:T(8,128)(2,1)S(1)} %fusion.17), channel_id=1, source_target_pairs={{0,4},{4,0},{1,5},{5,1},{2,6},{6,2},{3,7},{7,3},{8,12},{12,8},{9,1... | collective-permute-start | bytes 786440 | tf_op jit(solution)/shard_map/ppermute | solution.py:75
  20.2 1.6 broadcast_in_dim.24
  21.9 3.7 %all-to-all-start = ((bf16[4,2,64,2048]{3,2,1,0:T(8,128)(2,1)}), bf16[4,2,64,2048]{3,2,1,0:T(8,128)(2,1)S(1)}, u32[]{:S(2)}, u32[]{:S(2)}) async-start(bf16[4,2,64,2048]{3,2,1,0:T(8,128)(2,1)} %broadcast_in_dim.24), calls=%async_computation | async-start | bytes 4194304 | tf_op jit(solution)/shard_map/all_to_all | solution.py:245
  25.7 25.9 %all-to-all-done = bf16[4,2,64,2048]{3,2,1,0:T(8,128)(2,1)S(1)} async-done(((bf16[4,2,64,2048]{3,2,1,0:T(8,128)(2,1)}), bf16[4,2,64,2048]{3,2,1,0:T(8,128)(2,1)S(1)}, u32[]{:S(2)}, u32[]{:S(2)}) %all-to-all-start) | async-done | bytes 2097184 | tf_op jit(solution)/shard_map/all_to_all | solution.py:245
  51.6 1.3 broadcast_in_dim.25
  52.9 13.6 %all-to-all-start.1 = ((bf16[128,16,384]{2,1,0:T(8,128)(2,1)}), bf16[128,16,384]{2,1,0:T(8,128)(2,1)}, u32[]{:S(2)}, u32[]{:S(2)}) async-start(bf16[128,16,384]{2,1,0:T(8,128)(2,1)} %bitcast.4), calls=%async_computation.1 | async-start | bytes 3145728 | tf_op jit(solution)/shard_map/all_to_all | solution.py:115
  66.6 2.9 %collective-permute-start.3 = (f32[2,256]{1,0:T(2,128)S(1)}, f32[2,256]{1,0:T(2,128)S(1)}, u32[]{:S(2)}, u32[]{:S(2)}) collective-permute-start(f32[2,256]{1,0:T(2,128)S(1)} %copy-done.7), channel_id=1, source_target_pairs={{0,4},{4,0},{1,5},{5,1},{2,6},{6,2},{3,7},{7,3},{8,12},{12,8},{9,1... | collective-permute-start | bytes 6152 | tf_op jit(solution)/shard_map/ppermute | solution.py:75
  76.0 39.2 %all-to-all-done.1 = bf16[128,16,384]{2,1,0:T(8,128)(2,1)} async-done(((bf16[128,16,384]{2,1,0:T(8,128)(2,1)}), bf16[128,16,384]{2,1,0:T(8,128)(2,1)}, u32[]{:S(2)}, u32[]{:S(2)}) %all-to-all-start.1) | async-done | bytes 1572896 | tf_op jit(solution)/shard_map/all_to_all | solution.py:115
  115.2 2.7 %convolution_convert_fusion = bf16[512,384]{1,0:T(8,128)(2,1)S(1)} fusion(bf16[512,2048]{1,0:T(8,128)(2,1)S(1)} %bitcast.98, bf16[2048,384]{1,0:T(8,128)(2,1)} %bitcast.5), kind=kOutput, calls=%fused_computation.12 | convolution fusion | flops 805502976 | bytes 4063232 | tf_op jit(solution)/shard_map/dot_general | solution.py:250
  119.7 1.4 concatenate.58
  121.1 9.6 %all-to-all-start.2 = ((f32[64,3,256]{2,1,0:T(4,128)}), f32[64,3,256]{2,1,0:T(4,128)S(1)}, u32[]{:S(2)}, u32[]{:S(2)}) async-start(f32[64,3,256]{2,1,0:T(4,128)} %concatenate.58), calls=%async_computation.2 | async-start | bytes 524288 | tf_op jit(solution)/shard_map/all_to_all | solution.py:98
  132.7 2.2 %collective-permute-start.2 = (bf16[256,128]{1,0:T(8,128)(2,1)S(1)}, bf16[256,128]{1,0:T(8,128)(2,1)S(1)}, u32[]{:S(2)}, u32[]{:S(2)}) collective-permute-start(bf16[256,128]{1,0:T(8,128)(2,1)S(1)} %dynamic-slice_bitcast_fusion), channel_id=1, source_target_pairs={{0,4},{4,0},{1,5},{5,1},{2,6},{6,2},{3,7},{7,3},{8,12},{12,8},{9,1... | collective-permute-start | bytes 196616 | tf_op jit(solution)/shard_map/ppermute | solution.py:75
  135.7 2.2 %collective-permute-start.1 = (bf16[256,256]{1,0:T(8,128)(2,1)S(1)}, bf16[256,256]{1,0:T(8,128)(2,1)S(1)}, u32[]{:S(2)}, u32[]{:S(2)}) collective-permute-start(bf16[256,256]{1,0:T(8,128)(2,1)S(1)} %bitcast.117), channel_id=1, source_target_pairs={{0,4},{4,0},{1,5},{5,1},{2,6},{6,2},{3,7},{7,3},{8,12},{12,8},{9,1... | collective-permute-start | bytes 393224 | tf_op jit(solution)/shard_map/ppermute | solution.py:75
  137.9 6.4 %all-to-all-done.2.parts_ref = f32[64,3,256]{2,1,0:T(4,128)S(1)} async-done(((f32[64,3,256]{2,1,0:T(4,128)}), f32[64,3,256]{2,1,0:T(4,128)S(1)}, u32[]{:S(2)}, u32[]{:S(2)}) %all-to-all-start.2) | async-done | bytes 196640 | tf_op jit(solution)/shard_map/all_to_all | solution.py:98
  145.0 1.7 shard_map.118
  146.7 5.8 %all-to-all-start.3 = ((f32[64,2,256]{2,1,0:T(2,128)}), f32[64,2,256]{2,1,0:T(2,128)S(1)}, u32[]{:S(2)}, u32[]{:S(2)}) async-start(f32[64,2,256]{2,1,0:T(2,128)} %shard_map.118), calls=%async_computation.3 | async-start | bytes 262144 | tf_op jit(solution)/shard_map/all_to_all | solution.py:102
  152.6 11.5 %all-to-all-done.3 = f32[64,2,256]{2,1,0:T(2,128)S(1)} async-done(((f32[64,2,256]{2,1,0:T(2,128)}), f32[64,2,256]{2,1,0:T(2,128)S(1)}, u32[]{:S(2)}, u32[]{:S(2)}) %all-to-all-start.3) | async-done | bytes 131104 | tf_op jit(solution)/shard_map/all_to_all | solution.py:102
  164.4 4.2 %collective-permute-start.4 = (bf16[2,128,256]{1,2,0:T(8,128)(2,1)S(1)}, bf16[2,128,256]{1,2,0:T(8,128)(2,1)S(1)}, u32[]{:S(2)}, u32[]{:S(2)}) collective-permute-start(bf16[2,128,256]{1,2,0:T(8,128)(2,1)S(1)} %bitcast.118), channel_id=1, source_target_pairs={{0,4},{4,0},{1,5},{5,1},{2,6},{6,2},{3,7},{7,3},{8,12},{12,8},{9,1... | collective-permute-start | bytes 393224 | tf_op jit(solution)/shard_map/ppermute | solution.py:75
  169.5 3.3 %fusion.7 = bf16[256,896]{1,0:T(8,128)(2,1)S(1)} fusion(bf16[256,2048]{1,0:T(8,128)(2,1)S(1)} %bitcast.102, bf16[2048,1920]{1,0:T(8,128)(2,1)} %all-gather.2.cloned.1.call-done), kind=kOutput, calls=%fused_computation.11 | convolution fusion | flops 939753472 | bytes 5177344 | tf_op jit(solution)/shard_map/dot_general | solution.py:275
  174.5 2.6 %collective-permute-start.5 = (bf16[128,128]{1,0:T(8,128)(2,1)S(1)}, bf16[128,128]{1,0:T(8,128)(2,1)S(1)}, u32[]{:S(2)}, u32[]{:S(2)}) collective-permute-start(bf16[128,128]{1,0:T(8,128)(2,1)S(1)} %slice.131), channel_id=1, source_target_pairs={{0,4},{4,8},{8,12},{12,16},{16,20},{20,24},{24,28},{28,32},{32,36}... | collective-permute-start | bytes 98312 | tf_op jit(solution)/shard_map/ppermute | solution.py:25
  177.1 2.3 %fusion.4 = f32[256,2048]{1,0:T(8,128)S(1)} fusion(bf16[256,512]{1,0:T(8,128)(2,1)S(1)} %bitcast.101, bf16[2048,1920]{1,0:T(8,128)(2,1)} %all-gather.2.cloned.1.call-done), kind=kOutput, calls=%fused_computation.5 | convolution fusion | flops 536870912 | bytes 4456448 | tf_op jit(solution)/shard_map/dot_general | solution.py:285
  182.1 2.4 %fusion.2 = bf16[256,2048]{1,0:T(8,128)(2,1)S(1)} fusion(f32[256,2048]{1,0:T(8,128)S(1)} %fusion.4, bf16[2048,1920]{1,0:T(8,128)(2,1)} %all-gather.2.cloned.1.call-done, bf16[64,8,2,128]{3,2,1,0:T(2,128)(2,1)S(1)} %bitcast.108), kind=kOutput, calls=%fused_computation.3 | convolution fusion | flops 537919488 | bytes 5505024 | tf_op jit(solution)/shard_map/dot_general | solution.py:286
  184.5 17.8 %all_to_all.25 = bf16[4,64,2048]{2,1,0:T(8,128)(2,1)S(1)} all-to-all(bf16[4,64,2048]{2,1,0:T(8,128)(2,1)S(1)} %bitcast.99), channel_id=1, replica_groups=mesh['sp_0'=8,'sp_1'=8,'sp_2'=2,'tp'=4] {'tp'}, dimensions={0} | all-to-all | bytes 2097152 | tf_op jit(solution)/shard_map/all_to_all | solution.py:49
  (117 shorter events, 18.7 us)
Async XLA Ops:
  6.5 163.0 %all-gather.2.cloned.1.call-start = ((), (), s32[]{:S(2)}) async-start(), calls=%async_computation.5 | async-start | bytes 7925760 | tf_op jit(solution)/shard_map/all_gather | solution.py:32
  10.3 9.9 %collective-permute-start = (bf16[64,2048]{1,0:T(8,128)(2,1)S(1)}, bf16[64,2048]{1,0:T(8,128)(2,1)S(1)}, u32[]{:S(2)}, u32[]{:S(2)}) collective-permute-start(bf16[64,2048]{1,0:T(8,128)(2,1)S(1)} %fusion.17), channel_id=1, source_target_pairs={{0,4},{4,0},{1,5},{5,1},{2,6},{6,2},{3,7},{7,3},{8,12},{12,8},{9,1... | collective-permute-start | bytes 786440 | tf_op jit(solution)/shard_map/ppermute | solution.py:75
  21.9 3.8 %copy-start.5 = (bf16[16,512]{1,0:T(8,128)(2,1)S(1)}, bf16[16,512]{1,0:T(8,128)(2,1)}, u32[]{:S(2)}) copy-start(bf16[16,512]{1,0:T(8,128)(2,1)} %param.16) | copy-start | bytes 49156
  21.9 3.8 %copy-start.6 = (bf16[16,256]{1,0:T(8,128)(2,1)S(1)}, bf16[16,256]{1,0:T(8,128)(2,1)}, u32[]{:S(2)}) copy-start(bf16[16,256]{1,0:T(8,128)(2,1)} %param.15) | copy-start | bytes 24580
  21.9 29.8 %all-to-all-start = ((bf16[4,2,64,2048]{3,2,1,0:T(8,128)(2,1)}), bf16[4,2,64,2048]{3,2,1,0:T(8,128)(2,1)S(1)}, u32[]{:S(2)}, u32[]{:S(2)}) async-start(bf16[4,2,64,2048]{3,2,1,0:T(8,128)(2,1)} %broadcast_in_dim.24), calls=%async_computation | async-start | bytes 4194304 | tf_op jit(solution)/shard_map/all_to_all | solution.py:245
  25.7 40.8 %copy-start.7 = (f32[2,256]{1,0:T(2,128)S(1)}, f32[2,256]{1,0:T(2,128)}, u32[]{:S(2)}) copy-start(f32[2,256]{1,0:T(2,128)} %param.17) | copy-start | bytes 6148
  52.9 62.3 %all-to-all-start.1 = ((bf16[128,16,384]{2,1,0:T(8,128)(2,1)}), bf16[128,16,384]{2,1,0:T(8,128)(2,1)}, u32[]{:S(2)}, u32[]{:S(2)}) async-start(bf16[128,16,384]{2,1,0:T(8,128)(2,1)} %bitcast.4), calls=%async_computation.1 | async-start | bytes 3145728 | tf_op jit(solution)/shard_map/all_to_all | solution.py:115
  66.6 5.6 %collective-permute-start.3 = (f32[2,256]{1,0:T(2,128)S(1)}, f32[2,256]{1,0:T(2,128)S(1)}, u32[]{:S(2)}, u32[]{:S(2)}) collective-permute-start(f32[2,256]{1,0:T(2,128)S(1)} %copy-done.7), channel_id=1, source_target_pairs={{0,4},{4,0},{1,5},{5,1},{2,6},{6,2},{3,7},{7,3},{8,12},{12,8},{9,1... | collective-permute-start | bytes 6152 | tf_op jit(solution)/shard_map/ppermute | solution.py:75
  121.1 23.2 %all-to-all-start.2 = ((f32[64,3,256]{2,1,0:T(4,128)}), f32[64,3,256]{2,1,0:T(4,128)S(1)}, u32[]{:S(2)}, u32[]{:S(2)}) async-start(f32[64,3,256]{2,1,0:T(4,128)} %concatenate.58), calls=%async_computation.2 | async-start | bytes 524288 | tf_op jit(solution)/shard_map/all_to_all | solution.py:98
  132.7 19.9 %collective-permute-start.2 = (bf16[256,128]{1,0:T(8,128)(2,1)S(1)}, bf16[256,128]{1,0:T(8,128)(2,1)S(1)}, u32[]{:S(2)}, u32[]{:S(2)}) collective-permute-start(bf16[256,128]{1,0:T(8,128)(2,1)S(1)} %dynamic-slice_bitcast_fusion), channel_id=1, source_target_pairs={{0,4},{4,0},{1,5},{5,1},{2,6},{6,2},{3,7},{7,3},{8,12},{12,8},{9,1... | collective-permute-start | bytes 196616 | tf_op jit(solution)/shard_map/ppermute | solution.py:75
  135.7 33.0 %collective-permute-start.1 = (bf16[256,256]{1,0:T(8,128)(2,1)S(1)}, bf16[256,256]{1,0:T(8,128)(2,1)S(1)}, u32[]{:S(2)}, u32[]{:S(2)}) collective-permute-start(bf16[256,256]{1,0:T(8,128)(2,1)S(1)} %bitcast.117), channel_id=1, source_target_pairs={{0,4},{4,0},{1,5},{5,1},{2,6},{6,2},{3,7},{7,3},{8,12},{12,8},{9,1... | collective-permute-start | bytes 393224 | tf_op jit(solution)/shard_map/ppermute | solution.py:75
  144.2 0.7 copy-start.1
  146.7 17.4 %all-to-all-start.3 = ((f32[64,2,256]{2,1,0:T(2,128)}), f32[64,2,256]{2,1,0:T(2,128)S(1)}, u32[]{:S(2)}, u32[]{:S(2)}) async-start(f32[64,2,256]{2,1,0:T(2,128)} %shard_map.118), calls=%async_computation.3 | async-start | bytes 262144 | tf_op jit(solution)/shard_map/all_to_all | solution.py:102
  152.6 16.9 %copy-start = (bf16[4,1,64,2048]{3,2,1,0:T(8,128)(2,1)S(1)}, bf16[4,1,64,2048]{3,2,1,0:T(8,128)(2,1)}, u32[]{:S(2)}) copy-start(bf16[4,1,64,2048]{3,2,1,0:T(8,128)(2,1)} %slice.122) | copy-start | bytes 3145732
  164.4 5.0 %collective-permute-start.4 = (bf16[2,128,256]{1,2,0:T(8,128)(2,1)S(1)}, bf16[2,128,256]{1,2,0:T(8,128)(2,1)S(1)}, u32[]{:S(2)}, u32[]{:S(2)}) collective-permute-start(bf16[2,128,256]{1,2,0:T(8,128)(2,1)S(1)} %bitcast.118), channel_id=1, source_target_pairs={{0,4},{4,0},{1,5},{5,1},{2,6},{6,2},{3,7},{7,3},{8,12},{12,8},{9,1... | collective-permute-start | bytes 393224 | tf_op jit(solution)/shard_map/ppermute | solution.py:75
  169.5 3.5 %copy-start.3 = (f32[256,64]{0,1:T(8,128)S(1)}, f32[256,64]{0,1:T(8,128)}, u32[]{:S(2)}) copy-start(f32[256,64]{0,1:T(8,128)} %get-tuple-element.32) | copy-start | bytes 196612
  169.5 3.5 %copy-start.4 = (f32[256,64]{0,1:T(8,128)S(1)}, f32[256,64]{0,1:T(8,128)}, u32[]{:S(2)}) copy-start(f32[256,64]{0,1:T(8,128)} %get-tuple-element.33) | copy-start | bytes 196612
  174.5 5.5 %collective-permute-start.5 = (bf16[128,128]{1,0:T(8,128)(2,1)S(1)}, bf16[128,128]{1,0:T(8,128)(2,1)S(1)}, u32[]{:S(2)}, u32[]{:S(2)}) collective-permute-start(bf16[128,128]{1,0:T(8,128)(2,1)S(1)} %slice.131), channel_id=1, source_target_pairs={{0,4},{4,8},{8,12},{12,16},{16,20},{20,24},{24,28},{28,32},{32,36}... | collective-permute-start | bytes 98312 | tf_op jit(solution)/shard_map/ppermute | solution.py:25
  179.5 0.8 copy-start.2
  179.5 1.3 copy-start.8
Sparse Core Ops, SparseCore 0:
  10.5 117.4 all-gather.1

commit v2 on v1

--- a/solution.py
+++ b/solution.py
@@ -25,17 +25,10 @@
     return lax.ppermute(value, axis, [(source, source + steps) for source in range(initial, last)])
 
 
-def gather_turned(arrays, axis, dims):
-    turned = [jnp.moveaxis(a, dim, 0) for a, dim in zip(arrays, dims)]
-    widths = [t[0].size for t in turned]
-    both = jnp.concatenate([t.reshape(-1, w) for t, w in zip(turned, widths)], axis=1)
-    whole = lax.all_gather(both, axis, axis=0, tiled=True)
-    tiles = jnp.split(whole, [sum(widths[:k]) for k in range(1, len(widths))], axis=1)
-    return tuple(
-        (
-            jnp.moveaxis(b.reshape(-1, *t.shape[1:]), 0, dim)
-            for b, t, dim in zip(tiles, turned, dims)
-        )
+def from_everyone(value, axis):
+    size = lax.axis_size(axis)
+    return lax.all_to_all(
+        jnp.broadcast_to(value[None], (size, *value.shape)), axis, 0, 0, tiled=True
     )
 
 
@@ -103,17 +96,28 @@
 
 
 def weight_of_head(ret_key, ret_value):
-    devices = lax.axis_size(SP)
     rows = ret_key.shape[0]
     heads = lax.axis_size(CORE)
     keys = ret_key.reshape(rows, heads, RETAIN_KEY_SIZE)
     values = ret_value.reshape(rows, heads, V_DIM)
     both = jnp.moveaxis(jnp.concatenate([keys, values], axis=2), 1, 0)
-    sent = jnp.broadcast_to(both[None], (devices // heads, *both.shape)).reshape(
-        devices, rows, -1
-    )
-    arrived = lax.all_to_all(sent, SP, 0, 0, tiled=True)
-    return arrived.reshape(devices * rows, -1)
+    core = lax.axis_index(CORE)
+    mine = lax.dynamic_index_in_dim(both, core, 0, keepdims=False)
+    theirs = lax.dynamic_index_in_dim(both, 1 - core, 0, keepdims=False)
+    block = in_core_order(mine, core_swap(theirs), 0)
+    arrived = from_everyone(block, ZY)
+    return arrived.reshape(-1, block.shape[-1])
+
+
+def gathered_rows(value, axis):
+    size = lax.axis_size(axis)
+    pieces = [value] + [
+        lax.ppermute(value, axis, [((k + step) % size, k) for k in range(size)])
+        for step in range(1, size)
+    ]
+    turned = jnp.concatenate(pieces + pieces[:-1], axis=0)
+    start = (size - lax.axis_index(axis)) % size * value.shape[0]
+    return lax.dynamic_slice_in_dim(turned, start, size * value.shape[0], 0)
 
 
 def chain_of_head(kv, log_decay, anchor):
@@ -172,16 +176,12 @@
     return final_product.reshape(tok_count, heads_here * V_DIM).astype(jnp.bfloat16)
 
 
-def attention_path(query_att, key_att, value_att, sink_logits, anchor):
+def attention_path(query_att, stacked, sink_logits, anchor):
     tok_count = query_att.shape[0]
-    kv_here = key_att.shape[1] // HEAD_DIM
+    kv_here = stacked.shape[1] // (2 * HEAD_DIM)
     group_size = query_att.shape[1] // (kv_here * HEAD_DIM)
-    stacked = jnp.concatenate([key_att, value_att], axis=1)
-    window_rim = shifted(stacked[tok_count - WINDOW :], SP, 1)
     blocks = tok_count // WINDOW
-    extended = jnp.concatenate([window_rim, stacked], axis=0).reshape(
-        blocks + 1, WINDOW, 2, kv_here, HEAD_DIM
-    )
+    extended = stacked.reshape(blocks + 1, WINDOW, 2, kv_here, HEAD_DIM)
     paired = jnp.concatenate([extended[:-1], extended[1:]], axis=1)
     keys_pair = paired[:, :, 0]
     values_pair = paired[:, :, 1]
@@ -234,26 +234,20 @@
     weights = (ret_query, att_query, att_key, att_value)
     widths = [weight.shape[1] for weight in weights]
     points = [sum(widths[:index]) for index in range(1, len(widths))]
-    every_weight = gather_turned(
-        (ret_query, att_query, att_key, att_value, ret_out, att_out), SP, (0, 0, 0, 0, 1, 1)
-    )
-    gathered = every_weight[:4]
-    out_whole = every_weight[4:]
-
-    pair = jnp.stack([normed, core_swap(normed)])
-    size = lax.axis_size("tp")
-    arrived = lax.all_to_all(
-        jnp.broadcast_to(pair[None], (size, *pair.shape)), "tp", 0, 0, tiled=True
-    )
-    chip_rows = arrived.reshape(-1, arrived.shape[-1])
+    whole = lax.all_gather(
+        jnp.concatenate([*weights, ret_out.T, att_out.T], axis=1), SP, axis=0, tiled=True
+    )
     head_weight = weight_of_head(ret_key, ret_value)
+    own_rows = gathered_rows(normed, "tp")
+    other_rows = core_swap(own_rows)
+    tok_count = own_rows.shape[0]
+    rim = shifted(own_rows[tok_count - WINDOW :], SP, 1)
+    chip_rows = jnp.concatenate([own_rows, other_rows], axis=0)
     kv = jnp.dot(chip_rows, head_weight, preferred_element_type=jnp.float32).astype(jnp.bfloat16)
-    kv = jnp.moveaxis(kv.reshape(size, 2, -1, kv.shape[-1]), 1, 0)
-    kv = kv.reshape(2, -1, kv.shape[-1])
+    kv = kv.reshape(2, tok_count, kv.shape[-1])
     decay_other = core_swap(log_decay)
     own_head = lax.dynamic_index_in_dim(log_decay, core, 0, keepdims=False)
     other_half = lax.dynamic_index_in_dim(decay_other, core, 0, keepdims=False)
-    tok_count = kv.shape[1]
     anchor = lax.axis_index(SP) * tok_count
     chip_anchor = lax.axis_index(ZY) * (2 * tok_count)
     keys, values, before = chain_of_head(
@@ -270,24 +264,29 @@
     value_ret = heads_of_own_rows(values)
     before = heads_of_own_rows(before)
 
-    joined = jnp.concatenate(gathered, axis=1)
-    own_rows = arrived.reshape(size, 2, -1, arrived.shape[-1])[:, 0].reshape(tok_count, -1)
-    projected = jnp.dot(own_rows, joined, preferred_element_type=jnp.float32).astype(jnp.bfloat16)
+    input_width = sum(widths)
+    projected = jnp.dot(
+        own_rows, whole[:, :input_width], preferred_element_type=jnp.float32
+    ).astype(jnp.bfloat16)
+    rim_kv = jnp.dot(
+        rim, whole[:, points[1] : input_width], preferred_element_type=jnp.float32
+    ).astype(jnp.bfloat16)
     sections = jnp.split(projected, points, axis=1)
+    stacked = jnp.concatenate([rim_kv, projected[:, points[1] :]], axis=0)
     positions = anchor + jnp.arange(tok_count, dtype=jnp.int32)
     query_ret = rotate(sections[0].reshape(tok_count, -1, RETAIN_KEY_SIZE), positions).astype(
         jnp.bfloat16
     )
     ret_mix = retention_path(query_ret, key_ret, value_ret, log_decay, before)
-    att_mix = attention_path(sections[1], sections[2], sections[3], sink_logits, anchor)
-    mixed = sent_and_summed(
-        (
-            jnp.dot(ret_mix, out_whole[0], preferred_element_type=jnp.float32)
-            + jnp.dot(att_mix, out_whole[1], preferred_element_type=jnp.float32)
-        ).astype(jnp.bfloat16),
-        "tp",
-        0,
-    )
+    att_mix = attention_path(sections[1], stacked, sink_logits, anchor)
+    mixes = jnp.concatenate([ret_mix, att_mix], axis=1)
+    partial = lax.dot_general(
+        mixes,
+        whole[:, input_width:],
+        (((1,), (1,)), ((), ())),
+        preferred_element_type=jnp.float32,
+    )
+    mixed = sent_and_summed(partial.astype(jnp.bfloat16), "tp", 0)
     return mixed.astype(jnp.bfloat16)
 
 

time: 211 us -> 185 us (0.88)
  waiting for transfers between devices: 83.6 us -> 45.8 us
  starting transfers between devices: 55.5 us -> 64.8 us
    all_to_all x2 -> x1, waiting for transfers between devices: 65.1 us -> 29.6 us  [from_everyone(): lax.all_to_all(jnp.broadcast_to(value[None], (size, *value.shape)), axis,...]
    ppermute x0 -> x3, starting transfers between devices: none -> 10.1 us  [gathered_rows(): lax.ppermute(value, axis, [((k + step) % size, k) for k in range(size)])]
    all_to_all x2 -> x1, starting transfers between devices: 17.4 us -> 13.6 us  [from_everyone(): lax.all_to_all(jnp.broadcast_to(value[None], (size, *value.shape)), axis,...]
    all_to_all x1, waiting for transfers between devices: 6.35 us -> 3.64 us  [state_before(): arrived = lax.all_to_all(sent, ZY, 0, 0, tiled=True)]
    ppermute x1, starting transfers between devices: 2.59 us -> 4.95 us  [shifted(): lax.ppermute(value, axis, [(source, source + steps) for source in range(i...]
    ppermute x5 -> x6, starting transfers between devices: 20.2 us -> 19.7 us  [core_swap(): return lax.ppermute(value, CORE, [(0, 1), (1, 0)])]
  transfers between devices with their start and end apart: 11 -> 14, of which waited for: 5 -> 4; matrix products, arithmetic and copies ran while one was open for 11% -> 14% of each run, Pallas kernels for 1% -> 1%
where the time goes in v2:
time: 185 us; the launch traced here: 184 us
  starting transfers between devices  64.8 us (35%)
  waiting for transfers between devices  45.8 us (25%)
  blocking collectives  18.1 us (10%)
  between operations  16.9 us (9%)
  local copies, waits for them, and re-layouts  14.2 us (8%)
  matrix products  13.7 us (7%)
  other arithmetic  8.31 us (4%)
    all_to_all x1, waiting for transfers between devices, from_everyone(): lax.all_to_all(jnp.broadcast_to(value[None], (size, *value.shape)), axis,...  29.6 us
    ppermute x6, starting transfers between devices, core_swap(): return lax.ppermute(value, CORE, [(0, 1), (1, 0)])  19.7 us
    all_to_all x1, blocking collectives, sent_and_summed(): lax.all_to_all(tiles, axis, split_axis=0, concat_axis=0, tiled=True)  18.1 us
    all_to_all x1, starting transfers between devices, from_everyone(): lax.all_to_all(jnp.broadcast_to(value[None], (size, *value.shape)), axis,...  13.6 us
    all_to_all x1, waiting for transfers between devices, state_before(): lax.all_to_all(prefix, ZY, 0, 0, tiled=True).reshape(RETAIN_KEY_SIZE, V_DIM)  12 us
    ppermute x3, starting transfers between devices, gathered_rows(): lax.ppermute(value, axis, [((k + step) % size, k) for k in range(size)])  10.1 us
    all_to_all x1, starting transfers between devices, state_before(): arrived = lax.all_to_all(sent, ZY, 0, 0, tiled=True)  8.63 us
    all_to_all x1, starting transfers between devices, state_before(): lax.all_to_all(prefix, ZY, 0, 0, tiled=True).reshape(RETAIN_KEY_SIZE, V_DIM)  7.79 us
  transfers between devices with their start and end apart: 14, of which 4 were waited for; matrix products, arithmetic and copies ran while one was open for 14% of the time, Pallas kernels for 1%

profile of v2, /device:TPU:1, one launch (start us, length us, event | category | flops | bytes accessed | tf_op | source)
XLA Modules:
  0.0 183.5 jit_solution(5546180245445464101)
XLA Ops:
  6.5 1.5 concatenate.61
  10.3 5.2 %collective-permute-start = (bf16[64,2048]{1,0:T(8,128)(2,1)S(1)}, bf16[64,2048]{1,0:T(8,128)(2,1)S(1)}, u32[]{:S(2)}, u32[]{:S(2)}) collective-permute-start(bf16[64,2048]{1,0:T(8,128)(2,1)S(1)} %get-tuple-element.11), channel_id=1, source_target_pairs={{1,0},{2,1},{3,2},{0,3},{5,4},{6,5},{7,6},{4,7},{9,8},{10,9},{11,1... | collective-permute-start | bytes 786440 | tf_op jit(solution)/shard_map/ppermute | solution.py:115
  15.5 2.4 %collective-permute-start.1 = (bf16[64,2048]{1,0:T(8,128)(2,1)S(1)}, bf16[64,2048]{1,0:T(8,128)(2,1)S(1)}, u32[]{:S(2)}, u32[]{:S(2)}) collective-permute-start(bf16[64,2048]{1,0:T(8,128)(2,1)S(1)} %get-tuple-element.11), channel_id=1, source_target_pairs={{2,0},{3,1},{0,2},{1,3},{6,4},{7,5},{4,6},{5,7},{10,8},{11,9},{8,1... | collective-permute-start | bytes 786440 | tf_op jit(solution)/shard_map/ppermute | solution.py:115
  18.0 2.5 %collective-permute-start.2 = (bf16[64,2048]{1,0:T(8,128)(2,1)S(1)}, bf16[64,2048]{1,0:T(8,128)(2,1)S(1)}, u32[]{:S(2)}, u32[]{:S(2)}) collective-permute-start(bf16[64,2048]{1,0:T(8,128)(2,1)S(1)} %get-tuple-element.11), channel_id=1, source_target_pairs={{3,0},{0,1},{1,2},{2,3},{7,4},{4,5},{5,6},{6,7},{11,8},{8,9},{9,10... | collective-permute-start | bytes 786440 | tf_op jit(solution)/shard_map/ppermute | solution.py:115
  22.0 6.4 %collective-permute-start.4 = (bf16[16,384]{1,0:T(8,128)(2,1)S(1)}, bf16[16,384]{1,0:T(8,128)(2,1)S(1)}, u32[]{:S(2)}, u32[]{:S(2)}) collective-permute-start(bf16[16,384]{1,0:T(8,128)(2,1)S(1)} %bitcast.100), channel_id=1, source_target_pairs={{0,4},{4,0},{1,5},{5,1},{2,6},{6,2},{3,7},{7,3},{8,12},{12,8},{9,1... | collective-permute-start | bytes 36872 | tf_op jit(solution)/shard_map/ppermute | solution.py:68
  28.4 1.9 %collective-permute-start.7 = (f32[2,256]{1,0:T(2,128)}, f32[2,256]{1,0:T(2,128)S(1)}, u32[]{:S(2)}, u32[]{:S(2)}) collective-permute-start(f32[2,256]{1,0:T(2,128)} %param.17), channel_id=1, source_target_pairs={{0,4},{4,0},{1,5},{5,1},{2,6},{6,2},{3,7},{7,3},{8,12},{12,8},{9,1... | collective-permute-start | bytes 6152 | tf_op jit(solution)/shard_map/ppermute | solution.py:68
  33.4 13.6 %all-to-all-start = ((bf16[64,32,384]{2,1,0:T(8,128)(2,1)}), bf16[64,32,384]{2,1,0:T(8,128)(2,1)}, u32[]{:S(2)}, u32[]{:S(2)}) async-start(bf16[64,32,384]{2,1,0:T(8,128)(2,1)} %broadcast_in_dim.22), calls=%async_computation | async-start | bytes 3145728 | tf_op jit(solution)/shard_map/all_to_all | solution.py:30
  47.4 2.7 %collective-permute-start.3 = (bf16[256,2048]{1,0:T(8,128)(2,1)S(1)}, bf16[256,2048]{1,0:T(8,128)(2,1)}, u32[]{:S(2)}, u32[]{:S(2)}) collective-permute-start(bf16[256,2048]{1,0:T(8,128)(2,1)S(1)} %constant_dynamic-slice_fusion.11), channel_id=1, source_target_pairs={{0,4},{4,0},{1,5},{5,1},{2,6},{6,2},{3,7},{7,3},{8,12},{12,8},{9,1... | collective-permute-start | bytes 3145736 | tf_op jit(solution)/shard_map/ppermute | solution.py:68
  57.3 29.6 %all-to-all-done = bf16[64,32,384]{2,1,0:T(8,128)(2,1)} async-done(((bf16[64,32,384]{2,1,0:T(8,128)(2,1)}), bf16[64,32,384]{2,1,0:T(8,128)(2,1)}, u32[]{:S(2)}, u32[]{:S(2)}) %all-to-all-start) | async-done | bytes 1572896 | tf_op jit(solution)/shard_map/all_to_all | solution.py:30
  86.8 2.8 %fusion.15 = bf16[512,384]{0,1:T(8,128)(2,1)S(1)} fusion(bf16[2048,384]{1,0:T(8,128)(2,1)} %bitcast, bf16[256,2048]{1,0:T(8,128)(2,1)} %collective-permute-done.3, bf16[256,2048]{1,0:T(8,128)(2,1)S(1)} %constant_dynamic-slice_fusion.11), kind=kOutput, calls=%fused_computation.14 | convolution fusion | flops 809697280 | bytes 4063232 | tf_op jit(solution)/shard_map/dot_general | solution.py:246
  91.6 1.4 concatenate.68
  92.9 8.6 %all-to-all-start.1 = ((f32[64,3,256]{2,1,0:T(4,128)}), f32[64,3,256]{2,1,0:T(4,128)S(1)}, u32[]{:S(2)}, u32[]{:S(2)}) async-start(f32[64,3,256]{2,1,0:T(4,128)} %concatenate.68), calls=%async_computation.1 | async-start | bytes 524288 | tf_op jit(solution)/shard_map/all_to_all | solution.py:91
  102.5 4.9 %collective-permute-start.9 = (bf16[128,2048]{1,0:T(8,128)(2,1)}, bf16[128,2048]{1,0:T(8,128)(2,1)}, u32[]{:S(2)}, u32[]{:S(2)}) collective-permute-start(bf16[128,2048]{1,0:T(8,128)(2,1)} %constant_dynamic-slice_fusion), channel_id=1, source_target_pairs={{0,4},{4,8},{8,12},{12,16},{16,20},{20,24},{24,28},{28,32},{32,36}... | collective-permute-start | bytes 1572872 | tf_op jit(solution)/shard_map/ppermute | solution.py:25
  107.9 1.9 %collective-permute-start.6 = (bf16[256,128]{1,0:T(8,128)(2,1)S(1)}, bf16[256,128]{1,0:T(8,128)(2,1)S(1)}, u32[]{:S(2)}, u32[]{:S(2)}) collective-permute-start(bf16[256,128]{1,0:T(8,128)(2,1)S(1)} %bitcast.97), channel_id=1, source_target_pairs={{0,4},{4,0},{1,5},{5,1},{2,6},{6,2},{3,7},{7,3},{8,12},{12,8},{9,1... | collective-permute-start | bytes 196616 | tf_op jit(solution)/shard_map/ppermute | solution.py:68
  110.7 2.4 %collective-permute-start.5 = (bf16[256,256]{1,0:T(8,128)(2,1)S(1)}, bf16[256,256]{1,0:T(8,128)(2,1)S(1)}, u32[]{:S(2)}, u32[]{:S(2)}) collective-permute-start(bf16[256,256]{1,0:T(8,128)(2,1)S(1)} %bitcast.95), channel_id=1, source_target_pairs={{0,4},{4,0},{1,5},{5,1},{2,6},{6,2},{3,7},{7,3},{8,12},{12,8},{9,1... | collective-permute-start | bytes 393224 | tf_op jit(solution)/shard_map/ppermute | solution.py:68
  113.3 3.6 %all-to-all-done.1.parts_ref = f32[64,3,256]{2,1,0:T(4,128)S(1)} async-done(((f32[64,3,256]{2,1,0:T(4,128)}), f32[64,3,256]{2,1,0:T(4,128)S(1)}, u32[]{:S(2)}, u32[]{:S(2)}) %all-to-all-start.1) | async-done | bytes 196640 | tf_op jit(solution)/shard_map/all_to_all | solution.py:91
  117.6 1.7 shard_map.118
  119.4 7.8 %all-to-all-start.2 = ((f32[64,2,256]{2,1,0:T(2,128)}), f32[64,2,256]{2,1,0:T(2,128)S(1)}, u32[]{:S(2)}, u32[]{:S(2)}) async-start(f32[64,2,256]{2,1,0:T(2,128)} %shard_map.118), calls=%async_computation.2 | async-start | bytes 262144 | tf_op jit(solution)/shard_map/all_to_all | solution.py:95
  127.2 12.0 %all-to-all-done.2 = f32[64,2,256]{2,1,0:T(2,128)S(1)} async-done(((f32[64,2,256]{2,1,0:T(2,128)}), f32[64,2,256]{2,1,0:T(2,128)S(1)}, u32[]{:S(2)}, u32[]{:S(2)}) %all-to-all-start.2) | async-done | bytes 131104 | tf_op jit(solution)/shard_map/all_to_all | solution.py:95
  139.6 4.4 %collective-permute-start.8 = (bf16[2,128,256]{1,2,0:T(8,128)(2,1)S(1)}, bf16[2,128,256]{1,2,0:T(8,128)(2,1)S(1)}, u32[]{:S(2)}, u32[]{:S(2)}) collective-permute-start(bf16[2,128,256]{1,2,0:T(8,128)(2,1)S(1)} %bitcast.96), channel_id=1, source_target_pairs={{0,4},{4,0},{1,5},{5,1},{2,6},{6,2},{3,7},{7,3},{8,12},{12,8},{9,1... | collective-permute-start | bytes 393224 | tf_op jit(solution)/shard_map/ppermute | solution.py:68
  144.8 3.3 %fusion.12 = bf16[256,896]{1,0:T(8,128)(2,1)S(1)} fusion(bf16[256,2048]{1,0:T(8,128)(2,1)S(1)} %copy-done.1, bf16[2048,1920]{1,0:T(8,128)(2,1)} %all-gather.2.cloned.1.call-done), kind=kOutput, calls=%fused_computation.13 | convolution fusion | flops 939753472 | bytes 5177344 | tf_op jit(solution)/shard_map/dot_general | solution.py:268
  149.9 1.5 convolution_convert_fusion.1
  154.2 3.5 %fusion.4 = bf16[256,2048]{1,0:T(8,128)(2,1)S(1)} fusion(bf16[2048,1920]{1,0:T(8,128)(2,1)} %all-gather.2.cloned.1.call-done, bf16[256,512]{1,0:T(8,128)(2,1)S(1)} %reshape.443, bf16[256,512]{1,0:T(8,128)(2,1)S(1)} %bitcast.94), kind=kOutput, calls=%fused_computation.4 | convolution fusion | flops 1075314688 | bytes 5767168 | tf_op jit(solution)/shard_map/dot_general | solution.py:283
  157.7 18.1 %all_to_all.20 = bf16[4,64,2048]{2,1,0:T(8,128)(2,1)S(1)} all-to-all(bf16[4,64,2048]{2,1,0:T(8,128)(2,1)S(1)} %bitcast.87), channel_id=1, replica_groups=mesh['sp_0'=8,'sp_1'=8,'sp_2'=2,'tp'=4] {'tp'}, dimensions={0} | all-to-all | bytes 2097152 | tf_op jit(solution)/shard_map/all_to_all | solution.py:42
  (131 shorter events, 22.9 us)
Async XLA Ops:
  6.5 138.3 %all-gather.2.cloned.1.call-start = ((), (), s32[]{:S(2)}) async-start(), calls=%async_computation.4 | async-start | bytes 7925760 | tf_op jit(solution)/shard_map/all_gather | solution.py:237
  10.3 36.8 %collective-permute-start = (bf16[64,2048]{1,0:T(8,128)(2,1)S(1)}, bf16[64,2048]{1,0:T(8,128)(2,1)S(1)}, u32[]{:S(2)}, u32[]{:S(2)}) collective-permute-start(bf16[64,2048]{1,0:T(8,128)(2,1)S(1)} %get-tuple-element.11), channel_id=1, source_target_pairs={{1,0},{2,1},{3,2},{0,3},{5,4},{6,5},{7,6},{4,7},{9,8},{10,9},{11,1... | collective-permute-start | bytes 786440 | tf_op jit(solution)/shard_map/ppermute | solution.py:115
  15.5 31.6 %collective-permute-start.1 = (bf16[64,2048]{1,0:T(8,128)(2,1)S(1)}, bf16[64,2048]{1,0:T(8,128)(2,1)S(1)}, u32[]{:S(2)}, u32[]{:S(2)}) collective-permute-start(bf16[64,2048]{1,0:T(8,128)(2,1)S(1)} %get-tuple-element.11), channel_id=1, source_target_pairs={{2,0},{3,1},{0,2},{1,3},{6,4},{7,5},{4,6},{5,7},{10,8},{11,9},{8,1... | collective-permute-start | bytes 786440 | tf_op jit(solution)/shard_map/ppermute | solution.py:115
  18.0 29.2 %collective-permute-start.2 = (bf16[64,2048]{1,0:T(8,128)(2,1)S(1)}, bf16[64,2048]{1,0:T(8,128)(2,1)S(1)}, u32[]{:S(2)}, u32[]{:S(2)}) collective-permute-start(bf16[64,2048]{1,0:T(8,128)(2,1)S(1)} %get-tuple-element.11), channel_id=1, source_target_pairs={{3,0},{0,1},{1,2},{2,3},{7,4},{4,5},{5,6},{6,7},{11,8},{8,9},{9,10... | collective-permute-start | bytes 786440 | tf_op jit(solution)/shard_map/ppermute | solution.py:115
  22.0 10.1 %collective-permute-start.4 = (bf16[16,384]{1,0:T(8,128)(2,1)S(1)}, bf16[16,384]{1,0:T(8,128)(2,1)S(1)}, u32[]{:S(2)}, u32[]{:S(2)}) collective-permute-start(bf16[16,384]{1,0:T(8,128)(2,1)S(1)} %bitcast.100), channel_id=1, source_target_pairs={{0,4},{4,0},{1,5},{5,1},{2,6},{6,2},{3,7},{7,3},{8,12},{12,8},{9,1... | collective-permute-start | bytes 36872 | tf_op jit(solution)/shard_map/ppermute | solution.py:68
  28.4 23.8 %collective-permute-start.7 = (f32[2,256]{1,0:T(2,128)}, f32[2,256]{1,0:T(2,128)S(1)}, u32[]{:S(2)}, u32[]{:S(2)}) collective-permute-start(f32[2,256]{1,0:T(2,128)} %param.17), channel_id=1, source_target_pairs={{0,4},{4,0},{1,5},{5,1},{2,6},{6,2},{3,7},{7,3},{8,12},{12,8},{9,1... | collective-permute-start | bytes 6152 | tf_op jit(solution)/shard_map/ppermute | solution.py:68
  33.4 53.4 %all-to-all-start = ((bf16[64,32,384]{2,1,0:T(8,128)(2,1)}), bf16[64,32,384]{2,1,0:T(8,128)(2,1)}, u32[]{:S(2)}, u32[]{:S(2)}) async-start(bf16[64,32,384]{2,1,0:T(8,128)(2,1)} %broadcast_in_dim.22), calls=%async_computation | async-start | bytes 3145728 | tf_op jit(solution)/shard_map/all_to_all | solution.py:30
  47.2 5.1 %copy-start.7 = (f32[2,256]{1,0:T(2,128)S(1)}, f32[2,256]{1,0:T(2,128)}, u32[]{:S(2)}) copy-start(f32[2,256]{1,0:T(2,128)} %param.17) | copy-start | bytes 6148
  47.4 39.4 %copy-start = (bf16[256,2048]{1,0:T(8,128)(2,1)}, bf16[256,2048]{1,0:T(8,128)(2,1)S(1)}, u32[]{:S(2)}) copy-start(bf16[256,2048]{1,0:T(8,128)(2,1)S(1)} %constant_dynamic-slice_fusion.11) | copy-start | bytes 3145732
  47.4 9.9 %collective-permute-start.3 = (bf16[256,2048]{1,0:T(8,128)(2,1)S(1)}, bf16[256,2048]{1,0:T(8,128)(2,1)}, u32[]{:S(2)}, u32[]{:S(2)}) collective-permute-start(bf16[256,2048]{1,0:T(8,128)(2,1)S(1)} %constant_dynamic-slice_fusion.11), channel_id=1, source_target_pairs={{0,4},{4,0},{1,5},{5,1},{2,6},{6,2},{3,7},{7,3},{8,12},{12,8},{9,1... | collective-permute-start | bytes 3145736 | tf_op jit(solution)/shard_map/ppermute | solution.py:68
  92.9 24.0 %all-to-all-start.1 = ((f32[64,3,256]{2,1,0:T(4,128)}), f32[64,3,256]{2,1,0:T(4,128)S(1)}, u32[]{:S(2)}, u32[]{:S(2)}) async-start(f32[64,3,256]{2,1,0:T(4,128)} %concatenate.68), calls=%async_computation.1 | async-start | bytes 524288 | tf_op jit(solution)/shard_map/all_to_all | solution.py:91
  102.5 47.5 %collective-permute-start.9 = (bf16[128,2048]{1,0:T(8,128)(2,1)}, bf16[128,2048]{1,0:T(8,128)(2,1)}, u32[]{:S(2)}, u32[]{:S(2)}) collective-permute-start(bf16[128,2048]{1,0:T(8,128)(2,1)} %constant_dynamic-slice_fusion), channel_id=1, source_target_pairs={{0,4},{4,8},{8,12},{12,16},{16,20},{20,24},{24,28},{28,32},{32,36}... | collective-permute-start | bytes 1572872 | tf_op jit(solution)/shard_map/ppermute | solution.py:25
  107.9 19.2 %collective-permute-start.6 = (bf16[256,128]{1,0:T(8,128)(2,1)S(1)}, bf16[256,128]{1,0:T(8,128)(2,1)S(1)}, u32[]{:S(2)}, u32[]{:S(2)}) collective-permute-start(bf16[256,128]{1,0:T(8,128)(2,1)S(1)} %bitcast.97), channel_id=1, source_target_pairs={{0,4},{4,0},{1,5},{5,1},{2,6},{6,2},{3,7},{7,3},{8,12},{12,8},{9,1... | collective-permute-start | bytes 196616 | tf_op jit(solution)/shard_map/ppermute | solution.py:68
  110.7 33.2 %collective-permute-start.5 = (bf16[256,256]{1,0:T(8,128)(2,1)S(1)}, bf16[256,256]{1,0:T(8,128)(2,1)S(1)}, u32[]{:S(2)}, u32[]{:S(2)}) collective-permute-start(bf16[256,256]{1,0:T(8,128)(2,1)S(1)} %bitcast.95), channel_id=1, source_target_pairs={{0,4},{4,0},{1,5},{5,1},{2,6},{6,2},{3,7},{7,3},{8,12},{12,8},{9,1... | collective-permute-start | bytes 393224 | tf_op jit(solution)/shard_map/ppermute | solution.py:68
  116.9 0.7 copy-start.3
  119.4 19.8 %all-to-all-start.2 = ((f32[64,2,256]{2,1,0:T(2,128)}), f32[64,2,256]{2,1,0:T(2,128)S(1)}, u32[]{:S(2)}, u32[]{:S(2)}) async-start(f32[64,2,256]{2,1,0:T(2,128)} %shard_map.118), calls=%async_computation.2 | async-start | bytes 262144 | tf_op jit(solution)/shard_map/all_to_all | solution.py:95
  127.2 17.6 %copy-start.1 = (bf16[256,2048]{1,0:T(8,128)(2,1)S(1)}, bf16[256,2048]{1,0:T(8,128)(2,1)}, u32[]{:S(2)}) copy-start(bf16[256,2048]{1,0:T(8,128)(2,1)} %copy-done) | copy-start | bytes 3145732
  139.6 5.2 %collective-permute-start.8 = (bf16[2,128,256]{1,2,0:T(8,128)(2,1)S(1)}, bf16[2,128,256]{1,2,0:T(8,128)(2,1)S(1)}, u32[]{:S(2)}, u32[]{:S(2)}) collective-permute-start(bf16[2,128,256]{1,2,0:T(8,128)(2,1)S(1)} %bitcast.96), channel_id=1, source_target_pairs={{0,4},{4,0},{1,5},{5,1},{2,6},{6,2},{3,7},{7,3},{8,12},{12,8},{9,1... | collective-permute-start | bytes 393224 | tf_op jit(solution)/shard_map/ppermute | solution.py:68
  144.8 3.5 %copy-start.4 = (f32[256,64]{0,1:T(8,128)S(1)}, f32[256,64]{0,1:T(8,128)}, u32[]{:S(2)}) copy-start(f32[256,64]{0,1:T(8,128)} %get-tuple-element.41) | copy-start | bytes 196612
  144.8 3.9 %copy-start.5 = (f32[2,2,128]{2,0,1:T(2,128)S(1)}, f32[2,2,128]{2,0,1:T(2,128)}, u32[]{:S(2)}) copy-start(f32[2,2,128]{2,0,1:T(2,128)} %copy.95) | copy-start | bytes 6148
  148.1 1.4 copy-start.2
  148.1 1.0 copy-start.6
  149.5 2.2 %slice-start = ((bf16[256,896]{1,0:T(8,128)(2,1)}), bf16[256,512]{1,0:T(8,128)(2,1)S(1)}, s32[]{:S(2)}) async-start(bf16[256,896]{1,0:T(8,128)(2,1)} %copy-done.2), calls=%async_computation.5 | async-start | bytes 524288 | tf_op jit(solution)/shard_map/split | solution.py:274
  151.5 1.1 copy-start.8
Sparse Core Ops, SparseCore 0:
  10.5 126.6 all-gather.1

commit v3 on v2

--- a/solution.py
+++ b/solution.py
@@ -95,16 +95,21 @@
     return lax.all_to_all(prefix, ZY, 0, 0, tiled=True).reshape(RETAIN_KEY_SIZE, V_DIM)
 
 
+def columns_of_head(ret_key, ret_value, head):
+    return jnp.concatenate(
+        [
+            lax.dynamic_slice_in_dim(ret_key, head * RETAIN_KEY_SIZE, RETAIN_KEY_SIZE, 1),
+            lax.dynamic_slice_in_dim(ret_value, head * V_DIM, V_DIM, 1),
+        ],
+        axis=1,
+    )
+
+
 def weight_of_head(ret_key, ret_value):
-    rows = ret_key.shape[0]
-    heads = lax.axis_size(CORE)
-    keys = ret_key.reshape(rows, heads, RETAIN_KEY_SIZE)
-    values = ret_value.reshape(rows, heads, V_DIM)
-    both = jnp.moveaxis(jnp.concatenate([keys, values], axis=2), 1, 0)
     core = lax.axis_index(CORE)
-    mine = lax.dynamic_index_in_dim(both, core, 0, keepdims=False)
-    theirs = lax.dynamic_index_in_dim(both, 1 - core, 0, keepdims=False)
-    block = in_core_order(mine, core_swap(theirs), 0)
+    mine = columns_of_head(ret_key, ret_value, core)
+    theirs = core_swap(columns_of_head(ret_key, ret_value, 1 - core))
+    block = in_core_order(mine, theirs, 0)
     arrived = from_everyone(block, ZY)
     return arrived.reshape(-1, block.shape[-1])
 

time: 185 us -> 184 us (level)
  no operation moved by 1% of the time
where the time goes in v3:
time: 184 us; the launch traced here: 183 us
  starting transfers between devices  64.3 us (35%)
  waiting for transfers between devices  46.8 us (25%)
  blocking collectives  18 us (10%)
  between operations  16.9 us (9%)
  matrix products  13.7 us (7%)
  local copies, waits for them, and re-layouts  13.6 us (7%)
  other arithmetic  8.32 us (5%)
    all_to_all x1, waiting for transfers between devices, from_everyone(): lax.all_to_all(jnp.broadcast_to(value[None], (size, *value.shape)), axis,...  29.7 us
    ppermute x6, starting transfers between devices, core_swap(): return lax.ppermute(value, CORE, [(0, 1), (1, 0)])  19.7 us
    all_to_all x1, blocking collectives, sent_and_summed(): lax.all_to_all(tiles, axis, split_axis=0, concat_axis=0, tiled=True)  18 us
    all_to_all x1, starting transfers between devices, from_everyone(): lax.all_to_all(jnp.broadcast_to(value[None], (size, *value.shape)), axis,...  13.6 us
    all_to_all x1, waiting for transfers between devices, state_before(): lax.all_to_all(prefix, ZY, 0, 0, tiled=True).reshape(RETAIN_KEY_SIZE, V_DIM)  12.3 us
    ppermute x3, starting transfers between devices, gathered_rows(): lax.ppermute(value, axis, [((k + step) % size, k) for k in range(size)])  10.1 us
    all_to_all x1, starting transfers between devices, state_before(): arrived = lax.all_to_all(sent, ZY, 0, 0, tiled=True)  8.52 us
    all_to_all x1, starting transfers between devices, state_before(): lax.all_to_all(prefix, ZY, 0, 0, tiled=True).reshape(RETAIN_KEY_SIZE, V_DIM)  7.39 us
  transfers between devices with their start and end apart: 14, of which 4 were waited for; matrix products, arithmetic and copies ran while one was open for 14% of the time, Pallas kernels for 1%

profile of v3, /device:TPU:1, one launch (start us, length us, event | category | flops | bytes accessed | tf_op | source)
XLA Modules:
  0.0 183.3 jit_solution(5708241130288480507)
XLA Ops:
  6.5 1.5 concatenate.65
  10.3 5.2 %collective-permute-start = (bf16[64,2048]{1,0:T(8,128)(2,1)S(1)}, bf16[64,2048]{1,0:T(8,128)(2,1)S(1)}, u32[]{:S(2)}, u32[]{:S(2)}) collective-permute-start(bf16[64,2048]{1,0:T(8,128)(2,1)S(1)} %get-tuple-element.11), channel_id=1, source_target_pairs={{1,0},{2,1},{3,2},{0,3},{5,4},{6,5},{7,6},{4,7},{9,8},{10,9},{11,1... | collective-permute-start | bytes 786440 | tf_op jit(solution)/shard_map/ppermute | solution.py:120
  15.5 2.4 %collective-permute-start.1 = (bf16[64,2048]{1,0:T(8,128)(2,1)S(1)}, bf16[64,2048]{1,0:T(8,128)(2,1)S(1)}, u32[]{:S(2)}, u32[]{:S(2)}) collective-permute-start(bf16[64,2048]{1,0:T(8,128)(2,1)S(1)} %get-tuple-element.11), channel_id=1, source_target_pairs={{2,0},{3,1},{0,2},{1,3},{6,4},{7,5},{4,6},{5,7},{10,8},{11,9},{8,1... | collective-permute-start | bytes 786440 | tf_op jit(solution)/shard_map/ppermute | solution.py:120
  18.0 2.5 %collective-permute-start.2 = (bf16[64,2048]{1,0:T(8,128)(2,1)S(1)}, bf16[64,2048]{1,0:T(8,128)(2,1)S(1)}, u32[]{:S(2)}, u32[]{:S(2)}) collective-permute-start(bf16[64,2048]{1,0:T(8,128)(2,1)S(1)} %get-tuple-element.11), channel_id=1, source_target_pairs={{3,0},{0,1},{1,2},{2,3},{7,4},{4,5},{5,6},{6,7},{11,8},{8,9},{9,10... | collective-permute-start | bytes 786440 | tf_op jit(solution)/shard_map/ppermute | solution.py:120
  21.9 6.4 %collective-permute-start.4 = (bf16[16,384]{1,0:T(8,128)(2,1)S(1)}, bf16[16,384]{1,0:T(8,128)(2,1)S(1)}, u32[]{:S(2)}, u32[]{:S(2)}) collective-permute-start(bf16[16,384]{1,0:T(8,128)(2,1)S(1)} %pad_maximum_fusion.12), channel_id=1, source_target_pairs={{0,4},{4,0},{1,5},{5,1},{2,6},{6,2},{3,7},{7,3},{8,12},{12,8},{9,1... | collective-permute-start | bytes 36872 | tf_op jit(solution)/shard_map/ppermute | solution.py:68
  28.3 1.9 %collective-permute-start.7 = (f32[2,256]{1,0:T(2,128)}, f32[2,256]{1,0:T(2,128)S(1)}, u32[]{:S(2)}, u32[]{:S(2)}) collective-permute-start(f32[2,256]{1,0:T(2,128)} %param.17), channel_id=1, source_target_pairs={{0,4},{4,0},{1,5},{5,1},{2,6},{6,2},{3,7},{7,3},{8,12},{12,8},{9,1... | collective-permute-start | bytes 6152 | tf_op jit(solution)/shard_map/ppermute | solution.py:68
  33.3 13.6 %all-to-all-start = ((bf16[64,32,384]{2,1,0:T(8,128)(2,1)}), bf16[64,32,384]{2,1,0:T(8,128)(2,1)}, u32[]{:S(2)}, u32[]{:S(2)}) async-start(bf16[64,32,384]{2,1,0:T(8,128)(2,1)} %broadcast_in_dim.22), calls=%async_computation | async-start | bytes 3145728 | tf_op jit(solution)/shard_map/all_to_all | solution.py:30
  47.3 2.7 %collective-permute-start.3 = (bf16[256,2048]{1,0:T(8,128)(2,1)S(1)}, bf16[256,2048]{1,0:T(8,128)(2,1)}, u32[]{:S(2)}, u32[]{:S(2)}) collective-permute-start(bf16[256,2048]{1,0:T(8,128)(2,1)S(1)} %constant_dynamic-slice_fusion.11), channel_id=1, source_target_pairs={{0,4},{4,0},{1,5},{5,1},{2,6},{6,2},{3,7},{7,3},{8,12},{12,8},{9,1... | collective-permute-start | bytes 3145736 | tf_op jit(solution)/shard_map/ppermute | solution.py:68
  57.1 29.7 %all-to-all-done = bf16[64,32,384]{2,1,0:T(8,128)(2,1)} async-done(((bf16[64,32,384]{2,1,0:T(8,128)(2,1)}), bf16[64,32,384]{2,1,0:T(8,128)(2,1)}, u32[]{:S(2)}, u32[]{:S(2)}) %all-to-all-start) | async-done | bytes 1572896 | tf_op jit(solution)/shard_map/all_to_all | solution.py:30
  86.9 2.8 %fusion.15 = bf16[512,384]{0,1:T(8,128)(2,1)S(1)} fusion(bf16[2048,384]{1,0:T(8,128)(2,1)} %bitcast, bf16[256,2048]{1,0:T(8,128)(2,1)} %collective-permute-done.3, bf16[256,2048]{1,0:T(8,128)(2,1)S(1)} %constant_dynamic-slice_fusion.11), kind=kOutput, calls=%fused_computation.14 | convolution fusion | flops 809697280 | bytes 4063232 | tf_op jit(solution)/shard_map/dot_general | solution.py:251
  91.6 1.4 concatenate.72
  93.0 8.5 %all-to-all-start.1 = ((f32[64,3,256]{2,1,0:T(4,128)}), f32[64,3,256]{2,1,0:T(4,128)S(1)}, u32[]{:S(2)}, u32[]{:S(2)}) async-start(f32[64,3,256]{2,1,0:T(4,128)} %concatenate.72), calls=%async_computation.1 | async-start | bytes 524288 | tf_op jit(solution)/shard_map/all_to_all | solution.py:91
  102.4 4.9 %collective-permute-start.9 = (bf16[128,2048]{1,0:T(8,128)(2,1)}, bf16[128,2048]{1,0:T(8,128)(2,1)}, u32[]{:S(2)}, u32[]{:S(2)}) collective-permute-start(bf16[128,2048]{1,0:T(8,128)(2,1)} %constant_dynamic-slice_fusion), channel_id=1, source_target_pairs={{0,4},{4,8},{8,12},{12,16},{16,20},{20,24},{24,28},{28,32},{32,36}... | collective-permute-start | bytes 1572872 | tf_op jit(solution)/shard_map/ppermute | solution.py:25
  107.5 1.9 %collective-permute-start.6 = (bf16[256,128]{1,0:T(8,128)(2,1)S(1)}, bf16[256,128]{1,0:T(8,128)(2,1)S(1)}, u32[]{:S(2)}, u32[]{:S(2)}) collective-permute-start(bf16[256,128]{1,0:T(8,128)(2,1)S(1)} %dynamic-slice_bitcast_fusion), channel_id=1, source_target_pairs={{0,4},{4,0},{1,5},{5,1},{2,6},{6,2},{3,7},{7,3},{8,12},{12,8},{9,1... | collective-permute-start | bytes 196616 | tf_op jit(solution)/shard_map/ppermute | solution.py:68
  110.2 2.4 %collective-permute-start.5 = (bf16[256,256]{1,0:T(8,128)(2,1)S(1)}, bf16[256,256]{1,0:T(8,128)(2,1)S(1)}, u32[]{:S(2)}, u32[]{:S(2)}) collective-permute-start(bf16[256,256]{1,0:T(8,128)(2,1)S(1)} %bitcast.91), channel_id=1, source_target_pairs={{0,4},{4,0},{1,5},{5,1},{2,6},{6,2},{3,7},{7,3},{8,12},{12,8},{9,1... | collective-permute-start | bytes 393224 | tf_op jit(solution)/shard_map/ppermute | solution.py:68
  112.7 4.1 %all-to-all-done.1.parts_ref = f32[64,3,256]{2,1,0:T(4,128)S(1)} async-done(((f32[64,3,256]{2,1,0:T(4,128)}), f32[64,3,256]{2,1,0:T(4,128)S(1)}, u32[]{:S(2)}, u32[]{:S(2)}) %all-to-all-start.1) | async-done | bytes 196640 | tf_op jit(solution)/shard_map/all_to_all | solution.py:91
  117.5 1.7 shard_map.118
  119.2 7.4 %all-to-all-start.2 = ((f32[64,2,256]{2,1,0:T(2,128)}), f32[64,2,256]{2,1,0:T(2,128)S(1)}, u32[]{:S(2)}, u32[]{:S(2)}) async-start(f32[64,2,256]{2,1,0:T(2,128)} %shard_map.118), calls=%async_computation.2 | async-start | bytes 262144 | tf_op jit(solution)/shard_map/all_to_all | solution.py:95
  126.7 12.3 %all-to-all-done.2 = f32[64,2,256]{2,1,0:T(2,128)S(1)} async-done(((f32[64,2,256]{2,1,0:T(2,128)}), f32[64,2,256]{2,1,0:T(2,128)S(1)}, u32[]{:S(2)}, u32[]{:S(2)}) %all-to-all-start.2) | async-done | bytes 131104 | tf_op jit(solution)/shard_map/all_to_all | solution.py:95
  139.4 4.4 %collective-permute-start.8 = (bf16[2,128,256]{1,2,0:T(8,128)(2,1)S(1)}, bf16[2,128,256]{1,2,0:T(8,128)(2,1)S(1)}, u32[]{:S(2)}, u32[]{:S(2)}) collective-permute-start(bf16[2,128,256]{1,2,0:T(8,128)(2,1)S(1)} %bitcast.92), channel_id=1, source_target_pairs={{0,4},{4,0},{1,5},{5,1},{2,6},{6,2},{3,7},{7,3},{8,12},{12,8},{9,1... | collective-permute-start | bytes 393224 | tf_op jit(solution)/shard_map/ppermute | solution.py:68
  144.7 3.3 %fusion.12 = bf16[256,896]{1,0:T(8,128)(2,1)S(1)} fusion(bf16[256,2048]{1,0:T(8,128)(2,1)S(1)} %copy-done.1, bf16[2048,1920]{1,0:T(8,128)(2,1)} %all-gather.2.cloned.1.call-done), kind=kOutput, calls=%fused_computation.13 | convolution fusion | flops 939753472 | bytes 5177344 | tf_op jit(solution)/shard_map/dot_general | solution.py:273
  149.8 1.5 convolution_convert_fusion.1
  154.1 3.5 %fusion.4 = bf16[256,2048]{1,0:T(8,128)(2,1)S(1)} fusion(bf16[2048,1920]{1,0:T(8,128)(2,1)} %all-gather.2.cloned.1.call-done, bf16[256,512]{1,0:T(8,128)(2,1)S(1)} %reshape.431, bf16[256,512]{1,0:T(8,128)(2,1)S(1)} %bitcast.90), kind=kOutput, calls=%fused_computation.4 | convolution fusion | flops 1075314688 | bytes 5767168 | tf_op jit(solution)/shard_map/dot_general | solution.py:288
  157.6 18.0 %all_to_all.20 = bf16[4,64,2048]{2,1,0:T(8,128)(2,1)S(1)} all-to-all(bf16[4,64,2048]{2,1,0:T(8,128)(2,1)S(1)} %bitcast.81), channel_id=1, replica_groups=mesh['sp_0'=8,'sp_1'=8,'sp_2'=2,'tp'=4] {'tp'}, dimensions={0} | all-to-all | bytes 2097152 | tf_op jit(solution)/shard_map/all_to_all | solution.py:42
  (126 shorter events, 22.4 us)
Async XLA Ops:
  6.5 138.1 %all-gather.2.cloned.1.call-start = ((), (), s32[]{:S(2)}) async-start(), calls=%async_computation.4 | async-start | bytes 7925760 | tf_op jit(solution)/shard_map/all_gather | solution.py:242
  10.3 36.6 %collective-permute-start = (bf16[64,2048]{1,0:T(8,128)(2,1)S(1)}, bf16[64,2048]{1,0:T(8,128)(2,1)S(1)}, u32[]{:S(2)}, u32[]{:S(2)}) collective-permute-start(bf16[64,2048]{1,0:T(8,128)(2,1)S(1)} %get-tuple-element.11), channel_id=1, source_target_pairs={{1,0},{2,1},{3,2},{0,3},{5,4},{6,5},{7,6},{4,7},{9,8},{10,9},{11,1... | collective-permute-start | bytes 786440 | tf_op jit(solution)/shard_map/ppermute | solution.py:120
  15.5 31.5 %collective-permute-start.1 = (bf16[64,2048]{1,0:T(8,128)(2,1)S(1)}, bf16[64,2048]{1,0:T(8,128)(2,1)S(1)}, u32[]{:S(2)}, u32[]{:S(2)}) collective-permute-start(bf16[64,2048]{1,0:T(8,128)(2,1)S(1)} %get-tuple-element.11), channel_id=1, source_target_pairs={{2,0},{3,1},{0,2},{1,3},{6,4},{7,5},{4,6},{5,7},{10,8},{11,9},{8,1... | collective-permute-start | bytes 786440 | tf_op jit(solution)/shard_map/ppermute | solution.py:120
  18.0 29.1 %collective-permute-start.2 = (bf16[64,2048]{1,0:T(8,128)(2,1)S(1)}, bf16[64,2048]{1,0:T(8,128)(2,1)S(1)}, u32[]{:S(2)}, u32[]{:S(2)}) collective-permute-start(bf16[64,2048]{1,0:T(8,128)(2,1)S(1)} %get-tuple-element.11), channel_id=1, source_target_pairs={{3,0},{0,1},{1,2},{2,3},{7,4},{4,5},{5,6},{6,7},{11,8},{8,9},{9,10... | collective-permute-start | bytes 786440 | tf_op jit(solution)/shard_map/ppermute | solution.py:120
  21.9 10.1 %collective-permute-start.4 = (bf16[16,384]{1,0:T(8,128)(2,1)S(1)}, bf16[16,384]{1,0:T(8,128)(2,1)S(1)}, u32[]{:S(2)}, u32[]{:S(2)}) collective-permute-start(bf16[16,384]{1,0:T(8,128)(2,1)S(1)} %pad_maximum_fusion.12), channel_id=1, source_target_pairs={{0,4},{4,0},{1,5},{5,1},{2,6},{6,2},{3,7},{7,3},{8,12},{12,8},{9,1... | collective-permute-start | bytes 36872 | tf_op jit(solution)/shard_map/ppermute | solution.py:68
  28.3 23.8 %collective-permute-start.7 = (f32[2,256]{1,0:T(2,128)}, f32[2,256]{1,0:T(2,128)S(1)}, u32[]{:S(2)}, u32[]{:S(2)}) collective-permute-start(f32[2,256]{1,0:T(2,128)} %param.17), channel_id=1, source_target_pairs={{0,4},{4,0},{1,5},{5,1},{2,6},{6,2},{3,7},{7,3},{8,12},{12,8},{9,1... | collective-permute-start | bytes 6152 | tf_op jit(solution)/shard_map/ppermute | solution.py:68
  33.3 53.6 %all-to-all-start = ((bf16[64,32,384]{2,1,0:T(8,128)(2,1)}), bf16[64,32,384]{2,1,0:T(8,128)(2,1)}, u32[]{:S(2)}, u32[]{:S(2)}) async-start(bf16[64,32,384]{2,1,0:T(8,128)(2,1)} %broadcast_in_dim.22), calls=%async_computation | async-start | bytes 3145728 | tf_op jit(solution)/shard_map/all_to_all | solution.py:30
  47.0 5.1 %copy-start.7 = (f32[2,256]{1,0:T(2,128)S(1)}, f32[2,256]{1,0:T(2,128)}, u32[]{:S(2)}) copy-start(f32[2,256]{1,0:T(2,128)} %param.17) | copy-start | bytes 6148
  47.3 39.6 %copy-start = (bf16[256,2048]{1,0:T(8,128)(2,1)}, bf16[256,2048]{1,0:T(8,128)(2,1)S(1)}, u32[]{:S(2)}) copy-start(bf16[256,2048]{1,0:T(8,128)(2,1)S(1)} %constant_dynamic-slice_fusion.11) | copy-start | bytes 3145732
  47.3 9.9 %collective-permute-start.3 = (bf16[256,2048]{1,0:T(8,128)(2,1)S(1)}, bf16[256,2048]{1,0:T(8,128)(2,1)}, u32[]{:S(2)}, u32[]{:S(2)}) collective-permute-start(bf16[256,2048]{1,0:T(8,128)(2,1)S(1)} %constant_dynamic-slice_fusion.11), channel_id=1, source_target_pairs={{0,4},{4,0},{1,5},{5,1},{2,6},{6,2},{3,7},{7,3},{8,12},{12,8},{9,1... | collective-permute-start | bytes 3145736 | tf_op jit(solution)/shard_map/ppermute | solution.py:68
  93.0 23.8 %all-to-all-start.1 = ((f32[64,3,256]{2,1,0:T(4,128)}), f32[64,3,256]{2,1,0:T(4,128)S(1)}, u32[]{:S(2)}, u32[]{:S(2)}) async-start(f32[64,3,256]{2,1,0:T(4,128)} %concatenate.72), calls=%async_computation.1 | async-start | bytes 524288 | tf_op jit(solution)/shard_map/all_to_all | solution.py:91
  102.4 47.4 %collective-permute-start.9 = (bf16[128,2048]{1,0:T(8,128)(2,1)}, bf16[128,2048]{1,0:T(8,128)(2,1)}, u32[]{:S(2)}, u32[]{:S(2)}) collective-permute-start(bf16[128,2048]{1,0:T(8,128)(2,1)} %constant_dynamic-slice_fusion), channel_id=1, source_target_pairs={{0,4},{4,8},{8,12},{12,16},{16,20},{20,24},{24,28},{28,32},{32,36}... | collective-permute-start | bytes 1572872 | tf_op jit(solution)/shard_map/ppermute | solution.py:25
  107.5 19.1 %collective-permute-start.6 = (bf16[256,128]{1,0:T(8,128)(2,1)S(1)}, bf16[256,128]{1,0:T(8,128)(2,1)S(1)}, u32[]{:S(2)}, u32[]{:S(2)}) collective-permute-start(bf16[256,128]{1,0:T(8,128)(2,1)S(1)} %dynamic-slice_bitcast_fusion), channel_id=1, source_target_pairs={{0,4},{4,0},{1,5},{5,1},{2,6},{6,2},{3,7},{7,3},{8,12},{12,8},{9,1... | collective-permute-start | bytes 196616 | tf_op jit(solution)/shard_map/ppermute | solution.py:68
  110.2 33.7 %collective-permute-start.5 = (bf16[256,256]{1,0:T(8,128)(2,1)S(1)}, bf16[256,256]{1,0:T(8,128)(2,1)S(1)}, u32[]{:S(2)}, u32[]{:S(2)}) collective-permute-start(bf16[256,256]{1,0:T(8,128)(2,1)S(1)} %bitcast.91), channel_id=1, source_target_pairs={{0,4},{4,0},{1,5},{5,1},{2,6},{6,2},{3,7},{7,3},{8,12},{12,8},{9,1... | collective-permute-start | bytes 393224 | tf_op jit(solution)/shard_map/ppermute | solution.py:68
  116.8 0.7 copy-start.3
  119.2 19.8 %all-to-all-start.2 = ((f32[64,2,256]{2,1,0:T(2,128)}), f32[64,2,256]{2,1,0:T(2,128)S(1)}, u32[]{:S(2)}, u32[]{:S(2)}) async-start(f32[64,2,256]{2,1,0:T(2,128)} %shard_map.118), calls=%async_computation.2 | async-start | bytes 262144 | tf_op jit(solution)/shard_map/all_to_all | solution.py:95
  126.7 18.0 %copy-start.1 = (bf16[256,2048]{1,0:T(8,128)(2,1)S(1)}, bf16[256,2048]{1,0:T(8,128)(2,1)}, u32[]{:S(2)}) copy-start(bf16[256,2048]{1,0:T(8,128)(2,1)} %copy-done) | copy-start | bytes 3145732
  139.4 5.2 %collective-permute-start.8 = (bf16[2,128,256]{1,2,0:T(8,128)(2,1)S(1)}, bf16[2,128,256]{1,2,0:T(8,128)(2,1)S(1)}, u32[]{:S(2)}, u32[]{:S(2)}) collective-permute-start(bf16[2,128,256]{1,2,0:T(8,128)(2,1)S(1)} %bitcast.92), channel_id=1, source_target_pairs={{0,4},{4,0},{1,5},{5,1},{2,6},{6,2},{3,7},{7,3},{8,12},{12,8},{9,1... | collective-permute-start | bytes 393224 | tf_op jit(solution)/shard_map/ppermute | solution.py:68
  144.6 3.5 %copy-start.4 = (f32[256,64]{0,1:T(8,128)S(1)}, f32[256,64]{0,1:T(8,128)}, u32[]{:S(2)}) copy-start(f32[256,64]{0,1:T(8,128)} %get-tuple-element.41) | copy-start | bytes 196612
  144.6 3.9 %copy-start.5 = (f32[2,2,128]{2,0,1:T(2,128)S(1)}, f32[2,2,128]{2,0,1:T(2,128)}, u32[]{:S(2)}) copy-start(f32[2,2,128]{2,0,1:T(2,128)} %copy.77) | copy-start | bytes 6148
  148.0 1.4 copy-start.2
  148.0 1.0 copy-start.6
  149.4 2.2 %slice-start = ((bf16[256,896]{1,0:T(8,128)(2,1)}), bf16[256,512]{1,0:T(8,128)(2,1)S(1)}, s32[]{:S(2)}) async-start(bf16[256,896]{1,0:T(8,128)(2,1)} %copy-done.2), calls=%async_computation.5 | async-start | bytes 524288 | tf_op jit(solution)/shard_map/split | solution.py:279
  151.3 1.1 copy-start.8
Sparse Core Ops, SparseCore 0:
  10.5 126.4 all-gather.1

commit v4 on v3

--- a/solution.py
+++ b/solution.py
@@ -2,6 +2,7 @@
 import jax.numpy as jnp
 from jax import lax
 from jax.experimental import pallas as pl
+from jax.experimental.pallas import tpu as pltpu
 from jax.sharding import Mesh
 from jax.sharding import PartitionSpec as P
 
@@ -153,66 +154,138 @@
     return keys, values, jnp.stack(before)
 
 
-def retention_path(query_ret, key_ret, value_ret, log_decay, before):
-    tok_count, heads_here = (query_ret.shape[0], query_ret.shape[1])
-    blocks = tok_count // BLOCK
-    q_blocks = query_ret.reshape(blocks, BLOCK, heads_here, RETAIN_KEY_SIZE)
-    k_blocks = key_ret.reshape(heads_here, blocks, BLOCK, RETAIN_KEY_SIZE)
-    v_blocks = value_ret.reshape(heads_here, blocks, BLOCK, V_DIM)
-    running = jnp.cumsum(log_decay.reshape(heads_here, blocks, BLOCK), axis=-1)
+CHUNKS = 4
+
+
+def tail_body(
+    rows_ref, key_ref, value_ref, before_ref, weight_ref, fade_ref, cos_ref, sin_ref, bias_ref,
+    sink_ref, whole_ref, out_ref, win_ref, wout_ref, ret_ref, att_ref, sems,
+):
+    width, in_width = (rows_ref.shape[1], win_ref.shape[1])
+    length = out_ref.shape[0]
+    step = width // CHUNKS
+    copies = [
+        pltpu.make_async_copy(
+            whole_ref.at[pl.ds(k * step, step), pl.ds(0, in_width)],
+            win_ref.at[pl.ds(k * step, step)],
+            sems.at[k],
+        )
+        for k in range(CHUNKS)
+    ]
+    copies.append(
+        pltpu.make_async_copy(
+            whole_ref.at[:, pl.ds(in_width, wout_ref.shape[1])], wout_ref, sems.at[CHUNKS]
+        )
+    )
+    for copy in copies:
+        copy.start()
+    total = None
+    for k in range(CHUNKS):
+        copies[k].wait()
+        part = jnp.dot(
+            rows_ref[:, k * step : (k + 1) * step],
+            win_ref[k * step : (k + 1) * step],
+            preferred_element_type=jnp.float32,
+        )
+        total = part if total is None else total + part
+    projected = total.astype(jnp.bfloat16)
+    heads, blocks = (before_ref.shape[0], before_ref.shape[1])
+    rim = rows_ref.shape[0] - length
+    cosine = cos_ref[...]
+    sine_part = sin_ref[...]
+    contract_last = (((1,), (1,)), ((), ()))
+    for h in range(heads):
+        query = projected[rim:, h * RETAIN_KEY_SIZE : (h + 1) * RETAIN_KEY_SIZE].astype(jnp.float32)
+        turned = pltpu.roll(query, RETAIN_KEY_SIZE // 2, 1)
+        query = (query * cosine + turned * sine_part).astype(jnp.bfloat16)
+        faded = (query.astype(jnp.float32) * fade_ref[h]).astype(jnp.bfloat16)
+        for n in range(blocks):
+            part = slice(n * BLOCK, (n + 1) * BLOCK)
+            scores = lax.dot_general(
+                query[part], key_ref[h, part], contract_last, preferred_element_type=jnp.float32
+            )
+            scores = (scores * weight_ref[h, n]).astype(jnp.bfloat16)
+            mixed = jnp.dot(scores, value_ref[h, part], preferred_element_type=jnp.float32)
+            mixed = mixed + jnp.dot(faded[part], before_ref[h, n], preferred_element_type=jnp.float32)
+            mixed = mixed * lax.rsqrt(jnp.mean(mixed * mixed, axis=-1, keepdims=True) + epsilon)
+            ret_ref[part, h * V_DIM : (h + 1) * V_DIM] = mixed.astype(jnp.bfloat16)
+    first = heads * RETAIN_KEY_SIZE
+    group = sink_ref.shape[0]
+    keys_at = first + group * HEAD_DIM
+    keys = projected[:, keys_at : keys_at + HEAD_DIM]
+    values = projected[:, keys_at + HEAD_DIM : keys_at + 2 * HEAD_DIM]
+    for n in range(length // WINDOW):
+        seen = slice(n * WINDOW, (n + 2) * WINDOW)
+        bias = bias_ref[n]
+        for g in range(0, group, 2):
+            pair = []
+            for k in (g, g + 1):
+                at = first + k * HEAD_DIM
+                query = projected[rim + n * WINDOW : rim + (n + 1) * WINDOW, at : at + HEAD_DIM]
+                scores = lax.dot_general(
+                    query, keys[seen], contract_last, preferred_element_type=jnp.float32
+                )
+                scores = scores * HEAD_DIM ** (-0.5) + bias
+                sink = jnp.full((WINDOW, 1), sink_ref[k], jnp.float32)
+                highest = jnp.maximum(jnp.max(scores, axis=-1, keepdims=True), sink)
+                lifted = jnp.exp(scores - highest)
+                below = jnp.sum(lifted, axis=-1, keepdims=True) + jnp.exp(sink - highest)
+                found = jnp.dot(
+                    lifted.astype(jnp.bfloat16), values[seen], preferred_element_type=jnp.float32
+                )
+                pair.append(found / below)
+            att_ref[n * WINDOW : (n + 1) * WINDOW, g * HEAD_DIM : (g + 2) * HEAD_DIM] = (
+                jnp.concatenate(pair, axis=1).astype(jnp.bfloat16)
+            )
+    copies[CHUNKS].wait()
+    half = ret_ref.shape[1]
+    result = lax.dot_general(
+        ret_ref[...], wout_ref[:, :half], contract_last, preferred_element_type=jnp.float32
+    ) + lax.dot_general(
+        att_ref[...], wout_ref[:, half:], contract_last, preferred_element_type=jnp.float32
+    )
+    out_ref[...] = result.astype(jnp.bfloat16)
+
+
+def tail(rows, keys, values, before, log_decay, sink_logits, whole, anchor, in_width):
+    length = keys.shape[1]
+    heads, blocks = (before.shape[0], before.shape[1])
+    running = jnp.cumsum(log_decay.reshape(heads, blocks, BLOCK), axis=-1)
     within = running[:, :, :, None] - running[:, :, None, :]
     causal_mask = jnp.arange(BLOCK)[:, None] >= jnp.arange(BLOCK)[None, :]
     weighting = jnp.where(causal_mask, jnp.exp(jnp.minimum(within, 0.0)), 0.0)
-    scores = (
-        jnp.einsum("nihd,hnjd->hnij", q_blocks, k_blocks, preferred_element_type=jnp.float32)
-        * weighting
-    )
-    in_block = jnp.einsum(
-        "hnij,hnjv->nihv", scores.astype(jnp.bfloat16), v_blocks, preferred_element_type=jnp.float32
-    )
-    query_fade = (
-        q_blocks.astype(jnp.float32) * jnp.exp(running).transpose(1, 2, 0)[..., None]
-    ).astype(jnp.bfloat16)
-    carried_term = jnp.einsum("nihd,hndv->nihv", query_fade.astype(jnp.float32), before)
-    final_product = in_block + carried_term
-    final_product = final_product * lax.rsqrt(
-        jnp.mean(final_product * final_product, axis=-1, keepdims=True) + epsilon
-    )
-    return final_product.reshape(tok_count, heads_here * V_DIM).astype(jnp.bfloat16)
-
-
-def attention_path(query_att, stacked, sink_logits, anchor):
-    tok_count = query_att.shape[0]
-    kv_here = stacked.shape[1] // (2 * HEAD_DIM)
-    group_size = query_att.shape[1] // (kv_here * HEAD_DIM)
-    blocks = tok_count // WINDOW
-    extended = stacked.reshape(blocks + 1, WINDOW, 2, kv_here, HEAD_DIM)
-    paired = jnp.concatenate([extended[:-1], extended[1:]], axis=1)
-    keys_pair = paired[:, :, 0]
-    values_pair = paired[:, :, 1]
-    q_blocks = query_att.reshape(blocks, WINDOW, kv_here, group_size, HEAD_DIM)
-    scores = jnp.einsum(
-        "nihgd,njhd->nhgij", q_blocks, keys_pair, preferred_element_type=jnp.float32
-    ) * HEAD_DIM ** (-0.5)
-    query_pos = anchor + (jnp.arange(blocks) * WINDOW)[:, None] + jnp.arange(WINDOW)[None, :]
-    key_pos = (
-        anchor + (jnp.arange(blocks) * WINDOW - WINDOW)[:, None] + jnp.arange(2 * WINDOW)[None, :]
-    )
-    allowed = (
-        (key_pos[:, None, :] >= 0)
-        & (key_pos[:, None, :] <= query_pos[:, :, None])
-        & (query_pos[:, :, None] - key_pos[:, None, :] < WINDOW)
-    )
-    scores = jnp.where(allowed[:, None, None], scores, masked_out)
-    sink_logit = sink_logits.reshape(kv_here, group_size)[None, :, :, None]
-    highest = jnp.maximum(jnp.max(scores, axis=-1), sink_logit)
-    lifted = jnp.exp(scores - highest[..., None])
-    denominator = jnp.sum(lifted, axis=-1) + jnp.exp(sink_logit - highest)
-    attn_weights = (lifted / denominator[..., None]).astype(jnp.bfloat16)
-    final_product = jnp.einsum(
-        "nhgij,njhd->nihgd", attn_weights, values_pair, preferred_element_type=jnp.float32
-    )
-    return final_product.reshape(tok_count, kv_here * group_size * HEAD_DIM).astype(jnp.bfloat16)
+    fade = jnp.exp(running).reshape(heads, length, 1)
+    half_dim = RETAIN_KEY_SIZE // 2
+    inverse = rope_base ** (-jnp.arange(half_dim, dtype=jnp.float32) / half_dim)
+    positions = anchor + jnp.arange(length, dtype=jnp.int32)
+    angles = positions.astype(jnp.float32)[:, None] * inverse[None, :]
+    cosine = jnp.concatenate([jnp.cos(angles)] * 2, axis=1)
+    sine_part = jnp.concatenate([-jnp.sin(angles), jnp.sin(angles)], axis=1)
+    starts = jnp.arange(length // WINDOW)[:, None, None] * WINDOW
+    ahead = jnp.arange(2 * WINDOW)[None, None, :] - jnp.arange(WINDOW)[None, :, None]
+    there = anchor + starts - WINDOW + jnp.arange(2 * WINDOW)[None, None, :] >= 0
+    bias = jnp.where((ahead > 0) & (ahead <= WINDOW) & there, 0.0, masked_out)
+    out_width = whole.shape[1] - in_width
+    features = rows.shape[1]
+    columns = whole.shape[0]
+    vmem = pl.BlockSpec(memory_space=pltpu.VMEM)
+    return pl.pallas_call(
+        tail_body,
+        out_shape=jax.ShapeDtypeStruct((length, columns), jnp.bfloat16),
+        in_specs=[vmem] * 9
+        + [pl.BlockSpec(memory_space=pltpu.SMEM), pl.BlockSpec(memory_space=pltpu.HBM)],
+        out_specs=vmem,
+        scratch_shapes=[
+            pltpu.VMEM((features, in_width), jnp.bfloat16),
+            pltpu.VMEM((columns, out_width), jnp.bfloat16),
+            pltpu.VMEM((length, heads * V_DIM), jnp.bfloat16),
+            pltpu.VMEM((length, sink_logits.shape[0] * HEAD_DIM), jnp.bfloat16),
+            pltpu.SemaphoreType.DMA((CHUNKS + 1,)),
+        ],
+        compiler_params=pltpu.CompilerParams(vmem_limit_bytes=40 * 1024 * 1024),
+        name="tail",
+    )(rows, keys, values, before, weighting, fade, cosine, sine_part, bias, sink_logits,
+      pltpu.with_memory_space_constraint(whole, pltpu.HBM))
 
 
 def on_device(
@@ -238,7 +311,6 @@
     ).astype(jnp.bfloat16)
     weights = (ret_query, att_query, att_key, att_value)
     widths = [weight.shape[1] for weight in weights]
-    points = [sum(widths[:index]) for index in range(1, len(widths))]
     whole = lax.all_gather(
         jnp.concatenate([*weights, ret_out.T, att_out.T], axis=1), SP, axis=0, tiled=True
     )
@@ -270,28 +342,18 @@
     before = heads_of_own_rows(before)
 
     input_width = sum(widths)
-    projected = jnp.dot(
-        own_rows, whole[:, :input_width], preferred_element_type=jnp.float32
-    ).astype(jnp.bfloat16)
-    rim_kv = jnp.dot(
-        rim, whole[:, points[1] : input_width], preferred_element_type=jnp.float32
-    ).astype(jnp.bfloat16)
-    sections = jnp.split(projected, points, axis=1)
-    stacked = jnp.concatenate([rim_kv, projected[:, points[1] :]], axis=0)
-    positions = anchor + jnp.arange(tok_count, dtype=jnp.int32)
-    query_ret = rotate(sections[0].reshape(tok_count, -1, RETAIN_KEY_SIZE), positions).astype(
-        jnp.bfloat16
-    )
-    ret_mix = retention_path(query_ret, key_ret, value_ret, log_decay, before)
-    att_mix = attention_path(sections[1], stacked, sink_logits, anchor)
-    mixes = jnp.concatenate([ret_mix, att_mix], axis=1)
-    partial = lax.dot_general(
-        mixes,
-        whole[:, input_width:],
-        (((1,), (1,)), ((), ())),
-        preferred_element_type=jnp.float32,
-    )
-    mixed = sent_and_summed(partial.astype(jnp.bfloat16), "tp", 0)
+    partial = tail(
+        jnp.concatenate([rim, own_rows], axis=0),
+        key_ret,
+        value_ret,
+        before.astype(jnp.bfloat16),
+        log_decay,
+        sink_logits,
+        whole,
+        anchor,
+        input_width,
+    )
+    mixed = sent_and_summed(partial, "tp", 0)
     return mixed.astype(jnp.bfloat16)
 
 

time: 184 us -> 180 us (0.978)
  matrix products: 13.7 us -> 2.96 us
  waiting for transfers between devices: 46.8 us -> 37.8 us
  Pallas kernels: 1.75 us -> 8.56 us
  local copies, waits for them, and re-layouts: 13.6 us -> 18.3 us
  other arithmetic: 8.32 us -> 12.6 us
    dot_general x7 -> x0, matrix products: 10.1 us -> none  [the longest x1 3.48 us: on_device(): lax.dot_general(mixes, whole[:, input_width:], (((1,), (1,)), ((), ())),...]
    all_to_all x1, waiting for transfers between devices: 29.7 us -> 21.2 us  [from_everyone(): lax.all_to_all(jnp.broadcast_to(value[None], (size, *value.shape)), axis,...]
    pallas_call x0 -> x1, Pallas kernels: none -> 6.81 us  [tail(): pl.pallas_call(tail_body, out_shape=jax.ShapeDtypeStruct((length, columns...]
    ppermute x6, starting transfers between devices: 19.7 us -> 22.3 us  [core_swap(): return lax.ppermute(value, CORE, [(0, 1), (1, 0)])]
    unnamed x26 -> x11, local copies, waits for them, and re-layouts: 1.14 us -> 3.67 us
    ppermute x1, starting transfers between devices: 4.92 us -> 3.02 us  [shifted(): lax.ppermute(value, axis, [(source, source + steps) for source in range(i...]
  transfers between devices with their start and end apart: 14 -> 14, of which waited for: 4 -> 3; matrix products, arithmetic and copies ran while one was open for 14% -> 18% of each run, Pallas kernels for 1% -> 1%
where the time goes in v4:
time: 180 us; the launch traced here: 179 us
  starting transfers between devices  64.3 us (36%)
  waiting for transfers between devices  37.8 us (21%)
  local copies, waits for them, and re-layouts  18.3 us (10%)
  blocking collectives  18.1 us (10%)
  between operations  16.6 us (9%)
  other arithmetic  12.6 us (7%)
  Pallas kernels  8.56 us (5%)
  matrix products  2.96 us (2%)
    ppermute x6, starting transfers between devices, core_swap(): return lax.ppermute(value, CORE, [(0, 1), (1, 0)])  22.3 us
    all_to_all x1, waiting for transfers between devices, from_everyone(): lax.all_to_all(jnp.broadcast_to(value[None], (size, *value.shape)), axis,...  21.2 us
    all_to_all x1, blocking collectives, sent_and_summed(): lax.all_to_all(tiles, axis, split_axis=0, concat_axis=0, tiled=True)  18.1 us
    all_to_all x1, starting transfers between devices, from_everyone(): lax.all_to_all(jnp.broadcast_to(value[None], (size, *value.shape)), axis,...  13.7 us
    all_to_all x1, waiting for transfers between devices, state_before(): lax.all_to_all(prefix, ZY, 0, 0, tiled=True).reshape(RETAIN_KEY_SIZE, V_DIM)  10.7 us
    ppermute x3, starting transfers between devices, gathered_rows(): lax.ppermute(value, axis, [((k + step) % size, k) for k in range(size)])  10.1 us
    all_to_all x1, starting transfers between devices, state_before(): arrived = lax.all_to_all(sent, ZY, 0, 0, tiled=True)  8.24 us
    all_to_all x1, starting transfers between devices, state_before(): lax.all_to_all(prefix, ZY, 0, 0, tiled=True).reshape(RETAIN_KEY_SIZE, V_DIM)  6.9 us
  transfers between devices with their start and end apart: 14, of which 3 were waited for; matrix products, arithmetic and copies ran while one was open for 18% of the time, Pallas kernels for 1%

profile of v4, /device:TPU:1, one launch (start us, length us, event | category | flops | bytes accessed | tf_op | source)
XLA Modules:
  0.0 179.2 jit_solution(9255767619338935785)
XLA Ops:
  6.5 1.5 concatenate.65
  9.2 1.9 %constant_dynamic-update-slice_fusion.6 = (bf16[448,2048]{1,0:T(8,128)(2,1)}, bf16[64,2048]{1,0:T(8,128)(2,1)S(1)}) fusion(f32[2048]{0:T(1024)} %param.13, f32[64]{0:T(128)S(1)} %add_rsqrt_fusion, bf16[64,2048]{1,0:T(8,128)(2,1)} %param.12), kind=kLoop, calls=%fused_computation.67 | loop fusion | flops 524287 | bytes 794880
  11.0 5.2 %collective-permute-start = (bf16[64,2048]{1,0:T(8,128)(2,1)S(1)}, bf16[64,2048]{1,0:T(8,128)(2,1)S(1)}, u32[]{:S(2)}, u32[]{:S(2)}) collective-permute-start(bf16[64,2048]{1,0:T(8,128)(2,1)S(1)} %get-tuple-element.11), channel_id=1, source_target_pairs={{1,0},{2,1},{3,2},{0,3},{5,4},{6,5},{7,6},{4,7},{9,8},{10,9},{11,1... | collective-permute-start | bytes 786440 | tf_op jit(solution)/shard_map/ppermute | solution.py:121
  16.2 2.4 %collective-permute-start.1 = (bf16[64,2048]{1,0:T(8,128)(2,1)S(1)}, bf16[64,2048]{1,0:T(8,128)(2,1)S(1)}, u32[]{:S(2)}, u32[]{:S(2)}) collective-permute-start(bf16[64,2048]{1,0:T(8,128)(2,1)S(1)} %get-tuple-element.11), channel_id=1, source_target_pairs={{2,0},{3,1},{0,2},{1,3},{6,4},{7,5},{4,6},{5,7},{10,8},{11,9},{8,1... | collective-permute-start | bytes 786440 | tf_op jit(solution)/shard_map/ppermute | solution.py:121
  18.7 2.5 %collective-permute-start.2 = (bf16[64,2048]{1,0:T(8,128)(2,1)S(1)}, bf16[64,2048]{1,0:T(8,128)(2,1)S(1)}, u32[]{:S(2)}, u32[]{:S(2)}) collective-permute-start(bf16[64,2048]{1,0:T(8,128)(2,1)S(1)} %get-tuple-element.11), channel_id=1, source_target_pairs={{3,0},{0,1},{1,2},{2,3},{7,4},{4,5},{5,6},{6,7},{11,8},{8,9},{9,10... | collective-permute-start | bytes 786440 | tf_op jit(solution)/shard_map/ppermute | solution.py:121
  22.6 6.4 %collective-permute-start.5 = (bf16[16,384]{1,0:T(8,128)(2,1)S(1)}, bf16[16,384]{1,0:T(8,128)(2,1)S(1)}, u32[]{:S(2)}, u32[]{:S(2)}) collective-permute-start(bf16[16,384]{1,0:T(8,128)(2,1)S(1)} %pad_maximum_fusion.10), channel_id=1, source_target_pairs={{0,4},{4,0},{1,5},{5,1},{2,6},{6,2},{3,7},{7,3},{8,12},{12,8},{9,1... | collective-permute-start | bytes 36872 | tf_op jit(solution)/shard_map/ppermute | solution.py:69
  29.0 1.9 %collective-permute-start.8 = (f32[2,256]{1,0:T(2,128)}, f32[2,256]{1,0:T(2,128)S(1)}, u32[]{:S(2)}, u32[]{:S(2)}) collective-permute-start(f32[2,256]{1,0:T(2,128)} %param.17), channel_id=1, source_target_pairs={{0,4},{4,0},{1,5},{5,1},{2,6},{6,2},{3,7},{7,3},{8,12},{12,8},{9,1... | collective-permute-start | bytes 6152 | tf_op jit(solution)/shard_map/ppermute | solution.py:69
  33.1 13.7 %all-to-all-start = ((bf16[64,32,384]{2,1,0:T(8,128)(2,1)}), bf16[64,32,384]{2,1,0:T(8,128)(2,1)}, u32[]{:S(2)}, u32[]{:S(2)}) async-start(bf16[64,32,384]{2,1,0:T(8,128)(2,1)} %broadcast_in_dim.20), calls=%async_computation | async-start | bytes 3145728 | tf_op jit(solution)/shard_map/all_to_all | solution.py:31
  53.3 2.7 %collective-permute-start.4 = (bf16[256,2048]{1,0:T(8,128)(2,1)S(1)}, bf16[256,2048]{1,0:T(8,128)(2,1)}, u32[]{:S(2)}, u32[]{:S(2)}) collective-permute-start(bf16[256,2048]{1,0:T(8,128)(2,1)S(1)} %constant_dynamic-slice_fusion.7), channel_id=1, source_target_pairs={{0,4},{4,0},{1,5},{5,1},{2,6},{6,2},{3,7},{7,3},{8,12},{12,8},{9,1... | collective-permute-start | bytes 3145736 | tf_op jit(solution)/shard_map/ppermute | solution.py:69
  60.9 1.9 %constant_dynamic-slice_fusion = bf16[128,2048]{1,0:T(8,128)(2,1)} fusion(bf16[448,2048]{1,0:T(8,128)(2,1)} %constant_dynamic-update-slice_fusion, s32[]{:T(128)S(6)} %add.179), kind=kLoop, calls=%fused_computation.72 | loop fusion | bytes 1048580 | tf_op jit(solution)/shard_map/slice | solution.py:321
  62.8 3.0 %collective-permute-start.3 = (bf16[128,2048]{1,0:T(8,128)(2,1)}, bf16[128,2048]{1,0:T(8,128)(2,1)}, u32[]{:S(2)}, u32[]{:S(2)}) collective-permute-start(bf16[128,2048]{1,0:T(8,128)(2,1)} %constant_dynamic-slice_fusion), channel_id=1, source_target_pairs={{0,4},{4,8},{8,12},{12,16},{16,20},{20,24},{24,28},{28,32},{32,36}... | collective-permute-start | bytes 1572872 | tf_op jit(solution)/shard_map/ppermute | solution.py:26
  65.8 21.2 %all-to-all-done = bf16[64,32,384]{2,1,0:T(8,128)(2,1)} async-done(((bf16[64,32,384]{2,1,0:T(8,128)(2,1)}), bf16[64,32,384]{2,1,0:T(8,128)(2,1)}, u32[]{:S(2)}, u32[]{:S(2)}) %all-to-all-start) | async-done | bytes 1572896 | tf_op jit(solution)/shard_map/all_to_all | solution.py:31
  87.1 2.8 %fusion.4 = bf16[512,384]{0,1:T(8,128)(2,1)S(1)} fusion(bf16[2048,384]{1,0:T(8,128)(2,1)} %bitcast, bf16[256,2048]{1,0:T(8,128)(2,1)} %collective-permute-done.4, bf16[256,2048]{1,0:T(8,128)(2,1)S(1)} %constant_dynamic-slice_fusion.7), kind=kOutput, calls=%fused_computation.5 | convolution fusion | flops 809697280 | bytes 4063232 | tf_op jit(solution)/shard_map/dot_general | solution.py:323
  92.5 8.2 %all-to-all-start.1 = ((f32[64,3,256]{2,1,0:T(4,128)}), f32[64,3,256]{2,1,0:T(4,128)}, u32[]{:S(2)}, u32[]{:S(2)}) async-start(f32[64,3,256]{2,1,0:T(4,128)} %concatenate.61), calls=%async_computation.1 | async-start | bytes 524288 | tf_op jit(solution)/shard_map/all_to_all | solution.py:92
  103.8 3.8 %collective-permute-start.6 = (bf16[256,128]{1,0:T(8,128)(2,1)S(1)}, bf16[256,128]{1,0:T(8,128)(2,1)S(1)}, u32[]{:S(2)}, u32[]{:S(2)}) collective-permute-start(bf16[256,128]{1,0:T(8,128)(2,1)S(1)} %dynamic-slice_bitcast_fusion.2), channel_id=1, source_target_pairs={{0,4},{4,0},{1,5},{5,1},{2,6},{6,2},{3,7},{7,3},{8,12},{12,8},{9,1... | collective-permute-start | bytes 196616 | tf_op jit(solution)/shard_map/ppermute | solution.py:69
  108.2 1.9 %collective-permute-start.7 = (bf16[256,256]{1,0:T(8,128)(2,1)}, bf16[256,256]{1,0:T(8,128)(2,1)}, u32[]{:S(2)}, u32[]{:S(2)}) collective-permute-start(bf16[256,256]{1,0:T(8,128)(2,1)} %dynamic-slice_bitcast_fusion.1), channel_id=1, source_target_pairs={{0,4},{4,0},{1,5},{5,1},{2,6},{6,2},{3,7},{7,3},{8,12},{12,8},{9,1... | collective-permute-start | bytes 393224 | tf_op jit(solution)/shard_map/ppermute | solution.py:69
  110.2 5.8 %all-to-all-done.1.parts_ref = f32[64,3,256]{2,1,0:T(4,128)} async-done(((f32[64,3,256]{2,1,0:T(4,128)}), f32[64,3,256]{2,1,0:T(4,128)}, u32[]{:S(2)}, u32[]{:S(2)}) %all-to-all-start.1) | async-done | bytes 196640 | tf_op jit(solution)/shard_map/all_to_all | solution.py:92
  115.9 1.7 shard_map.118
  117.7 6.9 %all-to-all-start.2 = ((f32[64,2,256]{2,1,0:T(2,128)}), f32[64,2,256]{2,1,0:T(2,128)}, u32[]{:S(2)}, u32[]{:S(2)}) async-start(f32[64,2,256]{2,1,0:T(2,128)} %shard_map.118), calls=%async_computation.2 | async-start | bytes 262144 | tf_op jit(solution)/shard_map/all_to_all | solution.py:96
  125.5 10.7 %all-to-all-done.2 = f32[64,2,256]{2,1,0:T(2,128)} async-done(((f32[64,2,256]{2,1,0:T(2,128)}), f32[64,2,256]{2,1,0:T(2,128)}, u32[]{:S(2)}, u32[]{:S(2)}) %all-to-all-start.2) | async-done | bytes 131104 | tf_op jit(solution)/shard_map/all_to_all | solution.py:96
  136.2 1.6 stack_reshape.3
  139.8 5.6 %collective-permute-start.9 = (bf16[2,128,256]{2,1,0:T(8,128)(2,1)S(1)}, bf16[2,128,256]{2,1,0:T(8,128)(2,1)S(1)}, u32[]{:S(2)}, u32[]{:S(2)}) collective-permute-start(bf16[2,128,256]{2,1,0:T(8,128)(2,1)S(1)} %dynamic-slice_bitcast_fusion), channel_id=1, source_target_pairs={{0,4},{4,0},{1,5},{5,1},{2,6},{6,2},{3,7},{7,3},{8,12},{12,8},{9,1... | collective-permute-start | bytes 393224 | tf_op jit(solution)/shard_map/ppermute | solution.py:69
  146.5 6.8 %tail.1 = bf16[256,2048]{1,0:T(8,128)(2,1)S(1)} custom-call(bf16[384,2048]{1,0:T(8,128)(2,1)S(1)} %pad_maximum_fusion.rows_ref, bf16[2,256,128]{2,1,0:T(8,128)(2,1)S(1)} %pad_maximum_fusion.5.key_ref, bf16[2,256,256]{2,1,0:T(8,128)(2,1)S(1)} %pad_maximum_fusion.3.value_ref, bf16[2,2,128,256]{3,2,1,0:T(8,128)(2,1)S(1)} %pad_maximum_fusion.4.before_ref, ...), custom_call_target="tpu_custom_call" | custom-call | tf_op jit(solution)/shard_map/tail/pallas_call | solution.py:272
  153.4 18.1 %all_to_all.20 = bf16[4,64,2048]{2,1,0:T(8,128)(2,1)S(1)} all-to-all(bf16[4,64,2048]{2,1,0:T(8,128)(2,1)S(1)} %bitcast.39), channel_id=1, replica_groups=mesh['sp_0'=8,'sp_1'=8,'sp_2'=2,'tp'=4] {'tp'}, dimensions={0} | all-to-all | bytes 2097152 | tf_op jit(solution)/shard_map/all_to_all | solution.py:43
  (80 shorter events, 24.2 us)
Async XLA Ops:
  6.5 140.0 %all-gather.2.cloned.1.call-start = ((), (), s32[]{:S(2)}) async-start(), calls=%async_computation.4 | async-start | bytes 7925760 | tf_op jit(solution)/shard_map/all_gather | solution.py:314
  11.0 36.6 %collective-permute-start = (bf16[64,2048]{1,0:T(8,128)(2,1)S(1)}, bf16[64,2048]{1,0:T(8,128)(2,1)S(1)}, u32[]{:S(2)}, u32[]{:S(2)}) collective-permute-start(bf16[64,2048]{1,0:T(8,128)(2,1)S(1)} %get-tuple-element.11), channel_id=1, source_target_pairs={{1,0},{2,1},{3,2},{0,3},{5,4},{6,5},{7,6},{4,7},{9,8},{10,9},{11,1... | collective-permute-start | bytes 786440 | tf_op jit(solution)/shard_map/ppermute | solution.py:121
  16.2 32.2 %collective-permute-start.1 = (bf16[64,2048]{1,0:T(8,128)(2,1)S(1)}, bf16[64,2048]{1,0:T(8,128)(2,1)S(1)}, u32[]{:S(2)}, u32[]{:S(2)}) collective-permute-start(bf16[64,2048]{1,0:T(8,128)(2,1)S(1)} %get-tuple-element.11), channel_id=1, source_target_pairs={{2,0},{3,1},{0,2},{1,3},{6,4},{7,5},{4,6},{5,7},{10,8},{11,9},{8,1... | collective-permute-start | bytes 786440 | tf_op jit(solution)/shard_map/ppermute | solution.py:121
  18.7 30.5 %collective-permute-start.2 = (bf16[64,2048]{1,0:T(8,128)(2,1)S(1)}, bf16[64,2048]{1,0:T(8,128)(2,1)S(1)}, u32[]{:S(2)}, u32[]{:S(2)}) collective-permute-start(bf16[64,2048]{1,0:T(8,128)(2,1)S(1)} %get-tuple-element.11), channel_id=1, source_target_pairs={{3,0},{0,1},{1,2},{2,3},{7,4},{4,5},{5,6},{6,7},{11,8},{8,9},{9,10... | collective-permute-start | bytes 786440 | tf_op jit(solution)/shard_map/ppermute | solution.py:121
  22.6 9.1 %collective-permute-start.5 = (bf16[16,384]{1,0:T(8,128)(2,1)S(1)}, bf16[16,384]{1,0:T(8,128)(2,1)S(1)}, u32[]{:S(2)}, u32[]{:S(2)}) collective-permute-start(bf16[16,384]{1,0:T(8,128)(2,1)S(1)} %pad_maximum_fusion.10), channel_id=1, source_target_pairs={{0,4},{4,0},{1,5},{5,1},{2,6},{6,2},{3,7},{7,3},{8,12},{12,8},{9,1... | collective-permute-start | bytes 36872 | tf_op jit(solution)/shard_map/ppermute | solution.py:69
  29.0 27.4 %collective-permute-start.8 = (f32[2,256]{1,0:T(2,128)}, f32[2,256]{1,0:T(2,128)S(1)}, u32[]{:S(2)}, u32[]{:S(2)}) collective-permute-start(f32[2,256]{1,0:T(2,128)} %param.17), channel_id=1, source_target_pairs={{0,4},{4,0},{1,5},{5,1},{2,6},{6,2},{3,7},{7,3},{8,12},{12,8},{9,1... | collective-permute-start | bytes 6152 | tf_op jit(solution)/shard_map/ppermute | solution.py:69
  33.1 13.8 %copy-start.2 = (f32[2,256]{1,0:T(2,128)S(1)}, f32[2,256]{1,0:T(2,128)}, u32[]{:S(2)}) copy-start(f32[2,256]{1,0:T(2,128)} %param.17) | copy-start | bytes 6148
  33.1 54.0 %all-to-all-start = ((bf16[64,32,384]{2,1,0:T(8,128)(2,1)}), bf16[64,32,384]{2,1,0:T(8,128)(2,1)}, u32[]{:S(2)}, u32[]{:S(2)}) async-start(bf16[64,32,384]{2,1,0:T(8,128)(2,1)} %broadcast_in_dim.20), calls=%async_computation | async-start | bytes 3145728 | tf_op jit(solution)/shard_map/all_to_all | solution.py:31
  53.3 36.5 %copy-start.1 = (bf16[256,2048]{1,0:T(8,128)(2,1)}, bf16[256,2048]{1,0:T(8,128)(2,1)S(1)}, u32[]{:S(2)}) copy-start(bf16[256,2048]{1,0:T(8,128)(2,1)S(1)} %constant_dynamic-slice_fusion.7) | copy-start | bytes 3145732
  53.3 12.5 %collective-permute-start.4 = (bf16[256,2048]{1,0:T(8,128)(2,1)S(1)}, bf16[256,2048]{1,0:T(8,128)(2,1)}, u32[]{:S(2)}, u32[]{:S(2)}) collective-permute-start(bf16[256,2048]{1,0:T(8,128)(2,1)S(1)} %constant_dynamic-slice_fusion.7), channel_id=1, source_target_pairs={{0,4},{4,0},{1,5},{5,1},{2,6},{6,2},{3,7},{7,3},{8,12},{12,8},{9,1... | collective-permute-start | bytes 3145736 | tf_op jit(solution)/shard_map/ppermute | solution.py:69
  62.8 37.9 %collective-permute-start.3 = (bf16[128,2048]{1,0:T(8,128)(2,1)}, bf16[128,2048]{1,0:T(8,128)(2,1)}, u32[]{:S(2)}, u32[]{:S(2)}) collective-permute-start(bf16[128,2048]{1,0:T(8,128)(2,1)} %constant_dynamic-slice_fusion), channel_id=1, source_target_pairs={{0,4},{4,8},{8,12},{12,16},{16,20},{20,24},{24,28},{28,32},{32,36}... | collective-permute-start | bytes 1572872 | tf_op jit(solution)/shard_map/ppermute | solution.py:26
  92.5 23.5 %all-to-all-start.1 = ((f32[64,3,256]{2,1,0:T(4,128)}), f32[64,3,256]{2,1,0:T(4,128)}, u32[]{:S(2)}, u32[]{:S(2)}) async-start(f32[64,3,256]{2,1,0:T(4,128)} %concatenate.61), calls=%async_computation.1 | async-start | bytes 524288 | tf_op jit(solution)/shard_map/all_to_all | solution.py:92
  103.8 20.8 %collective-permute-start.6 = (bf16[256,128]{1,0:T(8,128)(2,1)S(1)}, bf16[256,128]{1,0:T(8,128)(2,1)S(1)}, u32[]{:S(2)}, u32[]{:S(2)}) collective-permute-start(bf16[256,128]{1,0:T(8,128)(2,1)S(1)} %dynamic-slice_bitcast_fusion.2), channel_id=1, source_target_pairs={{0,4},{4,0},{1,5},{5,1},{2,6},{6,2},{3,7},{7,3},{8,12},{12,8},{9,1... | collective-permute-start | bytes 196616 | tf_op jit(solution)/shard_map/ppermute | solution.py:69
  108.2 37.2 %collective-permute-start.7 = (bf16[256,256]{1,0:T(8,128)(2,1)}, bf16[256,256]{1,0:T(8,128)(2,1)}, u32[]{:S(2)}, u32[]{:S(2)}) collective-permute-start(bf16[256,256]{1,0:T(8,128)(2,1)} %dynamic-slice_bitcast_fusion.1), channel_id=1, source_target_pairs={{0,4},{4,0},{1,5},{5,1},{2,6},{6,2},{3,7},{7,3},{8,12},{12,8},{9,1... | collective-permute-start | bytes 393224 | tf_op jit(solution)/shard_map/ppermute | solution.py:69
  117.7 18.5 %all-to-all-start.2 = ((f32[64,2,256]{2,1,0:T(2,128)}), f32[64,2,256]{2,1,0:T(2,128)}, u32[]{:S(2)}, u32[]{:S(2)}) async-start(f32[64,2,256]{2,1,0:T(2,128)} %shard_map.118), calls=%async_computation.2 | async-start | bytes 262144 | tf_op jit(solution)/shard_map/all_to_all | solution.py:96
  137.9 8.7 %copy-start = (f32[8]{0:T(128)S(1)}, f32[8]{0:T(128)}, u32[]{:S(2)}) copy-start(f32[8]{0:T(128)} %sink_ref.1) | copy-start | bytes 100
  139.8 6.6 %collective-permute-start.9 = (bf16[2,128,256]{2,1,0:T(8,128)(2,1)S(1)}, bf16[2,128,256]{2,1,0:T(8,128)(2,1)S(1)}, u32[]{:S(2)}, u32[]{:S(2)}) collective-permute-start(bf16[2,128,256]{2,1,0:T(8,128)(2,1)S(1)} %dynamic-slice_bitcast_fusion), channel_id=1, source_target_pairs={{0,4},{4,0},{1,5},{5,1},{2,6},{6,2},{3,7},{7,3},{8,12},{12,8},{9,1... | collective-permute-start | bytes 393224 | tf_op jit(solution)/shard_map/ppermute | solution.py:69
Sparse Core Ops, SparseCore 0:
  10.5 125.3 all-gather.1

commit v5 on v4

--- a/solution.py
+++ b/solution.py
@@ -33,15 +33,36 @@
     )
 
 
-def cut_along(value, dim, size):
-    before, after = (value.shape[:dim], value.shape[dim + 1 :])
-    return jnp.moveaxis(value.reshape(*before, size, -1, *after), dim, 0)
-
-
-def sent_and_summed(value, axis, dim):
-    tiles = cut_along(value, dim, lax.axis_size(axis))
-    arrived = lax.all_to_all(tiles, axis, split_axis=0, concat_axis=0, tiled=True)
-    return arrived.astype(jnp.float32).sum(axis=0)
+def moved(value, axis, step):
+    size = lax.axis_size(axis)
+    return lax.ppermute(value, axis, [(k, (k + step) % size) for k in range(size)])
+
+
+def added(first, second):
+    return (first.astype(jnp.float32) + second.astype(jnp.float32)).astype(jnp.bfloat16)
+
+
+def summed_over_four(value, axis):
+    size = lax.axis_size(axis)
+    here = lax.axis_index(axis)
+    tiles = value.reshape(size, -1, value.shape[-1])
+    half = tiles.shape[1] // 2
+
+    def for_device(step):
+        return lax.dynamic_index_in_dim(tiles, (here + step) % size, 0, keepdims=False)
+
+    far = for_device(2)
+    from_below = moved(far[half:], axis, 1)
+    from_above = moved(far[:half], axis, -1)
+    up = for_device(1)
+    down = for_device(3)
+    up = jnp.concatenate([up[:half], added(up[half:], from_below)], axis=0)
+    down = jnp.concatenate([added(down[:half], from_above), down[half:]], axis=0)
+    return (
+        for_device(0).astype(jnp.float32)
+        + moved(up, axis, 1).astype(jnp.float32)
+        + moved(down, axis, -1).astype(jnp.float32)
+    )
 
 
 def rotate(values, positions):
@@ -111,19 +132,46 @@
     mine = columns_of_head(ret_key, ret_value, core)
     theirs = core_swap(columns_of_head(ret_key, ret_value, 1 - core))
     block = in_core_order(mine, theirs, 0)
-    arrived = from_everyone(block, ZY)
-    return arrived.reshape(-1, block.shape[-1])
+    arrived = from_everyone(block, "sp_1")
+    part = arrived.reshape(-1, block.shape[-1])
+    return ring_gathered(part, "sp_0")
+
+
+def ring_gathered(part, axis):
+    size = lax.axis_size(axis)
+    here = lax.axis_index(axis)
+    rows = part.shape[0]
+    whole = jnp.zeros((size * rows, part.shape[1]), part.dtype)
+
+    def put(whole, value, owner, offset=0):
+        return lax.dynamic_update_slice_in_dim(whole, value, owner % size * rows + offset, 0)
+
+    whole = put(whole, part, here)
+    up = down = part
+    for step in range(1, size // 2):
+        up = moved(up, axis, 1)
+        down = moved(down, axis, -1)
+        whole = put(whole, up, here - step + size)
+        whole = put(whole, down, here + step)
+    half = rows // 2
+    up = moved(up[:half], axis, 1)
+    down = moved(down[half:], axis, -1)
+    whole = put(whole, up, here + size // 2)
+    return put(whole, down, here + size // 2, half)
 
 
 def gathered_rows(value, axis):
     size = lax.axis_size(axis)
-    pieces = [value] + [
-        lax.ppermute(value, axis, [((k + step) % size, k) for k in range(size)])
-        for step in range(1, size)
-    ]
-    turned = jnp.concatenate(pieces + pieces[:-1], axis=0)
-    start = (size - lax.axis_index(axis)) % size * value.shape[0]
-    return lax.dynamic_slice_in_dim(turned, start, size * value.shape[0], 0)
+    here = lax.axis_index(axis)
+    rows = value.shape[0]
+    whole = jnp.zeros((size * rows, value.shape[1]), value.dtype)
+    whole = lax.dynamic_update_slice_in_dim(whole, value, here * rows, 0)
+    for step in range(1, size):
+        piece = moved(value, axis, step)
+        whole = lax.dynamic_update_slice_in_dim(
+            whole, piece, (here - step + size) % size * rows, 0
+        )
+    return whole
 
 
 def chain_of_head(kv, log_decay, anchor):
@@ -353,7 +401,7 @@
         anchor,
         input_width,
     )
-    mixed = sent_and_summed(partial, "tp", 0)
+    mixed = summed_over_four(partial, "tp")
     return mixed.astype(jnp.bfloat16)
 
 

time: 180 us -> 209 us (1.16); the launches traced: 179 us -> 206 us
  starting transfers between devices: 64.3 us -> 111 us
  blocking collectives: 18.1 us -> 0 us
  local copies, waits for them, and re-layouts: 18.3 us -> 13.6 us
  waiting for transfers between devices: 37.8 us -> 42.4 us
    ppermute x3 -> x15, starting transfers between devices: 10.1 us -> 63.6 us  [moved(): lax.ppermute(value, axis, [(k, (k + step) % size) for k in range(size)])]
    ppermute x3 -> x15, waiting for transfers between devices: 0.01 us -> 22.9 us  [moved(): lax.ppermute(value, axis, [(k, (k + step) % size) for k in range(size)])]
    all_to_all x1 -> x0, blocking collectives: 18.1 us -> none  [sent_and_summed(): lax.all_to_all(tiles, axis, split_axis=0, concat_axis=0, tiled=True)]
    all_to_all x1, waiting for transfers between devices: 21.2 us -> 8.41 us  [from_everyone(): lax.all_to_all(jnp.broadcast_to(value[None], (size, *value.shape)), axis,...]
    all_to_all x1, starting transfers between devices: 13.7 us -> 3.88 us  [from_everyone(): lax.all_to_all(jnp.broadcast_to(value[None], (size, *value.shape)), axis,...]
    all_to_all x1, waiting for transfers between devices: 5.77 us -> 1.05 us  [state_before(): arrived = lax.all_to_all(sent, ZY, 0, 0, tiled=True)]
    all_to_all x1, starting transfers between devices: 6.9 us -> 11.3 us  [state_before(): lax.all_to_all(prefix, ZY, 0, 0, tiled=True).reshape(RETAIN_KEY_SIZE, V_DIM)]
    unnamed x11 -> x28, local copies, waits for them, and re-layouts: 3.67 us -> 4.57 us
  transfers between devices with their start and end apart: 14 -> 26, of which waited for: 3 -> 10; matrix products, arithmetic and copies ran while one was open for 18% -> 10% of each run, Pallas kernels for 1% -> 1%
where the time goes in v5:
time: 209 us; the launch traced here: 206 us
  starting transfers between devices  111 us (53%)
  waiting for transfers between devices  42.4 us (20%)
  between operations  17.2 us (8%)
  local copies, waits for them, and re-layouts  13.6 us (7%)
  other arithmetic  12.1 us (6%)
  Pallas kernels  8.55 us (4%)
    ppermute x15, starting transfers between devices, moved(): lax.ppermute(value, axis, [(k, (k + step) % size) for k in range(size)])  63.6 us
    ppermute x6, starting transfers between devices, core_swap(): return lax.ppermute(value, CORE, [(0, 1), (1, 0)])  23.2 us
    ppermute x15, waiting for transfers between devices, moved(): lax.ppermute(value, axis, [(k, (k + step) % size) for k in range(size)])  22.9 us
    all_to_all x1, starting transfers between devices, state_before(): lax.all_to_all(prefix, ZY, 0, 0, tiled=True).reshape(RETAIN_KEY_SIZE, V_DIM)  11.3 us
    all_to_all x1, waiting for transfers between devices, state_before(): lax.all_to_all(prefix, ZY, 0, 0, tiled=True).reshape(RETAIN_KEY_SIZE, V_DIM)  9.98 us
    all_to_all x1, waiting for transfers between devices, from_everyone(): lax.all_to_all(jnp.broadcast_to(value[None], (size, *value.shape)), axis,...  8.41 us
    pallas_call x1, Pallas kernels, tail(): pl.pallas_call(tail_body, out_shape=jax.ShapeDtypeStruct((length, columns...  6.81 us
    all_to_all x1, starting transfers between devices, state_before(): arrived = lax.all_to_all(sent, ZY, 0, 0, tiled=True)  6.73 us
  transfers between devices with their start and end apart: 26, of which 10 were waited for; matrix products, arithmetic and copies ran while one was open for 10% of the time, Pallas kernels for 1%

profile of v5, /device:TPU:1, one launch (start us, length us, event | category | flops | bytes accessed | tf_op | source)
XLA Modules:
  0.0 206.1 jit_solution(15264226679842321801)
XLA Ops:
  10.2 3.9 %collective-permute-start = (bf16[64,2048]{1,0:T(8,128)(2,1)S(1)}, bf16[64,2048]{1,0:T(8,128)(2,1)S(1)}, u32[]{:S(2)}, u32[]{:S(2)}) collective-permute-start(bf16[64,2048]{1,0:T(8,128)(2,1)S(1)} %get-tuple-element.11), channel_id=1, source_target_pairs={{0,1},{1,2},{2,3},{3,0},{4,5},{5,6},{6,7},{7,4},{8,9},{9,10},{10,1... | collective-permute-start | bytes 786440 | tf_op jit(solution)/shard_map/ppermute | solution.py:38
  14.2 4.4 %collective-permute-start.1 = (bf16[64,2048]{1,0:T(8,128)(2,1)S(1)}, bf16[64,2048]{1,0:T(8,128)(2,1)S(1)}, u32[]{:S(2)}, u32[]{:S(2)}) collective-permute-start(bf16[64,2048]{1,0:T(8,128)(2,1)S(1)} %get-tuple-element.11), channel_id=1, source_target_pairs={{0,2},{1,3},{2,0},{3,1},{4,6},{5,7},{6,4},{7,5},{8,10},{9,11},{10,... | collective-permute-start | bytes 786440 | tf_op jit(solution)/shard_map/ppermute | solution.py:38
  18.5 3.1 %collective-permute-start.2 = (bf16[64,2048]{1,0:T(8,128)(2,1)S(1)}, bf16[64,2048]{1,0:T(8,128)(2,1)S(1)}, u32[]{:S(2)}, u32[]{:S(2)}) collective-permute-start(bf16[64,2048]{1,0:T(8,128)(2,1)S(1)} %get-tuple-element.11), channel_id=1, source_target_pairs={{0,3},{1,0},{2,1},{3,2},{4,7},{5,4},{6,5},{7,6},{8,11},{9,8},{10,9... | collective-permute-start | bytes 786440 | tf_op jit(solution)/shard_map/ppermute | solution.py:38
  21.7 6.4 %collective-permute-start.5 = (bf16[16,384]{1,0:T(8,128)(2,1)S(1)}, bf16[16,384]{1,0:T(8,128)(2,1)S(1)}, u32[]{:S(2)}, u32[]{:S(2)}) collective-permute-start(bf16[16,384]{1,0:T(8,128)(2,1)S(1)} %pad_maximum_fusion.12), channel_id=1, source_target_pairs={{0,4},{4,0},{1,5},{5,1},{2,6},{6,2},{3,7},{7,3},{8,12},{12,8},{9,1... | collective-permute-start | bytes 36872 | tf_op jit(solution)/shard_map/ppermute | solution.py:90
  38.1 3.9 %all-to-all-start = ((bf16[8,32,384]{2,1,0:T(8,128)(2,1)}), bf16[8,32,384]{2,1,0:T(8,128)(2,1)S(1)}, u32[]{:S(2)}, u32[]{:S(2)}) async-start(bf16[8,32,384]{2,1,0:T(8,128)(2,1)} %broadcast_in_dim.26), calls=%async_computation | async-start | bytes 393216 | tf_op jit(solution)/shard_map/all_to_all | solution.py:31
  42.1 8.4 %all-to-all-done = bf16[8,32,384]{2,1,0:T(8,128)(2,1)S(1)} async-done(((bf16[8,32,384]{2,1,0:T(8,128)(2,1)}), bf16[8,32,384]{2,1,0:T(8,128)(2,1)S(1)}, u32[]{:S(2)}, u32[]{:S(2)}) %all-to-all-start) | async-done | bytes 196640 | tf_op jit(solution)/shard_map/all_to_all | solution.py:31
  50.5 6.3 %collective-permute-start.6 = (bf16[256,384]{1,0:T(8,128)(2,1)S(1)}, bf16[256,384]{1,0:T(8,128)(2,1)S(1)}, u32[]{:S(2)}, u32[]{:S(2)}) collective-permute-start(bf16[256,384]{1,0:T(8,128)(2,1)S(1)} %bitcast.68), channel_id=1, source_target_pairs={{0,64},{64,128},{128,192},{192,256},{256,320},{320,384},{384,448},... | collective-permute-start | bytes 589832 | tf_op jit(solution)/shard_map/ppermute | solution.py:38
  56.8 7.8 %collective-permute-start.7 = (bf16[256,384]{1,0:T(8,128)(2,1)S(1)}, bf16[256,384]{1,0:T(8,128)(2,1)S(1)}, u32[]{:S(2)}, u32[]{:S(2)}) collective-permute-start(bf16[256,384]{1,0:T(8,128)(2,1)S(1)} %bitcast.69), channel_id=1, source_target_pairs={{0,448},{64,0},{128,64},{192,128},{256,192},{320,256},{384,320},{4... | collective-permute-start | bytes 589832 | tf_op jit(solution)/shard_map/ppermute | solution.py:38
  64.7 3.9 %collective-permute-start.4 = (bf16[256,2048]{1,0:T(8,128)(2,1)S(1)}, bf16[256,2048]{1,0:T(8,128)(2,1)S(1)}, u32[]{:S(2)}, u32[]{:S(2)}) collective-permute-start(bf16[256,2048]{1,0:T(8,128)(2,1)S(1)} %constant_dynamic-update-slice_fusion.9), channel_id=1, source_target_pairs={{0,4},{4,0},{1,5},{5,1},{2,6},{6,2},{3,7},{7,3},{8,12},{12,8},{9,1... | collective-permute-start | bytes 3145736 | tf_op jit(solution)/shard_map/ppermute | solution.py:90
  72.9 4.6 %collective-permute-start.9 = (bf16[256,384]{1,0:T(8,128)(2,1)S(1)}, bf16[256,384]{1,0:T(8,128)(2,1)S(1)}, u32[]{:S(2)}, u32[]{:S(2)}) collective-permute-start(bf16[256,384]{1,0:T(8,128)(2,1)S(1)} %collective-permute-done.7), channel_id=1, source_target_pairs={{0,448},{64,0},{128,64},{192,128},{256,192},{320,256},{384,320},{4... | collective-permute-start | bytes 589832 | tf_op jit(solution)/shard_map/ppermute | solution.py:38
  77.6 5.9 %collective-permute-done.8 = bf16[256,384]{1,0:T(8,128)(2,1)S(1)} collective-permute-done((bf16[256,384]{1,0:T(8,128)(2,1)S(1)}, bf16[256,384]{1,0:T(8,128)(2,1)S(1)}, u32[]{:S(2)}, u32[]{:S(2)}) %collective-permute-start.8) | collective-permute-done | bytes 196640 | tf_op jit(solution)/shard_map/ppermute | solution.py:38
  83.5 4.2 %collective-permute-start.10 = (bf16[256,384]{1,0:T(8,128)(2,1)S(1)}, bf16[256,384]{1,0:T(8,128)(2,1)S(1)}, u32[]{:S(2)}, u32[]{:S(2)}) collective-permute-start(bf16[256,384]{1,0:T(8,128)(2,1)S(1)} %collective-permute-done.8), channel_id=1, source_target_pairs={{0,64},{64,128},{128,192},{192,256},{256,320},{320,384},{384,448},... | collective-permute-start | bytes 589832 | tf_op jit(solution)/shard_map/ppermute | solution.py:38
  87.7 7.3 %collective-permute-start.11 = (bf16[256,384]{1,0:T(8,128)(2,1)S(1)}, bf16[256,384]{1,0:T(8,128)(2,1)S(1)}, u32[]{:S(2)}, u32[]{:S(2)}) collective-permute-start(bf16[256,384]{1,0:T(8,128)(2,1)S(1)} %collective-permute-done.9), channel_id=1, source_target_pairs={{0,448},{64,0},{128,64},{192,128},{256,192},{320,256},{384,320},{4... | collective-permute-start | bytes 589832 | tf_op jit(solution)/shard_map/ppermute | solution.py:38
  95.1 7.6 %collective-permute-done.10 = bf16[256,384]{1,0:T(8,128)(2,1)S(1)} collective-permute-done((bf16[256,384]{1,0:T(8,128)(2,1)S(1)}, bf16[256,384]{1,0:T(8,128)(2,1)S(1)}, u32[]{:S(2)}, u32[]{:S(2)}) %collective-permute-start.10) | collective-permute-done | bytes 196640 | tf_op jit(solution)/shard_map/ppermute | solution.py:38
  104.6 4.6 %collective-permute-start.13 = (bf16[128,384]{1,0:T(8,128)(2,1)S(1)}, bf16[128,384]{1,0:T(8,128)(2,1)S(1)}, u32[]{:S(2)}, u32[]{:S(2)}) collective-permute-start(bf16[128,384]{1,0:T(8,128)(2,1)S(1)} %slice.134), channel_id=1, source_target_pairs={{0,448},{64,0},{128,64},{192,128},{256,192},{320,256},{384,320},{4... | collective-permute-start | bytes 294920 | tf_op jit(solution)/shard_map/ppermute | solution.py:38
  116.4 6.7 %all-to-all-start.1 = ((f32[64,3,256]{2,1,0:T(4,128)}), f32[64,3,256]{2,1,0:T(4,128)}, u32[]{:S(2)}, u32[]{:S(2)}) async-start(f32[64,3,256]{2,1,0:T(4,128)} %concatenate.63), calls=%async_computation.1 | async-start | bytes 524288 | tf_op jit(solution)/shard_map/all_to_all | solution.py:113
  126.0 4.9 %collective-permute-start.14 = (bf16[256,128]{1,0:T(8,128)(2,1)}, bf16[256,128]{1,0:T(8,128)(2,1)}, u32[]{:S(2)}, u32[]{:S(2)}) collective-permute-start(bf16[256,128]{1,0:T(8,128)(2,1)} %dynamic-slice_bitcast_fusion.8), channel_id=1, source_target_pairs={{0,4},{4,0},{1,5},{5,1},{2,6},{6,2},{3,7},{7,3},{8,12},{12,8},{9,1... | collective-permute-start | bytes 196616 | tf_op jit(solution)/shard_map/ppermute | solution.py:90
  137.3 11.3 %all-to-all-start.2 = ((f32[64,2,256]{2,1,0:T(2,128)}), f32[64,2,256]{2,1,0:T(2,128)S(1)}, u32[]{:S(2)}, u32[]{:S(2)}) async-start(f32[64,2,256]{2,1,0:T(2,128)} %shard_map.118), calls=%async_computation.2 | async-start | bytes 262144 | tf_op jit(solution)/shard_map/all_to_all | solution.py:117
  150.1 10.0 %all-to-all-done.2 = f32[64,2,256]{2,1,0:T(2,128)S(1)} async-done(((f32[64,2,256]{2,1,0:T(2,128)}), f32[64,2,256]{2,1,0:T(2,128)S(1)}, u32[]{:S(2)}, u32[]{:S(2)}) %all-to-all-start.2) | async-done | bytes 131104 | tf_op jit(solution)/shard_map/all_to_all | solution.py:117
  160.3 4.1 %collective-permute-start.17 = (bf16[2,128,256]{2,1,0:T(8,128)(2,1)S(1)}, bf16[2,128,256]{2,1,0:T(8,128)(2,1)S(1)}, u32[]{:S(2)}, u32[]{:S(2)}) collective-permute-start(bf16[2,128,256]{2,1,0:T(8,128)(2,1)S(1)} %dynamic-slice_bitcast_fusion), channel_id=1, source_target_pairs={{0,4},{4,0},{1,5},{5,1},{2,6},{6,2},{3,7},{7,3},{8,12},{12,8},{9,1... | collective-permute-start | bytes 393224 | tf_op jit(solution)/shard_map/ppermute | solution.py:90
  170.6 6.8 %tail.1 = bf16[256,2048]{1,0:T(8,128)(2,1)S(1)} custom-call(bf16[384,2048]{1,0:T(8,128)(2,1)S(1)} %pad_maximum_fusion.rows_ref, bf16[2,256,128]{2,1,0:T(8,128)(2,1)S(1)} %copy-done.3, bf16[2,256,256]{2,1,0:T(8,128)(2,1)S(1)} %copy-done, bf16[2,2,128,256]{3,2,1,0:T(8,128)(2,1)S(1)} %copy-done.1, f32[2,2,128,128]{3,2,1,0:T(8,128)S(1)} %exponential_select_fusion.weight_ref, ...), custom_call_target="tpu_custom_call" | custom-call | tf_op jit(solution)/shard_map/tail/pallas_call | solution.py:320
  179.7 4.3 %collective-permute-start.20 = (bf16[32,2048]{1,0:T(8,128)(2,1)S(1)}, bf16[32,2048]{1,0:T(8,128)(2,1)S(1)}, u32[]{:S(2)}, u32[]{:S(2)}) collective-permute-start(bf16[32,2048]{1,0:T(8,128)(2,1)S(1)} %get-tuple-element.15), channel_id=1, source_target_pairs={{0,3},{1,0},{2,1},{3,2},{4,7},{5,4},{6,5},{7,6},{8,11},{9,8},{10,9... | collective-permute-start | bytes 393224 | tf_op jit(solution)/shard_map/ppermute | solution.py:38
  188.7 5.2 %collective-permute-start.21 = (bf16[64,2048]{1,0:T(8,128)(2,1)S(1)}, bf16[64,2048]{1,0:T(8,128)(2,1)S(1)}, u32[]{:S(2)}, u32[]{:S(2)}) collective-permute-start(bf16[64,2048]{1,0:T(8,128)(2,1)S(1)} %pad_maximum_fusion.6), channel_id=1, source_target_pairs={{0,3},{1,0},{2,1},{3,2},{4,7},{5,4},{6,5},{7,6},{8,11},{9,8},{10,9... | collective-permute-start | bytes 786440 | tf_op jit(solution)/shard_map/ppermute | solution.py:38
  193.9 3.5 %collective-permute-done.19 = bf16[64,2048]{1,0:T(8,128)(2,1)S(1)} collective-permute-done((bf16[64,2048]{1,0:T(8,128)(2,1)S(1)}, bf16[64,2048]{1,0:T(8,128)(2,1)S(1)}, u32[]{:S(2)}, u32[]{:S(2)}) %collective-permute-start.19) | collective-permute-done | bytes 262176 | tf_op jit(solution)/shard_map/ppermute | solution.py:38
  (138 shorter events, 49.8 us)
Async XLA Ops:
  6.5 160.4 %all-gather.2.cloned.1.call-start = ((), (), s32[]{:S(2)}) async-start(), calls=%async_computation.3 | async-start | bytes 7925760 | tf_op jit(solution)/shard_map/all_gather | solution.py:362
  10.2 31.8 %collective-permute-start = (bf16[64,2048]{1,0:T(8,128)(2,1)S(1)}, bf16[64,2048]{1,0:T(8,128)(2,1)S(1)}, u32[]{:S(2)}, u32[]{:S(2)}) collective-permute-start(bf16[64,2048]{1,0:T(8,128)(2,1)S(1)} %get-tuple-element.11), channel_id=1, source_target_pairs={{0,1},{1,2},{2,3},{3,0},{4,5},{5,6},{6,7},{7,4},{8,9},{9,10},{10,1... | collective-permute-start | bytes 786440 | tf_op jit(solution)/shard_map/ppermute | solution.py:38
  14.2 27.9 %collective-permute-start.1 = (bf16[64,2048]{1,0:T(8,128)(2,1)S(1)}, bf16[64,2048]{1,0:T(8,128)(2,1)S(1)}, u32[]{:S(2)}, u32[]{:S(2)}) collective-permute-start(bf16[64,2048]{1,0:T(8,128)(2,1)S(1)} %get-tuple-element.11), channel_id=1, source_target_pairs={{0,2},{1,3},{2,0},{3,1},{4,6},{5,7},{6,4},{7,5},{8,10},{9,11},{10,... | collective-permute-start | bytes 786440 | tf_op jit(solution)/shard_map/ppermute | solution.py:38
  18.5 46.1 %collective-permute-start.2 = (bf16[64,2048]{1,0:T(8,128)(2,1)S(1)}, bf16[64,2048]{1,0:T(8,128)(2,1)S(1)}, u32[]{:S(2)}, u32[]{:S(2)}) collective-permute-start(bf16[64,2048]{1,0:T(8,128)(2,1)S(1)} %get-tuple-element.11), channel_id=1, source_target_pairs={{0,3},{1,0},{2,1},{3,2},{4,7},{5,4},{6,5},{7,6},{8,11},{9,8},{10,9... | collective-permute-start | bytes 786440 | tf_op jit(solution)/shard_map/ppermute | solution.py:38
  21.7 15.7 %collective-permute-start.5 = (bf16[16,384]{1,0:T(8,128)(2,1)S(1)}, bf16[16,384]{1,0:T(8,128)(2,1)S(1)}, u32[]{:S(2)}, u32[]{:S(2)}) collective-permute-start(bf16[16,384]{1,0:T(8,128)(2,1)S(1)} %pad_maximum_fusion.12), channel_id=1, source_target_pairs={{0,4},{4,0},{1,5},{5,1},{2,6},{6,2},{3,7},{7,3},{8,12},{12,8},{9,1... | collective-permute-start | bytes 36872 | tf_op jit(solution)/shard_map/ppermute | solution.py:90
  38.1 12.4 %all-to-all-start = ((bf16[8,32,384]{2,1,0:T(8,128)(2,1)}), bf16[8,32,384]{2,1,0:T(8,128)(2,1)S(1)}, u32[]{:S(2)}, u32[]{:S(2)}) async-start(bf16[8,32,384]{2,1,0:T(8,128)(2,1)} %broadcast_in_dim.26), calls=%async_computation | async-start | bytes 393216 | tf_op jit(solution)/shard_map/all_to_all | solution.py:31
  50.5 20.4 %collective-permute-start.6 = (bf16[256,384]{1,0:T(8,128)(2,1)S(1)}, bf16[256,384]{1,0:T(8,128)(2,1)S(1)}, u32[]{:S(2)}, u32[]{:S(2)}) collective-permute-start(bf16[256,384]{1,0:T(8,128)(2,1)S(1)} %bitcast.68), channel_id=1, source_target_pairs={{0,64},{64,128},{128,192},{192,256},{256,320},{320,384},{384,448},... | collective-permute-start | bytes 589832 | tf_op jit(solution)/shard_map/ppermute | solution.py:38
  56.8 16.0 %collective-permute-start.7 = (bf16[256,384]{1,0:T(8,128)(2,1)S(1)}, bf16[256,384]{1,0:T(8,128)(2,1)S(1)}, u32[]{:S(2)}, u32[]{:S(2)}) collective-permute-start(bf16[256,384]{1,0:T(8,128)(2,1)S(1)} %bitcast.69), channel_id=1, source_target_pairs={{0,448},{64,0},{128,64},{192,128},{256,192},{320,256},{384,320},{4... | collective-permute-start | bytes 589832 | tf_op jit(solution)/shard_map/ppermute | solution.py:38
  64.7 47.1 %collective-permute-start.4 = (bf16[256,2048]{1,0:T(8,128)(2,1)S(1)}, bf16[256,2048]{1,0:T(8,128)(2,1)S(1)}, u32[]{:S(2)}, u32[]{:S(2)}) collective-permute-start(bf16[256,2048]{1,0:T(8,128)(2,1)S(1)} %constant_dynamic-update-slice_fusion.9), channel_id=1, source_target_pairs={{0,4},{4,0},{1,5},{5,1},{2,6},{6,2},{3,7},{7,3},{8,12},{12,8},{9,1... | collective-permute-start | bytes 3145736 | tf_op jit(solution)/shard_map/ppermute | solution.py:90
  68.6 54.5 %collective-permute-start.3 = (bf16[128,2048]{1,0:T(8,128)(2,1)S(1)}, bf16[128,2048]{1,0:T(8,128)(2,1)}, u32[]{:S(2)}, u32[]{:S(2)}) collective-permute-start(bf16[128,2048]{1,0:T(8,128)(2,1)S(1)} %slice.132), channel_id=1, source_target_pairs={{0,4},{4,8},{8,12},{12,16},{16,20},{20,24},{24,28},{28,32},{32,36}... | collective-permute-start | bytes 1572872 | tf_op jit(solution)/shard_map/ppermute | solution.py:26
  70.9 12.5 %collective-permute-start.8 = (bf16[256,384]{1,0:T(8,128)(2,1)S(1)}, bf16[256,384]{1,0:T(8,128)(2,1)S(1)}, u32[]{:S(2)}, u32[]{:S(2)}) collective-permute-start(bf16[256,384]{1,0:T(8,128)(2,1)S(1)} %collective-permute-done.6), channel_id=1, source_target_pairs={{0,64},{64,128},{128,192},{192,256},{256,320},{320,384},{384,448},... | collective-permute-start | bytes 589832 | tf_op jit(solution)/shard_map/ppermute | solution.py:38
  72.9 14.8 %collective-permute-start.9 = (bf16[256,384]{1,0:T(8,128)(2,1)S(1)}, bf16[256,384]{1,0:T(8,128)(2,1)S(1)}, u32[]{:S(2)}, u32[]{:S(2)}) collective-permute-start(bf16[256,384]{1,0:T(8,128)(2,1)S(1)} %collective-permute-done.7), channel_id=1, source_target_pairs={{0,448},{64,0},{128,64},{192,128},{256,192},{320,256},{384,320},{4... | collective-permute-start | bytes 589832 | tf_op jit(solution)/shard_map/ppermute | solution.py:38
  83.5 19.1 %collective-permute-start.10 = (bf16[256,384]{1,0:T(8,128)(2,1)S(1)}, bf16[256,384]{1,0:T(8,128)(2,1)S(1)}, u32[]{:S(2)}, u32[]{:S(2)}) collective-permute-start(bf16[256,384]{1,0:T(8,128)(2,1)S(1)} %collective-permute-done.8), channel_id=1, source_target_pairs={{0,64},{64,128},{128,192},{192,256},{256,320},{320,384},{384,448},... | collective-permute-start | bytes 589832 | tf_op jit(solution)/shard_map/ppermute | solution.py:38
  87.7 16.9 %collective-permute-start.11 = (bf16[256,384]{1,0:T(8,128)(2,1)S(1)}, bf16[256,384]{1,0:T(8,128)(2,1)S(1)}, u32[]{:S(2)}, u32[]{:S(2)}) collective-permute-start(bf16[256,384]{1,0:T(8,128)(2,1)S(1)} %collective-permute-done.9), channel_id=1, source_target_pairs={{0,448},{64,0},{128,64},{192,128},{256,192},{320,256},{384,320},{4... | collective-permute-start | bytes 589832 | tf_op jit(solution)/shard_map/ppermute | solution.py:38
  102.6 9.1 %collective-permute-start.12 = (bf16[128,384]{1,0:T(8,128)(2,1)S(1)}, bf16[128,384]{1,0:T(8,128)(2,1)S(1)}, u32[]{:S(2)}, u32[]{:S(2)}) collective-permute-start(bf16[128,384]{1,0:T(8,128)(2,1)S(1)} %slice.133), channel_id=1, source_target_pairs={{0,64},{64,128},{128,192},{192,256},{256,320},{320,384},{384,448},... | collective-permute-start | bytes 294920 | tf_op jit(solution)/shard_map/ppermute | solution.py:38
  104.6 7.1 %collective-permute-start.13 = (bf16[128,384]{1,0:T(8,128)(2,1)S(1)}, bf16[128,384]{1,0:T(8,128)(2,1)S(1)}, u32[]{:S(2)}, u32[]{:S(2)}) collective-permute-start(bf16[128,384]{1,0:T(8,128)(2,1)S(1)} %slice.134), channel_id=1, source_target_pairs={{0,448},{64,0},{128,64},{192,128},{256,192},{320,256},{384,320},{4... | collective-permute-start | bytes 294920 | tf_op jit(solution)/shard_map/ppermute | solution.py:38
  116.4 19.2 %all-to-all-start.1 = ((f32[64,3,256]{2,1,0:T(4,128)}), f32[64,3,256]{2,1,0:T(4,128)}, u32[]{:S(2)}, u32[]{:S(2)}) async-start(f32[64,3,256]{2,1,0:T(4,128)} %concatenate.63), calls=%async_computation.1 | async-start | bytes 524288 | tf_op jit(solution)/shard_map/all_to_all | solution.py:113
  126.0 22.6 %collective-permute-start.14 = (bf16[256,128]{1,0:T(8,128)(2,1)}, bf16[256,128]{1,0:T(8,128)(2,1)}, u32[]{:S(2)}, u32[]{:S(2)}) collective-permute-start(bf16[256,128]{1,0:T(8,128)(2,1)} %dynamic-slice_bitcast_fusion.8), channel_id=1, source_target_pairs={{0,4},{4,0},{1,5},{5,1},{2,6},{6,2},{3,7},{7,3},{8,12},{12,8},{9,1... | collective-permute-start | bytes 196616 | tf_op jit(solution)/shard_map/ppermute | solution.py:90
  132.4 32.0 %collective-permute-start.15 = (bf16[256,256]{1,0:T(8,128)(2,1)}, bf16[256,256]{1,0:T(8,128)(2,1)}, u32[]{:S(2)}, u32[]{:S(2)}) collective-permute-start(bf16[256,256]{1,0:T(8,128)(2,1)} %dynamic-slice_bitcast_fusion.7), channel_id=1, source_target_pairs={{0,4},{4,0},{1,5},{5,1},{2,6},{6,2},{3,7},{7,3},{8,12},{12,8},{9,1... | collective-permute-start | bytes 393224 | tf_op jit(solution)/shard_map/ppermute | solution.py:90
  137.3 22.8 %all-to-all-start.2 = ((f32[64,2,256]{2,1,0:T(2,128)}), f32[64,2,256]{2,1,0:T(2,128)S(1)}, u32[]{:S(2)}, u32[]{:S(2)}) async-start(f32[64,2,256]{2,1,0:T(2,128)} %shard_map.118), calls=%async_computation.2 | async-start | bytes 262144 | tf_op jit(solution)/shard_map/all_to_all | solution.py:117
  177.5 8.1 %collective-permute-start.18 = (bf16[32,2048]{1,0:T(8,128)(2,1)S(1)}, bf16[32,2048]{1,0:T(8,128)(2,1)S(1)}, u32[]{:S(2)}, u32[]{:S(2)}) collective-permute-start(bf16[32,2048]{1,0:T(8,128)(2,1)S(1)} %get-tuple-element.13), channel_id=1, source_target_pairs={{0,1},{1,2},{2,3},{3,0},{4,5},{5,6},{6,7},{7,4},{8,9},{9,10},{10,1... | collective-permute-start | bytes 393224 | tf_op jit(solution)/shard_map/ppermute | solution.py:38
  179.7 6.8 %collective-permute-start.20 = (bf16[32,2048]{1,0:T(8,128)(2,1)S(1)}, bf16[32,2048]{1,0:T(8,128)(2,1)S(1)}, u32[]{:S(2)}, u32[]{:S(2)}) collective-permute-start(bf16[32,2048]{1,0:T(8,128)(2,1)S(1)} %get-tuple-element.15), channel_id=1, source_target_pairs={{0,3},{1,0},{2,1},{3,2},{4,7},{5,4},{6,5},{7,6},{8,11},{9,8},{10,9... | collective-permute-start | bytes 393224 | tf_op jit(solution)/shard_map/ppermute | solution.py:38
  186.6 10.8 %collective-permute-start.19 = (bf16[64,2048]{1,0:T(8,128)(2,1)S(1)}, bf16[64,2048]{1,0:T(8,128)(2,1)S(1)}, u32[]{:S(2)}, u32[]{:S(2)}) collective-permute-start(bf16[64,2048]{1,0:T(8,128)(2,1)S(1)} %pad_maximum_fusion.5), channel_id=1, source_target_pairs={{0,1},{1,2},{2,3},{3,0},{4,5},{5,6},{6,7},{7,4},{8,9},{9,10},{10,1... | collective-permute-start | bytes 786440 | tf_op jit(solution)/shard_map/ppermute | solution.py:38
  188.7 9.7 %collective-permute-start.21 = (bf16[64,2048]{1,0:T(8,128)(2,1)S(1)}, bf16[64,2048]{1,0:T(8,128)(2,1)S(1)}, u32[]{:S(2)}, u32[]{:S(2)}) collective-permute-start(bf16[64,2048]{1,0:T(8,128)(2,1)S(1)} %pad_maximum_fusion.6), channel_id=1, source_target_pairs={{0,3},{1,0},{2,1},{3,2},{4,7},{5,4},{6,5},{7,6},{8,11},{9,8},{10,9... | collective-permute-start | bytes 786440 | tf_op jit(solution)/shard_map/ppermute | solution.py:38
  (16 other events, 149.9 us)
Sparse Core Ops, SparseCore 0:
  10.5 103.7 all-gather.1

commit v6 on v5

--- a/solution.py
+++ b/solution.py
@@ -38,31 +38,15 @@
     return lax.ppermute(value, axis, [(k, (k + step) % size) for k in range(size)])
 
 
-def added(first, second):
-    return (first.astype(jnp.float32) + second.astype(jnp.float32)).astype(jnp.bfloat16)
-
-
-def summed_over_four(value, axis):
-    size = lax.axis_size(axis)
-    here = lax.axis_index(axis)
-    tiles = value.reshape(size, -1, value.shape[-1])
-    half = tiles.shape[1] // 2
-
-    def for_device(step):
-        return lax.dynamic_index_in_dim(tiles, (here + step) % size, 0, keepdims=False)
-
-    far = for_device(2)
-    from_below = moved(far[half:], axis, 1)
-    from_above = moved(far[:half], axis, -1)
-    up = for_device(1)
-    down = for_device(3)
-    up = jnp.concatenate([up[:half], added(up[half:], from_below)], axis=0)
-    down = jnp.concatenate([added(down[:half], from_above), down[half:]], axis=0)
-    return (
-        for_device(0).astype(jnp.float32)
-        + moved(up, axis, 1).astype(jnp.float32)
-        + moved(down, axis, -1).astype(jnp.float32)
-    )
+def cut_along(value, dim, size):
+    before, after = (value.shape[:dim], value.shape[dim + 1 :])
+    return jnp.moveaxis(value.reshape(*before, size, -1, *after), dim, 0)
+
+
+def sent_and_summed(value, axis, dim):
+    tiles = cut_along(value, dim, lax.axis_size(axis))
+    arrived = lax.all_to_all(tiles, axis, split_axis=0, concat_axis=0, tiled=True)
+    return arrived.astype(jnp.float32).sum(axis=0)
 
 
 def rotate(values, positions):
@@ -100,9 +84,46 @@
 def prefix_body(parts_ref, out_ref):
     count = parts_ref.shape[0]
     carried = jnp.zeros(out_ref.shape[1:], jnp.float32)
+    fades = [jnp.exp(parts_ref[k, 2:3]) for k in range(count)]
     for k in range(count):
         out_ref[k] = carried
-        carried = carried * jnp.exp(parts_ref[k, 2:3]) + parts_ref[k, :2]
+        carried = carried * fades[k] + parts_ref[k, :2]
+
+
+def states_body(arrived_ref, contrib_ref, fade_ref, core_ref, mine_ref, theirs_ref, state_ref):
+    rows = arrived_ref.shape[1]
+    for k in range(arrived_ref.shape[0]):
+        state_ref[k * rows : (k + 1) * rows] = arrived_ref[k]
+    blocks = contrib_ref.shape[0]
+    here = blocks // 2
+    state = state_ref[...]
+    for n in range(blocks):
+        rounded = state.astype(jnp.bfloat16)
+
+        @pl.when(core_ref[0] == n // here)
+        def _():
+            mine_ref[n % here] = rounded
+
+        @pl.when(core_ref[0] != n // here)
+        def _():
+            theirs_ref[n % here] = rounded
+
+        if n + 1 < blocks:
+            state = state * fade_ref[n] + contrib_ref[n]
+
+
+def states(arrived, contrib, fades):
+    half = jax.ShapeDtypeStruct((contrib.shape[0] // 2, *contrib.shape[1:]), jnp.bfloat16)
+    vmem = pl.BlockSpec(memory_space=pltpu.VMEM)
+    smem = pl.BlockSpec(memory_space=pltpu.SMEM)
+    return pl.pallas_call(
+        states_body,
+        out_shape=(half, half),
+        in_specs=[vmem, vmem, smem, smem],
+        out_specs=(vmem, vmem),
+        scratch_shapes=[pltpu.VMEM(contrib.shape[1:], jnp.float32)],
+        name="states",
+    )(arrived, contrib, fades, lax.axis_index(CORE).reshape(1))
 
 
 def state_before(total, log_total):
@@ -114,7 +135,7 @@
     prefix = pl.pallas_call(
         prefix_body, out_shape=jax.ShapeDtypeStruct((count, 2, V_DIM), jnp.float32)
     )(arrived)
-    return lax.all_to_all(prefix, ZY, 0, 0, tiled=True).reshape(RETAIN_KEY_SIZE, V_DIM)
+    return lax.all_to_all(prefix, ZY, 0, 0, tiled=True)
 
 
 def columns_of_head(ret_key, ret_value, head):
@@ -194,20 +215,17 @@
     total = contrib[0]
     for n in range(1, blocks):
         total = total * jnp.exp(closing[n]) + contrib[n]
-    state = state_before(total, jnp.sum(closing))
-    before = []
-    for n in range(blocks):
-        before.append(state)
-        state = state * jnp.exp(closing[n]) + contrib[n]
-    return keys, values, jnp.stack(before)
+    arrived = state_before(total, jnp.sum(closing))
+    mine, theirs = states(arrived, contrib, jnp.exp(closing))
+    return keys, values, mine, core_swap(theirs)
 
 
 CHUNKS = 4
 
 
 def tail_body(
-    rows_ref, key_ref, value_ref, before_ref, weight_ref, fade_ref, cos_ref, sin_ref, bias_ref,
-    sink_ref, whole_ref, out_ref, win_ref, wout_ref, ret_ref, att_ref, sems,
+    rows_ref, key_ref, value_ref, own_ref, other_ref, running_ref, column_ref, cos_ref, sin_ref,
+    sink_ref, place_ref, whole_ref, out_ref, win_ref, wout_ref, ret_ref, att_ref, sems,
 ):
     width, in_width = (rows_ref.shape[1], win_ref.shape[1])
     length = out_ref.shape[0]
@@ -237,7 +255,10 @@
         )
         total = part if total is None else total + part
     projected = total.astype(jnp.bfloat16)
-    heads, blocks = (before_ref.shape[0], before_ref.shape[1])
+    heads, blocks = (key_ref.shape[0], own_ref.shape[0])
+    here = lax.broadcasted_iota(jnp.int32, (BLOCK, BLOCK), 0)
+    causal_mask = here >= lax.broadcasted_iota(jnp.int32, (BLOCK, BLOCK), 1)
+    core = place_ref[0]
     rim = rows_ref.shape[0] - length
     cosine = cos_ref[...]
     sine_part = sin_ref[...]
@@ -246,15 +267,18 @@
         query = projected[rim:, h * RETAIN_KEY_SIZE : (h + 1) * RETAIN_KEY_SIZE].astype(jnp.float32)
         turned = pltpu.roll(query, RETAIN_KEY_SIZE // 2, 1)
         query = (query * cosine + turned * sine_part).astype(jnp.bfloat16)
-        faded = (query.astype(jnp.float32) * fade_ref[h]).astype(jnp.bfloat16)
+        faded = (query.astype(jnp.float32) * jnp.exp(column_ref[h])).astype(jnp.bfloat16)
         for n in range(blocks):
             part = slice(n * BLOCK, (n + 1) * BLOCK)
             scores = lax.dot_general(
                 query[part], key_ref[h, part], contract_last, preferred_element_type=jnp.float32
             )
-            scores = (scores * weight_ref[h, n]).astype(jnp.bfloat16)
+            within = column_ref[h, part] - running_ref[h, n : n + 1]
+            weighting = jnp.where(causal_mask, jnp.exp(jnp.minimum(within, 0.0)), 0.0)
+            scores = (scores * weighting).astype(jnp.bfloat16)
+            before = jnp.where(core == h, own_ref[n], other_ref[n])
             mixed = jnp.dot(scores, value_ref[h, part], preferred_element_type=jnp.float32)
-            mixed = mixed + jnp.dot(faded[part], before_ref[h, n], preferred_element_type=jnp.float32)
+            mixed = mixed + jnp.dot(faded[part], before, preferred_element_type=jnp.float32)
             mixed = mixed * lax.rsqrt(jnp.mean(mixed * mixed, axis=-1, keepdims=True) + epsilon)
             ret_ref[part, h * V_DIM : (h + 1) * V_DIM] = mixed.astype(jnp.bfloat16)
     first = heads * RETAIN_KEY_SIZE
@@ -264,7 +288,10 @@
     values = projected[:, keys_at + HEAD_DIM : keys_at + 2 * HEAD_DIM]
     for n in range(length // WINDOW):
         seen = slice(n * WINDOW, (n + 2) * WINDOW)
-        bias = bias_ref[n]
+        ahead = lax.broadcasted_iota(jnp.int32, (WINDOW, 2 * WINDOW), 1)
+        offset = ahead - lax.broadcasted_iota(jnp.int32, (WINDOW, 2 * WINDOW), 0)
+        there = ahead + (place_ref[1] + (n - 1) * WINDOW) >= 0
+        allowed = (offset > 0) & (offset <= WINDOW) & there
         for g in range(0, group, 2):
             pair = []
             for k in (g, g + 1):
@@ -273,7 +300,7 @@
                 scores = lax.dot_general(
                     query, keys[seen], contract_last, preferred_element_type=jnp.float32
                 )
-                scores = scores * HEAD_DIM ** (-0.5) + bias
+                scores = jnp.where(allowed, scores * HEAD_DIM ** (-0.5), masked_out)
                 sink = jnp.full((WINDOW, 1), sink_ref[k], jnp.float32)
                 highest = jnp.maximum(jnp.max(scores, axis=-1, keepdims=True), sink)
                 lifted = jnp.exp(scores - highest)
@@ -295,24 +322,18 @@
     out_ref[...] = result.astype(jnp.bfloat16)
 
 
-def tail(rows, keys, values, before, log_decay, sink_logits, whole, anchor, in_width):
+def tail(rows, keys, values, own, other, core, log_decay, sink_logits, whole, anchor, in_width):
     length = keys.shape[1]
-    heads, blocks = (before.shape[0], before.shape[1])
+    heads, blocks = (keys.shape[0], own.shape[0])
     running = jnp.cumsum(log_decay.reshape(heads, blocks, BLOCK), axis=-1)
-    within = running[:, :, :, None] - running[:, :, None, :]
-    causal_mask = jnp.arange(BLOCK)[:, None] >= jnp.arange(BLOCK)[None, :]
-    weighting = jnp.where(causal_mask, jnp.exp(jnp.minimum(within, 0.0)), 0.0)
-    fade = jnp.exp(running).reshape(heads, length, 1)
+    column = running.reshape(heads, length, 1)
     half_dim = RETAIN_KEY_SIZE // 2
     inverse = rope_base ** (-jnp.arange(half_dim, dtype=jnp.float32) / half_dim)
     positions = anchor + jnp.arange(length, dtype=jnp.int32)
     angles = positions.astype(jnp.float32)[:, None] * inverse[None, :]
     cosine = jnp.concatenate([jnp.cos(angles)] * 2, axis=1)
     sine_part = jnp.concatenate([-jnp.sin(angles), jnp.sin(angles)], axis=1)
-    starts = jnp.arange(length // WINDOW)[:, None, None] * WINDOW
-    ahead = jnp.arange(2 * WINDOW)[None, None, :] - jnp.arange(WINDOW)[None, :, None]
-    there = anchor + starts - WINDOW + jnp.arange(2 * WINDOW)[None, None, :] >= 0
-    bias = jnp.where((ahead > 0) & (ahead <= WINDOW) & there, 0.0, masked_out)
+    place = jnp.stack([core, anchor]).astype(jnp.int32)
     out_width = whole.shape[1] - in_width
     features = rows.shape[1]
     columns = whole.shape[0]
@@ -321,7 +342,8 @@
         tail_body,
         out_shape=jax.ShapeDtypeStruct((length, columns), jnp.bfloat16),
         in_specs=[vmem] * 9
-        + [pl.BlockSpec(memory_space=pltpu.SMEM), pl.BlockSpec(memory_space=pltpu.HBM)],
+        + [pl.BlockSpec(memory_space=pltpu.SMEM)] * 2
+        + [pl.BlockSpec(memory_space=pltpu.HBM)],
         out_specs=vmem,
         scratch_shapes=[
             pltpu.VMEM((features, in_width), jnp.bfloat16),
@@ -332,8 +354,10 @@
         ],
         compiler_params=pltpu.CompilerParams(vmem_limit_bytes=40 * 1024 * 1024),
         name="tail",
-    )(rows, keys, values, before, weighting, fade, cosine, sine_part, bias, sink_logits,
-      pltpu.with_memory_space_constraint(whole, pltpu.HBM))
+    )(
+        rows, keys, values, own, other, running, column, cosine, sine_part, sink_logits, place,
+        pltpu.with_memory_space_constraint(whole, pltpu.HBM),
+    )
 
 
 def on_device(
@@ -357,6 +381,7 @@
         * lax.rsqrt(jnp.mean(tok_float * tok_float, axis=-1, keepdims=True) + epsilon)
         * norm_gain
     ).astype(jnp.bfloat16)
+    normed = lax.optimization_barrier(normed)
     weights = (ret_query, att_query, att_key, att_value)
     widths = [weight.shape[1] for weight in weights]
     whole = lax.all_gather(
@@ -375,7 +400,7 @@
     other_half = lax.dynamic_index_in_dim(decay_other, core, 0, keepdims=False)
     anchor = lax.axis_index(SP) * tok_count
     chip_anchor = lax.axis_index(ZY) * (2 * tok_count)
-    keys, values, before = chain_of_head(
+    keys, values, state_own, state_other = chain_of_head(
         in_core_order(kv[0], kv[1], 0), in_core_order(own_head, other_half, 0), chip_anchor
     )
 
@@ -387,21 +412,22 @@
 
     key_ret = heads_of_own_rows(keys)
     value_ret = heads_of_own_rows(values)
-    before = heads_of_own_rows(before)
 
     input_width = sum(widths)
     partial = tail(
         jnp.concatenate([rim, own_rows], axis=0),
         key_ret,
         value_ret,
-        before.astype(jnp.bfloat16),
+        state_own,
+        state_other,
+        core,
         log_decay,
         sink_logits,
         whole,
         anchor,
         input_width,
     )
-    mixed = summed_over_four(partial, "tp")
+    mixed = sent_and_summed(partial, "tp", 0)
     return mixed.astype(jnp.bfloat16)
 
 

time: 209 us -> 198 us (0.947)
  starting transfers between devices: 111 us -> 93.6 us
  blocking collectives: 0 us -> 17.3 us
  other arithmetic: 12.1 us -> 7.65 us
  local copies, waits for them, and re-layouts: 13.6 us -> 9.2 us
    all_to_all x0 -> x1, blocking collectives: none -> 17.3 us  [sent_and_summed(): lax.all_to_all(tiles, axis, split_axis=0, concat_axis=0, tiled=True)]
    ppermute x15 -> x11, starting transfers between devices: 63.6 us -> 48.6 us  [moved(): lax.ppermute(value, axis, [(k, (k + step) % size) for k in range(size)])]
    ppermute x15 -> x11, waiting for transfers between devices: 22.9 us -> 15 us  [moved(): lax.ppermute(value, axis, [(k, (k + step) % size) for k in range(size)])]
    unnamed x28 -> x10, local copies, waits for them, and re-layouts: 4.57 us -> 1.58 us
    all_to_all x1, starting transfers between devices: 11.3 us -> 8.43 us  [state_before(): return lax.all_to_all(prefix, ZY, 0, 0, tiled=True)]
    all_to_all x1, waiting for transfers between devices: 1.05 us -> 3.92 us  [state_before(): arrived = lax.all_to_all(sent, ZY, 0, 0, tiled=True)]
    squeeze x3 -> x2, local copies, waits for them, and re-layouts: 2.22 us -> 0.03 us  [heads_of_own_rows(): theirs = lax.dynamic_index_in_dim(halves, 1 - core, 0, keepdims=False)]
  transfers between devices with their start and end apart: 26 -> 22, of which waited for: 10 -> 7; matrix products, arithmetic and copies ran while one was open for 10% -> 7% of each run, Pallas kernels for 1% -> 2%
where the time goes in v6:
time: 198 us; the launch traced here: 197 us
  starting transfers between devices  93.6 us (47%)
  waiting for transfers between devices  40.8 us (21%)
  blocking collectives  17.3 us (9%)
  between operations  16.3 us (8%)
  Pallas kernels  10.6 us (5%)
  local copies, waits for them, and re-layouts  9.2 us (5%)
  other arithmetic  7.65 us (4%)
    ppermute x11, starting transfers between devices, moved(): lax.ppermute(value, axis, [(k, (k + step) % size) for k in range(size)])  48.6 us
    ppermute x6, starting transfers between devices, core_swap(): return lax.ppermute(value, CORE, [(0, 1), (1, 0)])  23.6 us
    all_to_all x1, blocking collectives, sent_and_summed(): lax.all_to_all(tiles, axis, split_axis=0, concat_axis=0, tiled=True)  17.3 us
    ppermute x11, waiting for transfers between devices, moved(): lax.ppermute(value, axis, [(k, (k + step) % size) for k in range(size)])  15 us
    all_to_all x1, waiting for transfers between devices, state_before(): return lax.all_to_all(prefix, ZY, 0, 0, tiled=True)  11.5 us
    all_to_all x1, waiting for transfers between devices, from_everyone(): lax.all_to_all(jnp.broadcast_to(value[None], (size, *value.shape)), axis,...  9.46 us
    all_to_all x1, starting transfers between devices, state_before(): return lax.all_to_all(prefix, ZY, 0, 0, tiled=True)  8.43 us
    all_to_all x1, starting transfers between devices, state_before(): arrived = lax.all_to_all(sent, ZY, 0, 0, tiled=True)  7.09 us
  transfers between devices with their start and end apart: 22, of which 7 were waited for; matrix products, arithmetic and copies ran while one was open for 7% of the time, Pallas kernels for 2%

profile of v6, /device:TPU:1, one launch (start us, length us, event | category | flops | bytes accessed | tf_op | source)
XLA Modules:
  0.0 196.7 jit_solution(338214203383427823)
XLA Ops:
  10.3 3.9 %collective-permute-start = (bf16[64,2048]{1,0:T(8,128)(2,1)S(1)}, bf16[64,2048]{1,0:T(8,128)(2,1)S(1)}, u32[]{:S(2)}, u32[]{:S(2)}) collective-permute-start(bf16[64,2048]{1,0:T(8,128)(2,1)S(1)} %fusion.9), channel_id=1, source_target_pairs={{0,1},{1,2},{2,3},{3,0},{4,5},{5,6},{6,7},{7,4},{8,9},{9,10},{10,1... | collective-permute-start | bytes 786440 | tf_op jit(solution)/shard_map/ppermute | solution.py:38
  14.2 4.4 %collective-permute-start.1 = (bf16[64,2048]{1,0:T(8,128)(2,1)S(1)}, bf16[64,2048]{1,0:T(8,128)(2,1)S(1)}, u32[]{:S(2)}, u32[]{:S(2)}) collective-permute-start(bf16[64,2048]{1,0:T(8,128)(2,1)S(1)} %fusion.9), channel_id=1, source_target_pairs={{0,2},{1,3},{2,0},{3,1},{4,6},{5,7},{6,4},{7,5},{8,10},{9,11},{10,... | collective-permute-start | bytes 786440 | tf_op jit(solution)/shard_map/ppermute | solution.py:38
  18.6 3.1 %collective-permute-start.2 = (bf16[64,2048]{1,0:T(8,128)(2,1)S(1)}, bf16[64,2048]{1,0:T(8,128)(2,1)S(1)}, u32[]{:S(2)}, u32[]{:S(2)}) collective-permute-start(bf16[64,2048]{1,0:T(8,128)(2,1)S(1)} %fusion.9), channel_id=1, source_target_pairs={{0,3},{1,0},{2,1},{3,2},{4,7},{5,4},{6,5},{7,6},{8,11},{9,8},{10,9... | collective-permute-start | bytes 786440 | tf_op jit(solution)/shard_map/ppermute | solution.py:38
  23.1 6.4 %collective-permute-start.5 = (bf16[16,384]{1,0:T(8,128)(2,1)S(1)}, bf16[16,384]{1,0:T(8,128)(2,1)S(1)}, u32[]{:S(2)}, u32[]{:S(2)}) collective-permute-start(bf16[16,384]{1,0:T(8,128)(2,1)S(1)} %pad_maximum_fusion.8), channel_id=1, source_target_pairs={{0,4},{4,0},{1,5},{5,1},{2,6},{6,2},{3,7},{7,3},{8,12},{12,8},{9,1... | collective-permute-start | bytes 36872 | tf_op jit(solution)/shard_map/ppermute | solution.py:74
  38.6 3.9 %all-to-all-start = ((bf16[8,32,384]{2,1,0:T(8,128)(2,1)}), bf16[8,32,384]{2,1,0:T(8,128)(2,1)S(1)}, u32[]{:S(2)}, u32[]{:S(2)}) async-start(bf16[8,32,384]{2,1,0:T(8,128)(2,1)} %broadcast_in_dim.14), calls=%async_computation | async-start | bytes 393216 | tf_op jit(solution)/shard_map/all_to_all | solution.py:31
  42.5 9.5 %all-to-all-done = bf16[8,32,384]{2,1,0:T(8,128)(2,1)S(1)} async-done(((bf16[8,32,384]{2,1,0:T(8,128)(2,1)}), bf16[8,32,384]{2,1,0:T(8,128)(2,1)S(1)}, u32[]{:S(2)}, u32[]{:S(2)}) %all-to-all-start) | async-done | bytes 196640 | tf_op jit(solution)/shard_map/all_to_all | solution.py:31
  52.0 5.7 %collective-permute-start.6 = (bf16[256,384]{1,0:T(8,128)(2,1)S(1)}, bf16[256,384]{1,0:T(8,128)(2,1)S(1)}, u32[]{:S(2)}, u32[]{:S(2)}) collective-permute-start(bf16[256,384]{1,0:T(8,128)(2,1)S(1)} %bitcast.34), channel_id=1, source_target_pairs={{0,64},{64,128},{128,192},{192,256},{256,320},{320,384},{384,448},... | collective-permute-start | bytes 589832 | tf_op jit(solution)/shard_map/ppermute | solution.py:38
  57.7 7.0 %collective-permute-start.7 = (bf16[256,384]{1,0:T(8,128)(2,1)S(1)}, bf16[256,384]{1,0:T(8,128)(2,1)S(1)}, u32[]{:S(2)}, u32[]{:S(2)}) collective-permute-start(bf16[256,384]{1,0:T(8,128)(2,1)S(1)} %bitcast.35), channel_id=1, source_target_pairs={{0,448},{64,0},{128,64},{192,128},{256,192},{320,256},{384,320},{4... | collective-permute-start | bytes 589832 | tf_op jit(solution)/shard_map/ppermute | solution.py:38
  64.8 4.2 %collective-permute-start.4 = (bf16[256,2048]{1,0:T(8,128)(2,1)S(1)}, bf16[256,2048]{1,0:T(8,128)(2,1)S(1)}, u32[]{:S(2)}, u32[]{:S(2)}) collective-permute-start(bf16[256,2048]{1,0:T(8,128)(2,1)S(1)} %constant_dynamic-update-slice_fusion.9), channel_id=1, source_target_pairs={{0,4},{4,0},{1,5},{5,1},{2,6},{6,2},{3,7},{7,3},{8,12},{12,8},{9,1... | collective-permute-start | bytes 3145736 | tf_op jit(solution)/shard_map/ppermute | solution.py:74
  69.0 2.1 %collective-permute-start.3 = (bf16[128,2048]{1,0:T(8,128)(2,1)S(1)}, bf16[128,2048]{1,0:T(8,128)(2,1)}, u32[]{:S(2)}, u32[]{:S(2)}) collective-permute-start(bf16[128,2048]{1,0:T(8,128)(2,1)S(1)} %slice.79), channel_id=1, source_target_pairs={{0,4},{4,8},{8,12},{12,16},{16,20},{20,24},{24,28},{28,32},{32,36}... | collective-permute-start | bytes 1572872 | tf_op jit(solution)/shard_map/ppermute | solution.py:26
  73.2 4.6 %collective-permute-start.9 = (bf16[256,384]{1,0:T(8,128)(2,1)S(1)}, bf16[256,384]{1,0:T(8,128)(2,1)S(1)}, u32[]{:S(2)}, u32[]{:S(2)}) collective-permute-start(bf16[256,384]{1,0:T(8,128)(2,1)S(1)} %collective-permute-done.7), channel_id=1, source_target_pairs={{0,448},{64,0},{128,64},{192,128},{256,192},{320,256},{384,320},{4... | collective-permute-start | bytes 589832 | tf_op jit(solution)/shard_map/ppermute | solution.py:38
  77.9 5.9 %collective-permute-done.8 = bf16[256,384]{1,0:T(8,128)(2,1)S(1)} collective-permute-done((bf16[256,384]{1,0:T(8,128)(2,1)S(1)}, bf16[256,384]{1,0:T(8,128)(2,1)S(1)}, u32[]{:S(2)}, u32[]{:S(2)}) %collective-permute-start.8) | collective-permute-done | bytes 196640 | tf_op jit(solution)/shard_map/ppermute | solution.py:38
  83.8 4.2 %collective-permute-start.10 = (bf16[256,384]{1,0:T(8,128)(2,1)S(1)}, bf16[256,384]{1,0:T(8,128)(2,1)S(1)}, u32[]{:S(2)}, u32[]{:S(2)}) collective-permute-start(bf16[256,384]{1,0:T(8,128)(2,1)S(1)} %collective-permute-done.8), channel_id=1, source_target_pairs={{0,64},{64,128},{128,192},{192,256},{256,320},{320,384},{384,448},... | collective-permute-start | bytes 589832 | tf_op jit(solution)/shard_map/ppermute | solution.py:38
  88.0 7.3 %collective-permute-start.11 = (bf16[256,384]{1,0:T(8,128)(2,1)S(1)}, bf16[256,384]{1,0:T(8,128)(2,1)S(1)}, u32[]{:S(2)}, u32[]{:S(2)}) collective-permute-start(bf16[256,384]{1,0:T(8,128)(2,1)S(1)} %collective-permute-done.9), channel_id=1, source_target_pairs={{0,448},{64,0},{128,64},{192,128},{256,192},{320,256},{384,320},{4... | collective-permute-start | bytes 589832 | tf_op jit(solution)/shard_map/ppermute | solution.py:38
  95.4 7.2 %collective-permute-done.10 = bf16[256,384]{1,0:T(8,128)(2,1)S(1)} collective-permute-done((bf16[256,384]{1,0:T(8,128)(2,1)S(1)}, bf16[256,384]{1,0:T(8,128)(2,1)S(1)}, u32[]{:S(2)}, u32[]{:S(2)}) %collective-permute-start.10) | collective-permute-done | bytes 196640 | tf_op jit(solution)/shard_map/ppermute | solution.py:38
  104.6 4.6 %collective-permute-start.13 = (bf16[128,384]{1,0:T(8,128)(2,1)S(1)}, bf16[128,384]{1,0:T(8,128)(2,1)S(1)}, u32[]{:S(2)}, u32[]{:S(2)}) collective-permute-start(bf16[128,384]{1,0:T(8,128)(2,1)S(1)} %slice.81), channel_id=1, source_target_pairs={{0,448},{64,0},{128,64},{192,128},{256,192},{320,256},{384,320},{4... | collective-permute-start | bytes 294920 | tf_op jit(solution)/shard_map/ppermute | solution.py:38
  115.0 7.1 %all-to-all-start.1 = ((f32[64,3,256]{2,1,0:T(4,128)}), f32[64,3,256]{2,1,0:T(4,128)}, u32[]{:S(2)}, u32[]{:S(2)}) async-start(f32[64,3,256]{2,1,0:T(4,128)} %concatenate.53), calls=%async_computation.1 | async-start | bytes 524288 | tf_op jit(solution)/shard_map/all_to_all | solution.py:134
  123.5 5.1 %collective-permute-start.14 = (bf16[256,128]{1,0:T(8,128)(2,1)S(1)}, bf16[256,128]{1,0:T(8,128)(2,1)S(1)}, u32[]{:S(2)}, u32[]{:S(2)}) collective-permute-start(bf16[256,128]{1,0:T(8,128)(2,1)S(1)} %dynamic-slice_bitcast_fusion.1), channel_id=1, source_target_pairs={{0,4},{4,0},{1,5},{5,1},{2,6},{6,2},{3,7},{7,3},{8,12},{12,8},{9,1... | collective-permute-start | bytes 196616 | tf_op jit(solution)/shard_map/ppermute | solution.py:74
  130.5 3.9 %all-to-all-done.1.parts_ref = f32[64,3,256]{2,1,0:T(4,128)} async-done(((f32[64,3,256]{2,1,0:T(4,128)}), f32[64,3,256]{2,1,0:T(4,128)}, u32[]{:S(2)}, u32[]{:S(2)}) %all-to-all-start.1) | async-done | bytes 196640 | tf_op jit(solution)/shard_map/all_to_all | solution.py:134
  136.2 8.4 %all-to-all-start.2 = ((f32[64,2,256]{2,1,0:T(2,128)}), f32[64,2,256]{2,1,0:T(2,128)S(1)}, u32[]{:S(2)}, u32[]{:S(2)}) async-start(f32[64,2,256]{2,1,0:T(2,128)} %shard_map.118), calls=%async_computation.2 | async-start | bytes 262144 | tf_op jit(solution)/shard_map/all_to_all | solution.py:138
  144.7 11.5 %all-to-all-done.2.arrived_ref = f32[64,2,256]{2,1,0:T(2,128)S(1)} async-done(((f32[64,2,256]{2,1,0:T(2,128)}), f32[64,2,256]{2,1,0:T(2,128)S(1)}, u32[]{:S(2)}, u32[]{:S(2)}) %all-to-all-start.2) | async-done | bytes 131104 | tf_op jit(solution)/shard_map/all_to_all | solution.py:138
  158.8 4.1 %collective-permute-start.17 = (bf16[2,128,256]{2,1,0:T(8,128)(2,1)}, bf16[2,128,256]{2,1,0:T(8,128)(2,1)S(1)}, u32[]{:S(2)}, u32[]{:S(2)}) collective-permute-start(bf16[2,128,256]{2,1,0:T(8,128)(2,1)} %get-tuple-element.8), channel_id=1, source_target_pairs={{0,4},{4,0},{1,5},{5,1},{2,6},{6,2},{3,7},{7,3},{8,12},{12,8},{9,1... | collective-permute-start | bytes 393224 | tf_op jit(solution)/shard_map/ppermute | solution.py:74
  164.8 6.8 %tail.1 = bf16[256,2048]{1,0:T(8,128)(2,1)S(1)} custom-call(bf16[384,2048]{1,0:T(8,128)(2,1)S(1)} %pad_maximum_fusion.rows_ref, bf16[2,256,128]{2,1,0:T(8,128)(2,1)S(1)} %pad_maximum_fusion.3.key_ref, bf16[2,256,256]{2,1,0:T(8,128)(2,1)S(1)} %pad_maximum_fusion.2.value_ref, bf16[2,128,256]{2,1,0:T(8,128)(2,1)S(1)} %copy-done, ...), custom_call_target="tpu_custom_call" | custom-call | tf_op jit(solution)/shard_map/tail/pallas_call | solution.py:341
  171.7 17.3 %all_to_all.20 = bf16[4,64,2048]{2,1,0:T(8,128)(2,1)S(1)} all-to-all(bf16[4,64,2048]{2,1,0:T(8,128)(2,1)S(1)} %bitcast.30), channel_id=1, replica_groups=mesh['sp_0'=8,'sp_1'=8,'sp_2'=2,'tp'=4] {'tp'}, dimensions={0} | all-to-all | bytes 2097152 | tf_op jit(solution)/shard_map/all_to_all | solution.py:48
  (100 shorter events, 32.4 us)
Async XLA Ops:
  6.5 157.4 %all-gather.2.cloned.1.call-start = ((), (), s32[]{:S(2)}) async-start(), calls=%async_computation.4 | async-start | bytes 7925760 | tf_op jit(solution)/shard_map/all_gather | solution.py:387
  10.3 22.2 %copy-start.4 = (f32[2,256]{1,0:T(2,128)S(1)}, f32[2,256]{1,0:T(2,128)}, u32[]{:S(2)}) copy-start(f32[2,256]{1,0:T(2,128)} %param.17) | copy-start | bytes 6148
  10.3 32.2 %collective-permute-start = (bf16[64,2048]{1,0:T(8,128)(2,1)S(1)}, bf16[64,2048]{1,0:T(8,128)(2,1)S(1)}, u32[]{:S(2)}, u32[]{:S(2)}) collective-permute-start(bf16[64,2048]{1,0:T(8,128)(2,1)S(1)} %fusion.9), channel_id=1, source_target_pairs={{0,1},{1,2},{2,3},{3,0},{4,5},{5,6},{6,7},{7,4},{8,9},{9,10},{10,1... | collective-permute-start | bytes 786440 | tf_op jit(solution)/shard_map/ppermute | solution.py:38
  14.2 28.3 %collective-permute-start.1 = (bf16[64,2048]{1,0:T(8,128)(2,1)S(1)}, bf16[64,2048]{1,0:T(8,128)(2,1)S(1)}, u32[]{:S(2)}, u32[]{:S(2)}) collective-permute-start(bf16[64,2048]{1,0:T(8,128)(2,1)S(1)} %fusion.9), channel_id=1, source_target_pairs={{0,2},{1,3},{2,0},{3,1},{4,6},{5,7},{6,4},{7,5},{8,10},{9,11},{10,... | collective-permute-start | bytes 786440 | tf_op jit(solution)/shard_map/ppermute | solution.py:38
  18.6 46.1 %collective-permute-start.2 = (bf16[64,2048]{1,0:T(8,128)(2,1)S(1)}, bf16[64,2048]{1,0:T(8,128)(2,1)S(1)}, u32[]{:S(2)}, u32[]{:S(2)}) collective-permute-start(bf16[64,2048]{1,0:T(8,128)(2,1)S(1)} %fusion.9), channel_id=1, source_target_pairs={{0,3},{1,0},{2,1},{3,2},{4,7},{5,4},{6,5},{7,6},{8,11},{9,8},{10,9... | collective-permute-start | bytes 786440 | tf_op jit(solution)/shard_map/ppermute | solution.py:38
  23.1 14.7 %collective-permute-start.5 = (bf16[16,384]{1,0:T(8,128)(2,1)S(1)}, bf16[16,384]{1,0:T(8,128)(2,1)S(1)}, u32[]{:S(2)}, u32[]{:S(2)}) collective-permute-start(bf16[16,384]{1,0:T(8,128)(2,1)S(1)} %pad_maximum_fusion.8), channel_id=1, source_target_pairs={{0,4},{4,0},{1,5},{5,1},{2,6},{6,2},{3,7},{7,3},{8,12},{12,8},{9,1... | collective-permute-start | bytes 36872 | tf_op jit(solution)/shard_map/ppermute | solution.py:74
  29.5 4.0 %collective-permute-start.16 = (f32[2,256]{1,0:T(2,128)}, f32[2,256]{1,0:T(2,128)S(1)}, u32[]{:S(2)}, u32[]{:S(2)}) collective-permute-start(f32[2,256]{1,0:T(2,128)} %param.17), channel_id=1, source_target_pairs={{0,4},{4,0},{1,5},{5,1},{2,6},{6,2},{3,7},{7,3},{8,12},{12,8},{9,1... | collective-permute-start | bytes 6152 | tf_op jit(solution)/shard_map/ppermute | solution.py:74
  38.6 13.4 %all-to-all-start = ((bf16[8,32,384]{2,1,0:T(8,128)(2,1)}), bf16[8,32,384]{2,1,0:T(8,128)(2,1)S(1)}, u32[]{:S(2)}, u32[]{:S(2)}) async-start(bf16[8,32,384]{2,1,0:T(8,128)(2,1)} %broadcast_in_dim.14), calls=%async_computation | async-start | bytes 393216 | tf_op jit(solution)/shard_map/all_to_all | solution.py:31
  52.0 19.3 %collective-permute-start.6 = (bf16[256,384]{1,0:T(8,128)(2,1)S(1)}, bf16[256,384]{1,0:T(8,128)(2,1)S(1)}, u32[]{:S(2)}, u32[]{:S(2)}) collective-permute-start(bf16[256,384]{1,0:T(8,128)(2,1)S(1)} %bitcast.34), channel_id=1, source_target_pairs={{0,64},{64,128},{128,192},{192,256},{256,320},{320,384},{384,448},... | collective-permute-start | bytes 589832 | tf_op jit(solution)/shard_map/ppermute | solution.py:38
  57.7 15.5 %collective-permute-start.7 = (bf16[256,384]{1,0:T(8,128)(2,1)S(1)}, bf16[256,384]{1,0:T(8,128)(2,1)S(1)}, u32[]{:S(2)}, u32[]{:S(2)}) collective-permute-start(bf16[256,384]{1,0:T(8,128)(2,1)S(1)} %bitcast.35), channel_id=1, source_target_pairs={{0,448},{64,0},{128,64},{192,128},{256,192},{320,256},{384,320},{4... | collective-permute-start | bytes 589832 | tf_op jit(solution)/shard_map/ppermute | solution.py:38
  64.8 46.5 %collective-permute-start.4 = (bf16[256,2048]{1,0:T(8,128)(2,1)S(1)}, bf16[256,2048]{1,0:T(8,128)(2,1)S(1)}, u32[]{:S(2)}, u32[]{:S(2)}) collective-permute-start(bf16[256,2048]{1,0:T(8,128)(2,1)S(1)} %constant_dynamic-update-slice_fusion.9), channel_id=1, source_target_pairs={{0,4},{4,0},{1,5},{5,1},{2,6},{6,2},{3,7},{7,3},{8,12},{12,8},{9,1... | collective-permute-start | bytes 3145736 | tf_op jit(solution)/shard_map/ppermute | solution.py:74
  69.0 53.1 %collective-permute-start.3 = (bf16[128,2048]{1,0:T(8,128)(2,1)S(1)}, bf16[128,2048]{1,0:T(8,128)(2,1)}, u32[]{:S(2)}, u32[]{:S(2)}) collective-permute-start(bf16[128,2048]{1,0:T(8,128)(2,1)S(1)} %slice.79), channel_id=1, source_target_pairs={{0,4},{4,8},{8,12},{12,16},{16,20},{20,24},{24,28},{28,32},{32,36}... | collective-permute-start | bytes 1572872 | tf_op jit(solution)/shard_map/ppermute | solution.py:26
  71.3 12.5 %collective-permute-start.8 = (bf16[256,384]{1,0:T(8,128)(2,1)S(1)}, bf16[256,384]{1,0:T(8,128)(2,1)S(1)}, u32[]{:S(2)}, u32[]{:S(2)}) collective-permute-start(bf16[256,384]{1,0:T(8,128)(2,1)S(1)} %collective-permute-done.6), channel_id=1, source_target_pairs={{0,64},{64,128},{128,192},{192,256},{256,320},{320,384},{384,448},... | collective-permute-start | bytes 589832 | tf_op jit(solution)/shard_map/ppermute | solution.py:38
  73.2 14.8 %collective-permute-start.9 = (bf16[256,384]{1,0:T(8,128)(2,1)S(1)}, bf16[256,384]{1,0:T(8,128)(2,1)S(1)}, u32[]{:S(2)}, u32[]{:S(2)}) collective-permute-start(bf16[256,384]{1,0:T(8,128)(2,1)S(1)} %collective-permute-done.7), channel_id=1, source_target_pairs={{0,448},{64,0},{128,64},{192,128},{256,192},{320,256},{384,320},{4... | collective-permute-start | bytes 589832 | tf_op jit(solution)/shard_map/ppermute | solution.py:38
  83.8 18.8 %collective-permute-start.10 = (bf16[256,384]{1,0:T(8,128)(2,1)S(1)}, bf16[256,384]{1,0:T(8,128)(2,1)S(1)}, u32[]{:S(2)}, u32[]{:S(2)}) collective-permute-start(bf16[256,384]{1,0:T(8,128)(2,1)S(1)} %collective-permute-done.8), channel_id=1, source_target_pairs={{0,64},{64,128},{128,192},{192,256},{256,320},{320,384},{384,448},... | collective-permute-start | bytes 589832 | tf_op jit(solution)/shard_map/ppermute | solution.py:38
  88.0 16.5 %collective-permute-start.11 = (bf16[256,384]{1,0:T(8,128)(2,1)S(1)}, bf16[256,384]{1,0:T(8,128)(2,1)S(1)}, u32[]{:S(2)}, u32[]{:S(2)}) collective-permute-start(bf16[256,384]{1,0:T(8,128)(2,1)S(1)} %collective-permute-done.9), channel_id=1, source_target_pairs={{0,448},{64,0},{128,64},{192,128},{256,192},{320,256},{384,320},{4... | collective-permute-start | bytes 589832 | tf_op jit(solution)/shard_map/ppermute | solution.py:38
  102.6 8.6 %collective-permute-start.12 = (bf16[128,384]{1,0:T(8,128)(2,1)S(1)}, bf16[128,384]{1,0:T(8,128)(2,1)S(1)}, u32[]{:S(2)}, u32[]{:S(2)}) collective-permute-start(bf16[128,384]{1,0:T(8,128)(2,1)S(1)} %slice.80), channel_id=1, source_target_pairs={{0,64},{64,128},{128,192},{192,256},{256,320},{320,384},{384,448},... | collective-permute-start | bytes 294920 | tf_op jit(solution)/shard_map/ppermute | solution.py:38
  104.6 6.7 %collective-permute-start.13 = (bf16[128,384]{1,0:T(8,128)(2,1)S(1)}, bf16[128,384]{1,0:T(8,128)(2,1)S(1)}, u32[]{:S(2)}, u32[]{:S(2)}) collective-permute-start(bf16[128,384]{1,0:T(8,128)(2,1)S(1)} %slice.81), channel_id=1, source_target_pairs={{0,448},{64,0},{128,64},{192,128},{256,192},{320,256},{384,320},{4... | collective-permute-start | bytes 294920 | tf_op jit(solution)/shard_map/ppermute | solution.py:38
  115.0 19.4 %all-to-all-start.1 = ((f32[64,3,256]{2,1,0:T(4,128)}), f32[64,3,256]{2,1,0:T(4,128)}, u32[]{:S(2)}, u32[]{:S(2)}) async-start(f32[64,3,256]{2,1,0:T(4,128)} %concatenate.53), calls=%async_computation.1 | async-start | bytes 524288 | tf_op jit(solution)/shard_map/all_to_all | solution.py:134
  123.5 21.2 %collective-permute-start.14 = (bf16[256,128]{1,0:T(8,128)(2,1)S(1)}, bf16[256,128]{1,0:T(8,128)(2,1)S(1)}, u32[]{:S(2)}, u32[]{:S(2)}) collective-permute-start(bf16[256,128]{1,0:T(8,128)(2,1)S(1)} %dynamic-slice_bitcast_fusion.1), channel_id=1, source_target_pairs={{0,4},{4,0},{1,5},{5,1},{2,6},{6,2},{3,7},{7,3},{8,12},{12,8},{9,1... | collective-permute-start | bytes 196616 | tf_op jit(solution)/shard_map/ppermute | solution.py:74
  128.5 35.4 %copy-start.1 = (f32[8]{0:T(128)S(1)}, f32[8]{0:T(128)}, u32[]{:S(2)}) copy-start(f32[8]{0:T(128)} %sink_ref.1) | copy-start | bytes 100
  128.6 34.3 %collective-permute-start.15 = (bf16[256,256]{1,0:T(8,128)(2,1)S(1)}, bf16[256,256]{1,0:T(8,128)(2,1)S(1)}, u32[]{:S(2)}, u32[]{:S(2)}) collective-permute-start(bf16[256,256]{1,0:T(8,128)(2,1)S(1)} %dynamic-slice_bitcast_fusion), channel_id=1, source_target_pairs={{0,4},{4,0},{1,5},{5,1},{2,6},{6,2},{3,7},{7,3},{8,12},{12,8},{9,1... | collective-permute-start | bytes 393224 | tf_op jit(solution)/shard_map/ppermute | solution.py:74
  136.2 20.0 %all-to-all-start.2 = ((f32[64,2,256]{2,1,0:T(2,128)}), f32[64,2,256]{2,1,0:T(2,128)S(1)}, u32[]{:S(2)}, u32[]{:S(2)}) async-start(f32[64,2,256]{2,1,0:T(2,128)} %shard_map.118), calls=%async_computation.2 | async-start | bytes 262144 | tf_op jit(solution)/shard_map/all_to_all | solution.py:138
  158.8 5.1 %collective-permute-start.17 = (bf16[2,128,256]{2,1,0:T(8,128)(2,1)}, bf16[2,128,256]{2,1,0:T(8,128)(2,1)S(1)}, u32[]{:S(2)}, u32[]{:S(2)}) collective-permute-start(bf16[2,128,256]{2,1,0:T(8,128)(2,1)} %get-tuple-element.8), channel_id=1, source_target_pairs={{0,4},{4,0},{1,5},{5,1},{2,6},{6,2},{3,7},{7,3},{8,12},{12,8},{9,1... | collective-permute-start | bytes 393224 | tf_op jit(solution)/shard_map/ppermute | solution.py:74
  (3 other events, 10.2 us)
Sparse Core Ops, SparseCore 0:
  10.5 103.2 all-gather.1

commit v7 on v6

--- a/solution.py
+++ b/solution.py
@@ -122,6 +122,7 @@
         in_specs=[vmem, vmem, smem, smem],
         out_specs=(vmem, vmem),
         scratch_shapes=[pltpu.VMEM(contrib.shape[1:], jnp.float32)],
+        compiler_params=pltpu.CompilerParams(vmem_limit_bytes=8 * 1024 * 1024),
         name="states",
     )(arrived, contrib, fades, lax.axis_index(CORE).reshape(1))
 
@@ -133,7 +134,9 @@
     sent = jnp.concatenate([slices, marks], axis=1)
     arrived = lax.all_to_all(sent, ZY, 0, 0, tiled=True)
     prefix = pl.pallas_call(
-        prefix_body, out_shape=jax.ShapeDtypeStruct((count, 2, V_DIM), jnp.float32)
+        prefix_body,
+        out_shape=jax.ShapeDtypeStruct((count, 2, V_DIM), jnp.float32),
+        compiler_params=pltpu.CompilerParams(vmem_limit_bytes=8 * 1024 * 1024),
     )(arrived)
     return lax.all_to_all(prefix, ZY, 0, 0, tiled=True)
 
@@ -181,20 +184,6 @@
     return put(whole, down, here + size // 2, half)
 
 
-def gathered_rows(value, axis):
-    size = lax.axis_size(axis)
-    here = lax.axis_index(axis)
-    rows = value.shape[0]
-    whole = jnp.zeros((size * rows, value.shape[1]), value.dtype)
-    whole = lax.dynamic_update_slice_in_dim(whole, value, here * rows, 0)
-    for step in range(1, size):
-        piece = moved(value, axis, step)
-        whole = lax.dynamic_update_slice_in_dim(
-            whole, piece, (here - step + size) % size * rows, 0
-        )
-    return whole
-
-
 def chain_of_head(kv, log_decay, anchor):
     length = kv.shape[0]
     blocks = length // BLOCK
@@ -205,30 +194,33 @@
     values = kv[:, RETAIN_KEY_SIZE:]
     running = jnp.cumsum(log_decay.reshape(blocks, BLOCK), axis=-1)
     closing = running[:, -1]
+    fades = jnp.exp(closing)
+    key_fades = jnp.exp(closing[:, None] - running)
+    log_total = jnp.sum(closing)
     faded = (
         keys.reshape(blocks, BLOCK, -1).astype(jnp.float32)
-        * jnp.exp(closing[:, None] - running)[..., None]
+        * key_fades[..., None]
     ).astype(jnp.bfloat16)
     contrib = jnp.einsum(
         "njd,njv->ndv", faded, values.reshape(blocks, BLOCK, -1), preferred_element_type=jnp.float32
     )
     total = contrib[0]
     for n in range(1, blocks):
-        total = total * jnp.exp(closing[n]) + contrib[n]
-    arrived = state_before(total, jnp.sum(closing))
-    mine, theirs = states(arrived, contrib, jnp.exp(closing))
+        total = total * fades[n] + contrib[n]
+    arrived = state_before(total, log_total)
+    mine, theirs = states(arrived, contrib, fades)
     return keys, values, mine, core_swap(theirs)
 
 
 CHUNKS = 4
 
 
-def tail_body(
-    rows_ref, key_ref, value_ref, own_ref, other_ref, running_ref, column_ref, cos_ref, sin_ref,
-    sink_ref, place_ref, whole_ref, out_ref, win_ref, wout_ref, ret_ref, att_ref, sems,
+def front_body(
+    rows_ref, key_ref, value_ref, running_ref, column_ref, cos_ref, sin_ref, sink_ref, place_ref,
+    whole_ref, inner_ref, faded_ref, part_ref, win_ref, wout_ref, att_ref, sems,
 ):
     width, in_width = (rows_ref.shape[1], win_ref.shape[1])
-    length = out_ref.shape[0]
+    length = part_ref.shape[0]
     step = width // CHUNKS
     copies = [
         pltpu.make_async_copy(
@@ -240,7 +232,9 @@
     ]
     copies.append(
         pltpu.make_async_copy(
-            whole_ref.at[:, pl.ds(in_width, wout_ref.shape[1])], wout_ref, sems.at[CHUNKS]
+            whole_ref.at[:, pl.ds(whole_ref.shape[1] - wout_ref.shape[1], wout_ref.shape[1])],
+            wout_ref,
+            sems.at[CHUNKS],
         )
     )
     for copy in copies:
@@ -255,10 +249,9 @@
         )
         total = part if total is None else total + part
     projected = total.astype(jnp.bfloat16)
-    heads, blocks = (key_ref.shape[0], own_ref.shape[0])
+    heads, blocks = (key_ref.shape[0], length // BLOCK)
     here = lax.broadcasted_iota(jnp.int32, (BLOCK, BLOCK), 0)
     causal_mask = here >= lax.broadcasted_iota(jnp.int32, (BLOCK, BLOCK), 1)
-    core = place_ref[0]
     rim = rows_ref.shape[0] - length
     cosine = cos_ref[...]
     sine_part = sin_ref[...]
@@ -267,7 +260,8 @@
         query = projected[rim:, h * RETAIN_KEY_SIZE : (h + 1) * RETAIN_KEY_SIZE].astype(jnp.float32)
         turned = pltpu.roll(query, RETAIN_KEY_SIZE // 2, 1)
         query = (query * cosine + turned * sine_part).astype(jnp.bfloat16)
-        faded = (query.astype(jnp.float32) * jnp.exp(column_ref[h])).astype(jnp.bfloat16)
+        faded = query.astype(jnp.float32) * jnp.exp(column_ref[h])
+        faded_ref[:, h * RETAIN_KEY_SIZE : (h + 1) * RETAIN_KEY_SIZE] = faded.astype(jnp.bfloat16)
         for n in range(blocks):
             part = slice(n * BLOCK, (n + 1) * BLOCK)
             scores = lax.dot_general(
@@ -276,11 +270,9 @@
             within = column_ref[h, part] - running_ref[h, n : n + 1]
             weighting = jnp.where(causal_mask, jnp.exp(jnp.minimum(within, 0.0)), 0.0)
             scores = (scores * weighting).astype(jnp.bfloat16)
-            before = jnp.where(core == h, own_ref[n], other_ref[n])
-            mixed = jnp.dot(scores, value_ref[h, part], preferred_element_type=jnp.float32)
-            mixed = mixed + jnp.dot(faded[part], before, preferred_element_type=jnp.float32)
-            mixed = mixed * lax.rsqrt(jnp.mean(mixed * mixed, axis=-1, keepdims=True) + epsilon)
-            ret_ref[part, h * V_DIM : (h + 1) * V_DIM] = mixed.astype(jnp.bfloat16)
+            inner_ref[part, h * V_DIM : (h + 1) * V_DIM] = jnp.dot(
+                scores, value_ref[h, part], preferred_element_type=jnp.float32
+            )
     first = heads * RETAIN_KEY_SIZE
     group = sink_ref.shape[0]
     keys_at = first + group * HEAD_DIM
@@ -290,7 +282,7 @@
         seen = slice(n * WINDOW, (n + 2) * WINDOW)
         ahead = lax.broadcasted_iota(jnp.int32, (WINDOW, 2 * WINDOW), 1)
         offset = ahead - lax.broadcasted_iota(jnp.int32, (WINDOW, 2 * WINDOW), 0)
-        there = ahead + (place_ref[1] + (n - 1) * WINDOW) >= 0
+        there = ahead + (place_ref[0] + (n - 1) * WINDOW) >= 0
         allowed = (offset > 0) & (offset <= WINDOW) & there
         for g in range(0, group, 2):
             pair = []
@@ -313,18 +305,41 @@
                 jnp.concatenate(pair, axis=1).astype(jnp.bfloat16)
             )
     copies[CHUNKS].wait()
-    half = ret_ref.shape[1]
-    result = lax.dot_general(
-        ret_ref[...], wout_ref[:, :half], contract_last, preferred_element_type=jnp.float32
-    ) + lax.dot_general(
-        att_ref[...], wout_ref[:, half:], contract_last, preferred_element_type=jnp.float32
+    part_ref[...] = lax.dot_general(
+        att_ref[...], wout_ref[...], contract_last, preferred_element_type=jnp.float32
+    )
+
+
+def back_body(
+    inner_ref, faded_ref, part_ref, own_ref, other_ref, place_ref, whole_ref, out_ref, wout_ref,
+    ret_ref, sem,
+):
+    width = wout_ref.shape[1]
+    start = whole_ref.shape[1] - 2 * width
+    copy = pltpu.make_async_copy(whole_ref.at[:, pl.ds(start, width)], wout_ref, sem)
+    copy.start()
+    core = place_ref[0]
+    for h in range(ret_ref.shape[1] // V_DIM):
+        columns = slice(h * V_DIM, (h + 1) * V_DIM)
+        depth = slice(h * RETAIN_KEY_SIZE, (h + 1) * RETAIN_KEY_SIZE)
+        for n in range(own_ref.shape[0]):
+            part = slice(n * BLOCK, (n + 1) * BLOCK)
+            before = jnp.where(core == h, own_ref[n], other_ref[n])
+            mixed = inner_ref[part, columns] + jnp.dot(
+                faded_ref[part, depth], before, preferred_element_type=jnp.float32
+            )
+            mixed = mixed * lax.rsqrt(jnp.mean(mixed * mixed, axis=-1, keepdims=True) + epsilon)
+            ret_ref[part, columns] = mixed.astype(jnp.bfloat16)
+    copy.wait()
+    result = part_ref[...] + lax.dot_general(
+        ret_ref[...], wout_ref[...], (((1,), (1,)), ((), ())), preferred_element_type=jnp.float32
     )
     out_ref[...] = result.astype(jnp.bfloat16)
 
 
 def tail(rows, keys, values, own, other, core, log_decay, sink_logits, whole, anchor, in_width):
     length = keys.shape[1]
-    heads, blocks = (keys.shape[0], own.shape[0])
+    heads, blocks = (keys.shape[0], length // BLOCK)
     running = jnp.cumsum(log_decay.reshape(heads, blocks, BLOCK), axis=-1)
     column = running.reshape(heads, length, 1)
     half_dim = RETAIN_KEY_SIZE // 2
@@ -333,31 +348,47 @@
     angles = positions.astype(jnp.float32)[:, None] * inverse[None, :]
     cosine = jnp.concatenate([jnp.cos(angles)] * 2, axis=1)
     sine_part = jnp.concatenate([-jnp.sin(angles), jnp.sin(angles)], axis=1)
-    place = jnp.stack([core, anchor]).astype(jnp.int32)
-    out_width = whole.shape[1] - in_width
+    half = (whole.shape[1] - in_width) // 2
     features = rows.shape[1]
     columns = whole.shape[0]
     vmem = pl.BlockSpec(memory_space=pltpu.VMEM)
+    smem = pl.BlockSpec(memory_space=pltpu.SMEM)
+    hbm = pl.BlockSpec(memory_space=pltpu.HBM)
+    whole = pltpu.with_memory_space_constraint(whole, pltpu.HBM)
+    inner, faded, part = pl.pallas_call(
+        front_body,
+        out_shape=(
+            jax.ShapeDtypeStruct((length, heads * V_DIM), jnp.float32),
+            jax.ShapeDtypeStruct((length, heads * RETAIN_KEY_SIZE), jnp.bfloat16),
+            jax.ShapeDtypeStruct((length, columns), jnp.float32),
+        ),
+        in_specs=[vmem] * 7 + [smem] * 2 + [hbm],
+        out_specs=(vmem, vmem, vmem),
+        scratch_shapes=[
+            pltpu.VMEM((features, in_width), jnp.bfloat16),
+            pltpu.VMEM((columns, half), jnp.bfloat16),
+            pltpu.VMEM((length, half), jnp.bfloat16),
+            pltpu.SemaphoreType.DMA((CHUNKS + 1,)),
+        ],
+        compiler_params=pltpu.CompilerParams(vmem_limit_bytes=24 * 1024 * 1024),
+        name="front",
+    )(
+        rows, keys, values, running, column, cosine, sine_part, sink_logits,
+        anchor.astype(jnp.int32).reshape(1), whole,
+    )
     return pl.pallas_call(
-        tail_body,
+        back_body,
         out_shape=jax.ShapeDtypeStruct((length, columns), jnp.bfloat16),
-        in_specs=[vmem] * 9
-        + [pl.BlockSpec(memory_space=pltpu.SMEM)] * 2
-        + [pl.BlockSpec(memory_space=pltpu.HBM)],
+        in_specs=[vmem] * 5 + [smem, hbm],
         out_specs=vmem,
         scratch_shapes=[
-            pltpu.VMEM((features, in_width), jnp.bfloat16),
-            pltpu.VMEM((columns, out_width), jnp.bfloat16),
+            pltpu.VMEM((columns, half), jnp.bfloat16),
             pltpu.VMEM((length, heads * V_DIM), jnp.bfloat16),
-            pltpu.VMEM((length, sink_logits.shape[0] * HEAD_DIM), jnp.bfloat16),
-            pltpu.SemaphoreType.DMA((CHUNKS + 1,)),
+            pltpu.SemaphoreType.DMA(()),
         ],
-        compiler_params=pltpu.CompilerParams(vmem_limit_bytes=40 * 1024 * 1024),
-        name="tail",
-    )(
-        rows, keys, values, own, other, running, column, cosine, sine_part, sink_logits, place,
-        pltpu.with_memory_space_constraint(whole, pltpu.HBM),
-    )
+        compiler_params=pltpu.CompilerParams(vmem_limit_bytes=16 * 1024 * 1024),
+        name="back",
+    )(inner, faded, part, own, other, core.astype(jnp.int32).reshape(1), whole)
 
 
 def on_device(
@@ -388,7 +419,7 @@
         jnp.concatenate([*weights, ret_out.T, att_out.T], axis=1), SP, axis=0, tiled=True
     )
     head_weight = weight_of_head(ret_key, ret_value)
-    own_rows = gathered_rows(normed, "tp")
+    own_rows = from_everyone(normed, "tp").reshape(-1, normed.shape[1])
     other_rows = core_swap(own_rows)
     tok_count = own_rows.shape[0]
     rim = shifted(own_rows[tok_count - WINDOW :], SP, 1)

time: 198 us -> 185 us (0.934)
  waiting for transfers between devices: 40.8 us -> 33.6 us
  starting transfers between devices: 93.6 us -> 88 us
  other arithmetic: 7.65 us -> 10.6 us
  between operations: 16.3 us -> 14.2 us
    ppermute x11 -> x8, starting transfers between devices: 48.6 us -> 36.2 us  [moved(): lax.ppermute(value, axis, [(k, (k + step) % size) for k in range(size)])]
    ppermute x11 -> x8, waiting for transfers between devices: 15 us -> 10.1 us  [moved(): lax.ppermute(value, axis, [(k, (k + step) % size) for k in range(size)])]
    ppermute x6, starting transfers between devices: 23.6 us -> 26.6 us  [core_swap(): return lax.ppermute(value, CORE, [(0, 1), (1, 0)])]
    all_to_all x1 -> x2, starting transfers between devices: 3.88 us -> 6.91 us  [from_everyone(): lax.all_to_all(jnp.broadcast_to(value[None], (size, *value.shape)), axis,...]
    pallas_call x1 -> x2, Pallas kernels: 6.85 us -> 8.73 us  [the longest x1 6.16 us: tail(): pl.pallas_call(front_body, out_shape=(jax.ShapeDtypeStruct((length, heads...]
    all_to_all x1 -> x2, waiting for transfers between devices: 9.46 us -> 8.88 us  [from_everyone(): lax.all_to_all(jnp.broadcast_to(value[None], (size, *value.shape)), axis,...]
  transfers between devices with their start and end apart: 22 -> 20, of which waited for: 7 -> 9; matrix products, arithmetic and copies ran while one was open for 7% -> 10% of each run, Pallas kernels for 2% -> 4%
where the time goes in v7:
time: 185 us; the launch traced here: 184 us
  starting transfers between devices  88 us (48%)
  waiting for transfers between devices  33.6 us (18%)
  blocking collectives  17.3 us (9%)
  between operations  14.2 us (8%)
  other arithmetic  10.6 us (6%)
  Pallas kernels  10.2 us (6%)
  local copies, waits for them, and re-layouts  8.61 us (5%)
    ppermute x8, starting transfers between devices, moved(): lax.ppermute(value, axis, [(k, (k + step) % size) for k in range(size)])  36.2 us
    ppermute x6, starting transfers between devices, core_swap(): return lax.ppermute(value, CORE, [(0, 1), (1, 0)])  26.6 us
    all_to_all x1, blocking collectives, sent_and_summed(): lax.all_to_all(tiles, axis, split_axis=0, concat_axis=0, tiled=True)  17.3 us
    all_to_all x1, waiting for transfers between devices, state_before(): return lax.all_to_all(prefix, ZY, 0, 0, tiled=True)  11.5 us
    ppermute x8, waiting for transfers between devices, moved(): lax.ppermute(value, axis, [(k, (k + step) % size) for k in range(size)])  10.1 us
    all_to_all x1, starting transfers between devices, state_before(): return lax.all_to_all(prefix, ZY, 0, 0, tiled=True)  9.33 us
    all_to_all x2, waiting for transfers between devices, from_everyone(): lax.all_to_all(jnp.broadcast_to(value[None], (size, *value.shape)), axis,...  8.88 us
    all_to_all x2, starting transfers between devices, from_everyone(): lax.all_to_all(jnp.broadcast_to(value[None], (size, *value.shape)), axis,...  6.91 us
  transfers between devices with their start and end apart: 20, of which 9 were waited for; matrix products, arithmetic and copies ran while one was open for 10% of the time, Pallas kernels for 4%

profile of v7, /device:TPU:1, one launch (start us, length us, event | category | flops | bytes accessed | tf_op | source)
XLA Modules:
  0.0 183.6 jit_solution(633249374590619119)
XLA Ops:
  9.5 8.7 %collective-permute-start.2 = (bf16[16,384]{1,0:T(8,128)(2,1)S(1)}, bf16[16,384]{1,0:T(8,128)(2,1)S(1)}, u32[]{:S(2)}, u32[]{:S(2)}) collective-permute-start(bf16[16,384]{1,0:T(8,128)(2,1)S(1)} %pad_maximum_fusion.8), channel_id=1, source_target_pairs={{0,4},{4,0},{1,5},{5,1},{2,6},{6,2},{3,7},{7,3},{8,12},{12,8},{9,1... | collective-permute-start | bytes 36872 | tf_op jit(solution)/shard_map/ppermute | solution.py:74
  18.2 1.9 %collective-permute-start.13 = (f32[2,256]{1,0:T(2,128)}, f32[2,256]{1,0:T(2,128)S(1)}, u32[]{:S(2)}, u32[]{:S(2)}) collective-permute-start(f32[2,256]{1,0:T(2,128)} %param.17), channel_id=1, source_target_pairs={{0,4},{4,0},{1,5},{5,1},{2,6},{6,2},{3,7},{7,3},{8,12},{12,8},{9,1... | collective-permute-start | bytes 6152 | tf_op jit(solution)/shard_map/ppermute | solution.py:74
  23.3 3.4 %all-to-all-start.1 = ((bf16[8,32,384]{2,1,0:T(8,128)(2,1)}), bf16[8,32,384]{2,1,0:T(8,128)(2,1)S(1)}, u32[]{:S(2)}, u32[]{:S(2)}) async-start(bf16[8,32,384]{2,1,0:T(8,128)(2,1)} %broadcast_in_dim.14), calls=%async_computation.1 | async-start | bytes 393216 | tf_op jit(solution)/shard_map/all_to_all | solution.py:31
  27.4 8.9 %all-to-all-done.1 = bf16[8,32,384]{2,1,0:T(8,128)(2,1)S(1)} async-done(((bf16[8,32,384]{2,1,0:T(8,128)(2,1)}), bf16[8,32,384]{2,1,0:T(8,128)(2,1)S(1)}, u32[]{:S(2)}, u32[]{:S(2)}) %all-to-all-start.1) | async-done | bytes 196640 | tf_op jit(solution)/shard_map/all_to_all | solution.py:31
  37.4 3.5 %all-to-all-start = ((bf16[4,64,2048]{2,1,0:T(8,128)(2,1)}), bf16[4,64,2048]{2,1,0:T(8,128)(2,1)S(1)}, u32[]{:S(2)}, u32[]{:S(2)}) async-start(bf16[4,64,2048]{2,1,0:T(8,128)(2,1)} %broadcast_in_dim.12), calls=%async_computation | async-start | bytes 2097152 | tf_op jit(solution)/shard_map/all_to_all | solution.py:31
  43.0 2.3 %collective-permute-start.3 = (bf16[256,384]{1,0:T(8,128)(2,1)S(1)}, bf16[256,384]{1,0:T(8,128)(2,1)S(1)}, u32[]{:S(2)}, u32[]{:S(2)}) collective-permute-start(bf16[256,384]{1,0:T(8,128)(2,1)S(1)} %bitcast.39), channel_id=1, source_target_pairs={{0,64},{64,128},{128,192},{192,256},{256,320},{320,384},{384,448},... | collective-permute-start | bytes 589832 | tf_op jit(solution)/shard_map/ppermute | solution.py:38
  45.2 8.9 %collective-permute-start.4 = (bf16[256,384]{1,0:T(8,128)(2,1)S(1)}, bf16[256,384]{1,0:T(8,128)(2,1)S(1)}, u32[]{:S(2)}, u32[]{:S(2)}) collective-permute-start(bf16[256,384]{1,0:T(8,128)(2,1)S(1)} %bitcast.40), channel_id=1, source_target_pairs={{0,448},{64,0},{128,64},{192,128},{256,192},{320,256},{384,320},{4... | collective-permute-start | bytes 589832 | tf_op jit(solution)/shard_map/ppermute | solution.py:38
  54.8 4.8 %collective-permute-start.1 = (bf16[256,2048]{1,0:T(8,128)(2,1)S(1)}, bf16[256,2048]{1,0:T(8,128)(2,1)S(1)}, u32[]{:S(2)}, u32[]{:S(2)}) collective-permute-start(bf16[256,2048]{1,0:T(8,128)(2,1)S(1)} %bitcast.33), channel_id=1, source_target_pairs={{0,4},{4,0},{1,5},{5,1},{2,6},{6,2},{3,7},{7,3},{8,12},{12,8},{9,1... | collective-permute-start | bytes 3145736 | tf_op jit(solution)/shard_map/ppermute | solution.py:74
  61.8 8.6 %collective-permute-start.6 = (bf16[256,384]{1,0:T(8,128)(2,1)S(1)}, bf16[256,384]{1,0:T(8,128)(2,1)S(1)}, u32[]{:S(2)}, u32[]{:S(2)}) collective-permute-start(bf16[256,384]{1,0:T(8,128)(2,1)S(1)} %collective-permute-done.4), channel_id=1, source_target_pairs={{0,448},{64,0},{128,64},{192,128},{256,192},{320,256},{384,320},{4... | collective-permute-start | bytes 589832 | tf_op jit(solution)/shard_map/ppermute | solution.py:38
  70.4 3.2 %collective-permute-done.5 = bf16[256,384]{1,0:T(8,128)(2,1)S(1)} collective-permute-done((bf16[256,384]{1,0:T(8,128)(2,1)S(1)}, bf16[256,384]{1,0:T(8,128)(2,1)S(1)}, u32[]{:S(2)}, u32[]{:S(2)}) %collective-permute-start.5) | collective-permute-done | bytes 196640 | tf_op jit(solution)/shard_map/ppermute | solution.py:38
  77.2 5.3 %collective-permute-start.8 = (bf16[256,384]{1,0:T(8,128)(2,1)S(1)}, bf16[256,384]{1,0:T(8,128)(2,1)S(1)}, u32[]{:S(2)}, u32[]{:S(2)}) collective-permute-start(bf16[256,384]{1,0:T(8,128)(2,1)S(1)} %collective-permute-done.6), channel_id=1, source_target_pairs={{0,448},{64,0},{128,64},{192,128},{256,192},{320,256},{384,320},{4... | collective-permute-start | bytes 589832 | tf_op jit(solution)/shard_map/ppermute | solution.py:38
  82.7 3.0 %collective-permute-start = (bf16[128,2048]{1,0:T(8,128)(2,1)S(1)}, bf16[128,2048]{1,0:T(8,128)(2,1)}, u32[]{:S(2)}, u32[]{:S(2)}) collective-permute-start(bf16[128,2048]{1,0:T(8,128)(2,1)S(1)} %bitcast.42), channel_id=1, source_target_pairs={{0,4},{4,8},{8,12},{12,16},{16,20},{20,24},{24,28},{28,32},{32,36}... | collective-permute-start | bytes 1572872 | tf_op jit(solution)/shard_map/ppermute | solution.py:26
  89.7 5.4 %collective-permute-start.10 = (bf16[128,384]{1,0:T(8,128)(2,1)S(1)}, bf16[128,384]{1,0:T(8,128)(2,1)S(1)}, u32[]{:S(2)}, u32[]{:S(2)}) collective-permute-start(bf16[128,384]{1,0:T(8,128)(2,1)S(1)} %slice.79), channel_id=1, source_target_pairs={{0,448},{64,0},{128,64},{192,128},{256,192},{320,256},{384,320},{4... | collective-permute-start | bytes 294920 | tf_op jit(solution)/shard_map/ppermute | solution.py:38
  95.4 3.0 %collective-permute-done.10 = bf16[128,384]{1,0:T(8,128)(2,1)S(1)} collective-permute-done((bf16[128,384]{1,0:T(8,128)(2,1)S(1)}, bf16[128,384]{1,0:T(8,128)(2,1)S(1)}, u32[]{:S(2)}, u32[]{:S(2)}) %collective-permute-start.10) | collective-permute-done | bytes 98336 | tf_op jit(solution)/shard_map/ppermute | solution.py:38
  100.6 1.9 %slice_add_fusion = f32[1,128,256]{2,1,0:T(8,128)S(1)} fusion(f32[4,128,256]{2,1,0:T(8,128)S(1)} %fusion.18.contrib_ref, f32[]{:T(128)} %bitcast.18, f32[]{:T(128)} %bitcast.17, f32[]{:T(128)} %bitcast.16), kind=kLoop, calls=%fused_computation.30 | loop fusion | flops 196608 | bytes 655372 | tf_op jit(solution)/shard_map/add | solution.py:209
  104.0 5.8 %all-to-all-start.2 = ((f32[64,3,256]{2,1,0:T(4,128)}), f32[64,3,256]{2,1,0:T(4,128)S(1)}, u32[]{:S(2)}, u32[]{:S(2)}) async-start(f32[64,3,256]{2,1,0:T(4,128)} %concatenate.56), calls=%async_computation.2 | async-start | bytes 524288 | tf_op jit(solution)/shard_map/all_to_all | solution.py:135
  111.4 5.2 %collective-permute-start.11 = (bf16[256,128]{1,0:T(8,128)(2,1)S(1)}, bf16[256,128]{1,0:T(8,128)(2,1)S(1)}, u32[]{:S(2)}, u32[]{:S(2)}) collective-permute-start(bf16[256,128]{1,0:T(8,128)(2,1)S(1)} %dynamic-slice_bitcast_fusion.1), channel_id=1, source_target_pairs={{0,4},{4,0},{1,5},{5,1},{2,6},{6,2},{3,7},{7,3},{8,12},{12,8},{9,1... | collective-permute-start | bytes 196616 | tf_op jit(solution)/shard_map/ppermute | solution.py:74
  119.2 3.1 %all-to-all-done.2.parts_ref = f32[64,3,256]{2,1,0:T(4,128)S(1)} async-done(((f32[64,3,256]{2,1,0:T(4,128)}), f32[64,3,256]{2,1,0:T(4,128)S(1)}, u32[]{:S(2)}, u32[]{:S(2)}) %all-to-all-start.2) | async-done | bytes 196640 | tf_op jit(solution)/shard_map/all_to_all | solution.py:135
  123.1 9.3 %all-to-all-start.3 = ((f32[64,2,256]{2,1,0:T(2,128)}), f32[64,2,256]{2,1,0:T(2,128)S(1)}, u32[]{:S(2)}, u32[]{:S(2)}) async-start(f32[64,2,256]{2,1,0:T(2,128)} %shard_map.118), calls=%async_computation.3 | async-start | bytes 262144 | tf_op jit(solution)/shard_map/all_to_all | solution.py:141
  132.5 11.5 %all-to-all-done.3.arrived_ref = f32[64,2,256]{2,1,0:T(2,128)S(1)} async-done(((f32[64,2,256]{2,1,0:T(2,128)}), f32[64,2,256]{2,1,0:T(2,128)S(1)}, u32[]{:S(2)}, u32[]{:S(2)}) %all-to-all-start.3) | async-done | bytes 131104 | tf_op jit(solution)/shard_map/all_to_all | solution.py:141
  144.7 4.1 %collective-permute-start.14 = (bf16[2,128,256]{2,1,0:T(8,128)(2,1)S(1)}, bf16[2,128,256]{2,1,0:T(8,128)(2,1)S(1)}, u32[]{:S(2)}, u32[]{:S(2)}) collective-permute-start(bf16[2,128,256]{2,1,0:T(8,128)(2,1)S(1)} %get-tuple-element.14), channel_id=1, source_target_pairs={{0,4},{4,0},{1,5},{5,1},{2,6},{6,2},{3,7},{7,3},{8,12},{12,8},{9,1... | collective-permute-start | bytes 393224 | tf_op jit(solution)/shard_map/ppermute | solution.py:74
  149.8 6.2 %front.1 = (f32[256,512]{1,0:T(8,128)S(1)}, bf16[256,256]{1,0:T(8,128)(2,1)S(1)}, f32[256,2048]{1,0:T(8,128)S(1)}) custom-call(bf16[384,2048]{1,0:T(8,128)(2,1)S(1)} %pad_maximum_fusion.rows_ref, bf16[2,256,128]{2,1,0:T(8,128)(2,1)S(1)} %pad_maximum_fusion.3.key_ref, bf16[2,256,256]{2,1,0:T(8,128)(2,1)S(1)} %pad_maximum_fusion.2.value_ref, ...), custom_call_target="tpu_custom_call" | custom-call | tf_op jit(solution)/shard_map/front/pallas_call | solution.py:358
  156.0 2.6 %back.1 = bf16[256,2048]{1,0:T(8,128)(2,1)S(1)} custom-call(f32[256,512]{1,0:T(8,128)S(1)} %get-tuple-element.10.inner_ref, bf16[256,256]{1,0:T(8,128)(2,1)S(1)} %get-tuple-element.11.faded_ref, f32[256,2048]{1,0:T(8,128)S(1)} %get-tuple-element.12.part_ref, bf16[2,128,256]{2,1,0:T(8,128)(2,1)S(1)} %get-tuple-element.13.own_ref, ...), custom_call_target="tpu_custom_call" | custom-call | tf_op jit(solution)/shard_map/back/pallas_call | solution.py:379
  158.6 17.3 %all_to_all.25 = bf16[4,64,2048]{2,1,0:T(8,128)(2,1)S(1)} all-to-all(bf16[4,64,2048]{2,1,0:T(8,128)(2,1)S(1)} %bitcast.32), channel_id=1, replica_groups=mesh['sp_0'=8,'sp_1'=8,'sp_2'=2,'tp'=4] {'tp'}, dimensions={0} | all-to-all | bytes 2097152 | tf_op jit(solution)/shard_map/all_to_all | solution.py:48
  (88 shorter events, 31.5 us)
Async XLA Ops:
  6.5 143.3 %all-gather.2.cloned.1.call-start = ((), (), s32[]{:S(2)}) async-start(), calls=%async_computation.5 | async-start | bytes 7925760 | tf_op jit(solution)/shard_map/all_gather | solution.py:418
  9.5 13.0 %collective-permute-start.2 = (bf16[16,384]{1,0:T(8,128)(2,1)S(1)}, bf16[16,384]{1,0:T(8,128)(2,1)S(1)}, u32[]{:S(2)}, u32[]{:S(2)}) collective-permute-start(bf16[16,384]{1,0:T(8,128)(2,1)S(1)} %pad_maximum_fusion.8), channel_id=1, source_target_pairs={{0,4},{4,0},{1,5},{5,1},{2,6},{6,2},{3,7},{7,3},{8,12},{12,8},{9,1... | collective-permute-start | bytes 36872 | tf_op jit(solution)/shard_map/ppermute | solution.py:74
  18.2 23.6 %collective-permute-start.13 = (f32[2,256]{1,0:T(2,128)}, f32[2,256]{1,0:T(2,128)S(1)}, u32[]{:S(2)}, u32[]{:S(2)}) collective-permute-start(f32[2,256]{1,0:T(2,128)} %param.17), channel_id=1, source_target_pairs={{0,4},{4,0},{1,5},{5,1},{2,6},{6,2},{3,7},{7,3},{8,12},{12,8},{9,1... | collective-permute-start | bytes 6152 | tf_op jit(solution)/shard_map/ppermute | solution.py:74
  23.3 13.0 %all-to-all-start.1 = ((bf16[8,32,384]{2,1,0:T(8,128)(2,1)}), bf16[8,32,384]{2,1,0:T(8,128)(2,1)S(1)}, u32[]{:S(2)}, u32[]{:S(2)}) async-start(bf16[8,32,384]{2,1,0:T(8,128)(2,1)} %broadcast_in_dim.14), calls=%async_computation.1 | async-start | bytes 393216 | tf_op jit(solution)/shard_map/all_to_all | solution.py:31
  27.3 13.6 %copy-start.2 = (f32[2,256]{1,0:T(2,128)S(1)}, f32[2,256]{1,0:T(2,128)}, u32[]{:S(2)}) copy-start(f32[2,256]{1,0:T(2,128)} %param.17) | copy-start | bytes 6148
  37.4 17.4 %all-to-all-start = ((bf16[4,64,2048]{2,1,0:T(8,128)(2,1)}), bf16[4,64,2048]{2,1,0:T(8,128)(2,1)S(1)}, u32[]{:S(2)}, u32[]{:S(2)}) async-start(bf16[4,64,2048]{2,1,0:T(8,128)(2,1)} %broadcast_in_dim.12), calls=%async_computation | async-start | bytes 2097152 | tf_op jit(solution)/shard_map/all_to_all | solution.py:31
  43.0 16.9 %collective-permute-start.3 = (bf16[256,384]{1,0:T(8,128)(2,1)S(1)}, bf16[256,384]{1,0:T(8,128)(2,1)S(1)}, u32[]{:S(2)}, u32[]{:S(2)}) collective-permute-start(bf16[256,384]{1,0:T(8,128)(2,1)S(1)} %bitcast.39), channel_id=1, source_target_pairs={{0,64},{64,128},{128,192},{192,256},{256,320},{320,384},{384,448},... | collective-permute-start | bytes 589832 | tf_op jit(solution)/shard_map/ppermute | solution.py:38
  45.2 16.5 %collective-permute-start.4 = (bf16[256,384]{1,0:T(8,128)(2,1)S(1)}, bf16[256,384]{1,0:T(8,128)(2,1)S(1)}, u32[]{:S(2)}, u32[]{:S(2)}) collective-permute-start(bf16[256,384]{1,0:T(8,128)(2,1)S(1)} %bitcast.40), channel_id=1, source_target_pairs={{0,448},{64,0},{128,64},{192,128},{256,192},{320,256},{384,320},{4... | collective-permute-start | bytes 589832 | tf_op jit(solution)/shard_map/ppermute | solution.py:38
  54.8 43.6 %copy-start.1 = (bf16[4,64,2048]{2,1,0:T(8,128)(2,1)}, bf16[4,64,2048]{2,1,0:T(8,128)(2,1)S(1)}, u32[]{:S(2)}) copy-start(bf16[4,64,2048]{2,1,0:T(8,128)(2,1)S(1)} %all-to-all-done) | copy-start | bytes 3145732
  54.8 43.6 %collective-permute-start.1 = (bf16[256,2048]{1,0:T(8,128)(2,1)S(1)}, bf16[256,2048]{1,0:T(8,128)(2,1)S(1)}, u32[]{:S(2)}, u32[]{:S(2)}) collective-permute-start(bf16[256,2048]{1,0:T(8,128)(2,1)S(1)} %bitcast.33), channel_id=1, source_target_pairs={{0,4},{4,0},{1,5},{5,1},{2,6},{6,2},{3,7},{7,3},{8,12},{12,8},{9,1... | collective-permute-start | bytes 3145736 | tf_op jit(solution)/shard_map/ppermute | solution.py:74
  59.8 13.8 %collective-permute-start.5 = (bf16[256,384]{1,0:T(8,128)(2,1)S(1)}, bf16[256,384]{1,0:T(8,128)(2,1)S(1)}, u32[]{:S(2)}, u32[]{:S(2)}) collective-permute-start(bf16[256,384]{1,0:T(8,128)(2,1)S(1)} %collective-permute-done.3), channel_id=1, source_target_pairs={{0,64},{64,128},{128,192},{192,256},{256,320},{320,384},{384,448},... | collective-permute-start | bytes 589832 | tf_op jit(solution)/shard_map/ppermute | solution.py:38
  61.8 15.5 %collective-permute-start.6 = (bf16[256,384]{1,0:T(8,128)(2,1)S(1)}, bf16[256,384]{1,0:T(8,128)(2,1)S(1)}, u32[]{:S(2)}, u32[]{:S(2)}) collective-permute-start(bf16[256,384]{1,0:T(8,128)(2,1)S(1)} %collective-permute-done.4), channel_id=1, source_target_pairs={{0,448},{64,0},{128,64},{192,128},{256,192},{320,256},{384,320},{4... | collective-permute-start | bytes 589832 | tf_op jit(solution)/shard_map/ppermute | solution.py:38
  73.6 13.3 %collective-permute-start.7 = (bf16[256,384]{1,0:T(8,128)(2,1)S(1)}, bf16[256,384]{1,0:T(8,128)(2,1)S(1)}, u32[]{:S(2)}, u32[]{:S(2)}) collective-permute-start(bf16[256,384]{1,0:T(8,128)(2,1)S(1)} %collective-permute-done.5), channel_id=1, source_target_pairs={{0,64},{64,128},{128,192},{192,256},{256,320},{320,384},{384,448},... | collective-permute-start | bytes 589832 | tf_op jit(solution)/shard_map/ppermute | solution.py:38
  77.2 12.5 %collective-permute-start.8 = (bf16[256,384]{1,0:T(8,128)(2,1)S(1)}, bf16[256,384]{1,0:T(8,128)(2,1)S(1)}, u32[]{:S(2)}, u32[]{:S(2)}) collective-permute-start(bf16[256,384]{1,0:T(8,128)(2,1)S(1)} %collective-permute-done.6), channel_id=1, source_target_pairs={{0,448},{64,0},{128,64},{192,128},{256,192},{320,256},{384,320},{4... | collective-permute-start | bytes 589832 | tf_op jit(solution)/shard_map/ppermute | solution.py:38
  82.7 27.1 %collective-permute-start = (bf16[128,2048]{1,0:T(8,128)(2,1)S(1)}, bf16[128,2048]{1,0:T(8,128)(2,1)}, u32[]{:S(2)}, u32[]{:S(2)}) collective-permute-start(bf16[128,2048]{1,0:T(8,128)(2,1)S(1)} %bitcast.42), channel_id=1, source_target_pairs={{0,4},{4,8},{8,12},{12,16},{16,20},{20,24},{24,28},{28,32},{32,36}... | collective-permute-start | bytes 1572872 | tf_op jit(solution)/shard_map/ppermute | solution.py:26
  87.0 8.4 %collective-permute-start.9 = (bf16[128,384]{1,0:T(8,128)(2,1)S(1)}, bf16[128,384]{1,0:T(8,128)(2,1)S(1)}, u32[]{:S(2)}, u32[]{:S(2)}) collective-permute-start(bf16[128,384]{1,0:T(8,128)(2,1)S(1)} %slice.78), channel_id=1, source_target_pairs={{0,64},{64,128},{128,192},{192,256},{256,320},{320,384},{384,448},... | collective-permute-start | bytes 294920 | tf_op jit(solution)/shard_map/ppermute | solution.py:38
  89.7 8.7 %collective-permute-start.10 = (bf16[128,384]{1,0:T(8,128)(2,1)S(1)}, bf16[128,384]{1,0:T(8,128)(2,1)S(1)}, u32[]{:S(2)}, u32[]{:S(2)}) collective-permute-start(bf16[128,384]{1,0:T(8,128)(2,1)S(1)} %slice.79), channel_id=1, source_target_pairs={{0,448},{64,0},{128,64},{192,128},{256,192},{320,256},{384,320},{4... | collective-permute-start | bytes 294920 | tf_op jit(solution)/shard_map/ppermute | solution.py:38
  104.0 18.4 %all-to-all-start.2 = ((f32[64,3,256]{2,1,0:T(4,128)}), f32[64,3,256]{2,1,0:T(4,128)S(1)}, u32[]{:S(2)}, u32[]{:S(2)}) async-start(f32[64,3,256]{2,1,0:T(4,128)} %concatenate.56), calls=%async_computation.2 | async-start | bytes 524288 | tf_op jit(solution)/shard_map/all_to_all | solution.py:135
  111.4 21.0 %collective-permute-start.11 = (bf16[256,128]{1,0:T(8,128)(2,1)S(1)}, bf16[256,128]{1,0:T(8,128)(2,1)S(1)}, u32[]{:S(2)}, u32[]{:S(2)}) collective-permute-start(bf16[256,128]{1,0:T(8,128)(2,1)S(1)} %dynamic-slice_bitcast_fusion.1), channel_id=1, source_target_pairs={{0,4},{4,0},{1,5},{5,1},{2,6},{6,2},{3,7},{7,3},{8,12},{12,8},{9,1... | collective-permute-start | bytes 196616 | tf_op jit(solution)/shard_map/ppermute | solution.py:74
  116.6 33.2 %copy-start = (f32[8]{0:T(128)S(1)}, f32[8]{0:T(128)}, u32[]{:S(2)}) copy-start(f32[8]{0:T(128)} %sink_ref.1) | copy-start | bytes 100
  117.3 31.5 %collective-permute-start.12 = (bf16[256,256]{1,0:T(8,128)(2,1)}, bf16[256,256]{1,0:T(8,128)(2,1)}, u32[]{:S(2)}, u32[]{:S(2)}) collective-permute-start(bf16[256,256]{1,0:T(8,128)(2,1)} %dynamic-slice_bitcast_fusion), channel_id=1, source_target_pairs={{0,4},{4,0},{1,5},{5,1},{2,6},{6,2},{3,7},{7,3},{8,12},{12,8},{9,1... | collective-permute-start | bytes 393224 | tf_op jit(solution)/shard_map/ppermute | solution.py:74
  123.1 20.9 %all-to-all-start.3 = ((f32[64,2,256]{2,1,0:T(2,128)}), f32[64,2,256]{2,1,0:T(2,128)S(1)}, u32[]{:S(2)}, u32[]{:S(2)}) async-start(f32[64,2,256]{2,1,0:T(2,128)} %shard_map.118), calls=%async_computation.3 | async-start | bytes 262144 | tf_op jit(solution)/shard_map/all_to_all | solution.py:141
  144.7 11.3 %collective-permute-start.14 = (bf16[2,128,256]{2,1,0:T(8,128)(2,1)S(1)}, bf16[2,128,256]{2,1,0:T(8,128)(2,1)S(1)}, u32[]{:S(2)}, u32[]{:S(2)}) collective-permute-start(bf16[2,128,256]{2,1,0:T(8,128)(2,1)S(1)} %get-tuple-element.14), channel_id=1, source_target_pairs={{0,4},{4,0},{1,5},{5,1},{2,6},{6,2},{3,7},{7,3},{8,12},{12,8},{9,1... | collective-permute-start | bytes 393224 | tf_op jit(solution)/shard_map/ppermute | solution.py:74
Sparse Core Ops, SparseCore 0:
  10.5 99.3 all-gather.1
